TPU v7x, 256 devices: a whole 4x4x8 slice. The times are simulated.
256 devices in a mesh: gr: 2 (over z_hi), sp: 16 (over z_lo, y), tp: 8 (over x, core).
Axes of the slice: x: 4, y: 4, z: 8 (z_hi: 2, z_lo: 4; z = z_hi * 4 + z_lo), core: 2. Of those that a mesh axis runs over, the one named last changes fastest.
Arguments:
- tokens: bfloat16 [4, 8192, 2048], P('gr', 'sp'), parts along dimension 0, may hold values from -6 to 6
- key_matrix: bfloat16 [2048, 2048], P(None, 'tp'), may hold values from -0.125 to 0.125
- value_matrix: bfloat16 [2048, 2048], P(None, 'tp'), may hold values from -0.125 to 0.125
- gate_matrix: bfloat16 [2048, 16], replicated, may hold values from -0.125 to 0.125
- decay_matrix: bfloat16 [2048, 16], replicated, may hold values from -0.125 to 0.125
- gate_bias_offset: float32 [16], replicated, may hold values from -8 to 1
- head_log_decay_rate: float32 [16], replicated, may hold values from -12 to -2
- extra_log_decay: float32 [4, 8192, 16], P('gr', 'sp', 'tp'), parts along dimension 0, may hold values from -1 to 0
- next_token_query: bfloat16 [4, 16, 128], P('gr', 'tp'), parts along dimension 0, may hold values from -6 to 6
- next_token_key: bfloat16 [4, 16, 128], P('gr', 'tp'), parts along dimension 0, may hold values from -6 to 6
- next_token_value: bfloat16 [4, 16, 128], P('gr', 'tp'), parts along dimension 0, may hold values from -6 to 6
- next_token_gate: float32 [4, 16], P('gr', 'tp'), parts along dimension 0, may hold values from -2 to 2
- readout_norm_gain: float32 [128], replicated, may hold values from 0.1 to 1.9
Outputs:
- state_cache: bfloat16 [4, 16, 128, 128], P('gr', 'tp', 'sp'), parts along dimension 0
- first_read: bfloat16 [4, 16, 128], P('gr', 'tp'), parts along dimension 0
There are 2 independent parts, one for each index of `gr`. A program takes and returns all parts, laid end to end along the dimension named above; an argument that names none is the same for every part. Nothing has to cross between parts.
All inputs are finite; a program needn't handle non-finite values.
Results may differ from a plain program's by a relative error of at most 0.009.
Values sent between devices are 32-bit elements; how exact they have to be, the bound alone decides.
No kernel may reach another device: no remote copies, remote signals or barrier semaphores. Data moves between devices by JAX's collectives and lax.ppermute only.
A program may use at most 64 MiB of HBM per device.

v0:
```python
import math

import jax
import jax.numpy as jnp
from jax import lax
from jax.sharding import Mesh
from jax.sharding import PartitionSpec as P

BLOCK = 64
SP = ("sp_0", "sp_1")


def filled_with(value, identity):
    return jnp.zeros_like(value) + jnp.asarray(identity, value.dtype)


def entering(value, axes, combine, identity):
    before = start = filled_with(value, identity)
    so_far = value
    for axis in reversed(axes):
        count, position = (lax.axis_size(axis), lax.axis_index(axis))
        pieces = lax.all_gather(so_far, axis)
        inside, so_far = (start, start)
        for k in reversed(range(count)):
            passed = k > position
            so_far = combine(so_far, pieces[k])
            inside = jnp.where(passed, so_far, inside)
        before = combine(inside, before)
    return before


def split_up(value, dim, count):
    shape = value.shape
    pieces = value.reshape(*shape[:dim], count, shape[dim] // count, *shape[dim + 1 :])
    return jnp.moveaxis(pieces, dim, 0)


def summed_on_arrival(value, axis, dim):
    count = lax.axis_size(axis)
    pieces = lax.all_to_all(split_up(value, dim, count), axis, 0, 0, tiled=True)
    return jnp.sum(pieces, axis=0)


def copy_for_each(value, axis):
    count = lax.axis_size(axis)
    return lax.all_to_all(
        jnp.broadcast_to(value[None], (count, *value.shape)), axis, 0, 0, tiled=True
    )


def taken_together(value, axis):
    return copy_for_each(value, axis).sum(axis=0)


def together(arrays, axis):
    ends = [0]
    for a in arrays:
        ends.append(ends[-1] + a.size)
    so_far = taken_together(jnp.concatenate([a.ravel() for a in arrays]), axis)
    return tuple((so_far[b:e].reshape(a.shape) for a, b, e in zip(arrays, ends, ends[1:])))


def unit_rows(array):
    return array * lax.rsqrt(jnp.sum(array * array, axis=-1, keepdims=True) + 1e-06)


def exact_matmul(left, right):
    return jnp.matmul(left, right, precision=lax.Precision.HIGHEST)


def to_blocks(array, block_len):
    seq_count, length, head_count = array.shape[:3]
    tail_dims = array.shape[3:]
    split_view = array.reshape((seq_count, length // block_len, block_len, head_count) + tail_dims)
    axes_order = (1, 0, 3, 2) + tuple(range(4, split_view.ndim))
    return jnp.transpose(split_view, axes_order)


def block_terms(key_rows, value_rows, beta_rows, decay_logarithm):
    block_len = key_rows.shape[-2]
    cumulative = jnp.cumsum(decay_logarithm, axis=-1)
    positions = jnp.arange(block_len)
    inclusive = positions[:, None] >= positions[None, :]
    strictly = positions[:, None] > positions[None, :]
    decay_mat = jnp.exp(
        jnp.where(inclusive, cumulative[..., :, None] - cumulative[..., None, :], -jnp.inf)
    )
    weighted = key_rows * beta_rows[..., None]
    lower_part = jnp.where(
        strictly,
        jnp.einsum("...id,...jd->...ij", weighted, key_rows, precision=lax.Precision.HIGHEST)
        * decay_mat,
        0.0,
    )
    identity = jnp.eye(block_len, dtype=jnp.float32)
    power_term = -lower_part
    inverse = identity + power_term
    for _ in range(block_len.bit_length() - 2):
        power_term = exact_matmul(power_term, power_term)
        inverse = exact_matmul(inverse, identity + power_term)
    fresh_part = exact_matmul(inverse, value_rows * beta_rows[..., None])
    pull_part = exact_matmul(inverse, weighted * jnp.exp(cumulative)[..., None])
    last_cum = cumulative[..., -1:]
    outward = key_rows * jnp.exp(last_cum - cumulative)[..., None]
    carry_decay = jnp.exp(last_cum)
    return (fresh_part, pull_part, outward, carry_decay)


def advance(state_mat, pieces):
    fresh_part, pull_part, outward, carry_decay = pieces
    update = fresh_part - jnp.einsum(
        "shck,shkv->shcv", pull_part, state_mat, precision=lax.Precision.HIGHEST
    )
    state_mat = state_mat * carry_decay[..., None] + jnp.einsum(
        "shck,shcv->shkv", outward, update, precision=lax.Precision.HIGHEST
    )
    return (state_mat, None)


def shards(
    tokens,
    key_matrix,
    value_matrix,
    gate_matrix,
    decay_matrix,
    gate_bias_offset,
    head_log_decay_rate,
    extra_log_decay,
    next_token_query,
    next_token_key,
    next_token_value,
    next_token_gate,
    readout_norm_gain,
):
    seq_count, seg_len, width = tokens.shape
    head_dim = next_token_key.shape[-1]
    local_heads = key_matrix.shape[1] // head_dim
    first_head = lax.axis_index("tp") * local_heads
    flat = tokens.reshape(seq_count * seg_len, width)
    key_proj = jnp.dot(flat, key_matrix, preferred_element_type=jnp.float32)
    value_proj = jnp.dot(flat, value_matrix, preferred_element_type=jnp.float32)
    key_rows = unit_rows(
        jax.nn.silu(key_proj).reshape(seq_count, seg_len, local_heads, head_dim)
    ).astype(jnp.bfloat16)
    value_rows = (
        jax.nn.silu(value_proj)
        .reshape(seq_count, seg_len, local_heads, head_dim)
        .astype(jnp.bfloat16)
    )
    gate_cols = lax.dynamic_slice_in_dim(gate_matrix, first_head, local_heads, 1)
    decay_cols = lax.dynamic_slice_in_dim(decay_matrix, first_head, local_heads, 1)
    shift_part = lax.dynamic_slice_in_dim(gate_bias_offset, first_head, local_heads, 0)
    rate_component = lax.dynamic_slice_in_dim(head_log_decay_rate, first_head, local_heads, 0)
    gate_pre = jnp.dot(flat, gate_cols, preferred_element_type=jnp.float32).reshape(
        seq_count, seg_len, local_heads
    )
    decay_logits = jnp.dot(flat, decay_cols, preferred_element_type=jnp.float32).reshape(
        seq_count, seg_len, local_heads
    )
    beta_rows = jax.nn.sigmoid(gate_pre + shift_part)
    decay_logarithm = -jnp.exp(rate_component) * jax.nn.softplus(decay_logits) + extra_log_decay
    fresh_part, pull_part, outward, carry_decay = block_terms(
        to_blocks(key_rows.astype(jnp.float32), BLOCK),
        to_blocks(value_rows.astype(jnp.float32), BLOCK),
        to_blocks(beta_rows, BLOCK),
        to_blocks(decay_logarithm, BLOCK),
    )
    fresh_aug = jnp.concatenate([jnp.zeros_like(fresh_part), fresh_part], axis=-1)
    identity_mat = jnp.broadcast_to(
        jnp.eye(head_dim, dtype=jnp.float32), (seq_count, local_heads, head_dim, head_dim)
    )
    zero_mat = jnp.zeros((seq_count, local_heads, head_dim, head_dim), jnp.float32)
    start_aug = jnp.concatenate([identity_mat, zero_mat], axis=-1)
    final_aug, _ = lax.scan(advance, start_aug, (fresh_aug, pull_part, outward, carry_decay))
    decay_map = final_aug[..., :head_dim]
    offset = final_aug[..., head_dim:]

    def chain(earlier, later):
        return exact_matmul(earlier, later)

    later_maps = entering(decay_map, SP, chain, identity_mat)
    term = exact_matmul(later_maps, offset)
    state_rows = summed_on_arrival(term, SP, 2)
    row_count = state_rows.shape[2]
    row_start = lax.axis_index(SP) * row_count
    query_unit = unit_rows(next_token_query.astype(jnp.float32))
    key_unit = unit_rows(next_token_key.astype(jnp.float32))
    key_part = lax.dynamic_slice_in_dim(key_unit, row_start, row_count, 2)
    query_part = lax.dynamic_slice_in_dim(query_unit, row_start, row_count, 2)
    key_read, query_read = together(
        (
            jnp.einsum("shk,shkv->shv", key_part, state_rows, precision=lax.Precision.HIGHEST),
            jnp.einsum("shk,shkv->shv", query_part, state_rows, precision=lax.Precision.HIGHEST),
        ),
        SP,
    )
    beta_new = jax.nn.sigmoid(next_token_gate)
    value_new = next_token_value.astype(jnp.float32)
    intersection = jnp.sum(key_unit * query_unit, axis=-1)
    missing = value_new - key_read
    updated = (
        state_rows + beta_new[..., None, None] * key_part[..., :, None] * missing[..., None, :]
    )
    read_vec = (query_read + (beta_new * intersection)[..., None] * missing) / math.sqrt(head_dim)
    normed = (
        read_vec
        * lax.rsqrt(jnp.mean(read_vec * read_vec, axis=-1, keepdims=True) + 1e-06)
        * readout_norm_gain
    )
    return (updated.astype(jnp.bfloat16), normed.astype(jnp.bfloat16))


def solution(mesh):
    finer = Mesh(
        mesh.devices.reshape(mesh.shape["gr"], 4, 4, mesh.shape["tp"]), ("gr", "sp_0", "sp_1", "tp")
    )
    in_specs = (
        P("gr", SP, None),
        P(None, "tp"),
        P(None, "tp"),
        P(),
        P(),
        P(),
        P(),
        P("gr", SP, "tp"),
        P("gr", "tp", None),
        P("gr", "tp", None),
        P("gr", "tp", None),
        P("gr", "tp"),
        P(),
    )
    out_specs = (P("gr", "tp", SP, None), P("gr", "tp", None))
    return jax.shard_map(
        shards, mesh=finer, in_specs=in_specs, out_specs=out_specs, check_vma=False
    )
```

profile of v0, /device:TPU:2, one launch (start us, length us, event | category | flops | bytes accessed | tf_op | source)
XLA Modules:
  0.0 188.4 jit_solution(18166529397369116090)
XLA Ops:
  8.1 3.4 %fusion.67 = f32[2,1024]{1,0:T(2,128)S(1)} fusion(bf16[1024,2048]{1,0:T(8,128)(2,1)} %bitcast.111, bf16[2048,16]{0,1:T(8,128)(2,1)} %param.19, s32[]{:T(128)S(6)} %select_n.72), kind=kOutput, calls=%fused_computation.91 | convolution fusion | flops 8388608 | bytes 4210692 | tf_op jit(solution)/shard_map/dot_general | solution.py:157
  12.9 4.4 %divide_multiply_fusion = (f32[1024,256]{1,0:T(8,128)}, f32[1024,256]{1,0:T(8,128)S(1)}) fusion(bf16[1024,2048]{1,0:T(8,128)(2,1)} %bitcast.112, bf16[2048,256]{1,0:T(8,128)(2,1)S(1)} %copy-done), kind=kOutput, calls=%fused_computation.36 | convolution fusion | flops 1075052544 | bytes 7340032 | tf_op jit(solution)/shard_map/dot_general | solution.py:140
  19.3 1.8 reshape.131
  21.1 3.4 %convolution_bitcast_fusion.1 = f32[1024,2]{0,1:T(2,128)S(1)} fusion(bf16[1024,2048]{1,0:T(8,128)(2,1)} %bitcast.113, bf16[2048,16]{0,1:T(8,128)(2,1)} %param.18, s32[]{:T(128)S(6)} %select_n.72), kind=kOutput, calls=%fused_computation.19 | convolution fusion | flops 8388608 | bytes 4210692 | tf_op jit(solution)/shard_map/dot_general | solution.py:154
  24.7 1.5 convert_multiply_fusion.1
  38.5 2.3 %fusion.24 = f32[1024,256]{1,0:T(8,128)} fusion(bf16[1024,2048]{1,0:T(8,128)(2,1)S(1)} %bitcast.114, bf16[2048,256]{1,0:T(8,128)(2,1)S(1)} %copy-done.10), kind=kOutput, calls=%fused_computation.37 | convolution fusion | flops 1075314688 | bytes 6291456 | tf_op jit(solution)/shard_map/dot_general | solution.py:141
  40.8 2.7 %reshape.136 = f32[2,8,64,2,128]{4,3,2,1,0:T(2,128)} reshape(f32[1024,256]{1,0:T(8,128)} %fusion.24) | data formatting | bytes 2097152 | tf_op jit(solution)/shard_map/transpose | solution.py:76
  44.7 2.6 %fusion.10 = f32[8,2,2,64,128]{4,3,2,1,0:T(8,128)S(1)} fusion(f32[8,2,2,64,64]{4,3,2,1,0:T(8,128)S(1)} %fusion.83, bf16[8,2,2,64,128]{4,3,2,1,0:T(8,128)(2,1)} %copy-done.3, f32[8,2,2,64]{3,2,1,0:T(2,128)S(1)} %copy.122, f32[8,2,2,64]{3,2,1,0:T(2,128)S(1)} %copy.118), kind=kOutput, calls=%fused_computation.20 | convolution fusion | flops 202113024 | bytes 2113536 | tf_op jit(solution)/shard_map/dot_general | solution.py:68
  48.5 1.6 concatenate.10
  50.4 24.6 %while.10 = (s32[]{:T(128)}, f32[2,2,128,256]{3,2,1,0:T(8,128)S(1)}, f32[8,2,2,1]{2,1,3,0:T(2,128)S(1)}, f32[8,2,2,64,128]{4,3,2,1,0:T(8,128)}, f32[8,2,2,64,256...) while((s32[]{:T(128)}, f32[2,2,128,256]{3,2,1,0:T(8,128)S(1)}, ...), condition=%wide.region_3.4_spmd, body=%wide.region_2.3_spmd.sunk | while | flops 201654272 | bytes 2623105 | solution.py:174
  51.8 1.6 convolution_add_fusion.3
  54.9 1.7 convolution_add_fusion.3
  58.0 1.7 convolution_add_fusion.3
  61.1 1.7 convolution_add_fusion.3
  64.1 1.7 convolution_add_fusion.3
  67.2 1.7 convolution_add_fusion.3
  70.3 1.7 convolution_add_fusion.3
  73.3 1.7 convolution_add_fusion.3
  75.8 29.7 %all-gather.5.cloned.1.call-done = f32[8,2,128,128]{3,2,1,0:T(8,128)} async-done(((f32[2,2,128,128]{3,2,1,0:T(8,128)}), f32[8,2,128,128]{3,2,1,0:T(8,128)}) %all-gather.5.cloned.1.call-update) | async-done | bytes 1048592 | tf_op jit(solution)/shard_map/all_gather | solution.py:22
  109.6 2.0 %fusion.41 = f32[2,2,128,128]{3,2,1,0:T(8,128)} fusion(f32[2,2,128,128]{3,2,1,0:T(8,128)S(1)} %fusion.43, f32[8,2,128,128]{3,2,1,0:T(8,128)} %all-gather.5.cloned.1.call-done), kind=kOutput, calls=%fused_computation.55 | convolution fusion | flops 100663296 | bytes 786432 | tf_op jit(solution)/shard_map/dot_general | solution.py:68
  112.3 33.4 %all-gather.7.cloned.1.call-done = f32[8,2,128,128]{3,2,1,0:T(8,128)} async-done(((f32[2,2,128,128]{3,2,1,0:T(8,128)}), f32[8,2,128,128]{3,2,1,0:T(8,128)}) %all-gather.7.cloned.1.call-update) | async-done | bytes 1048592 | tf_op jit(solution)/shard_map/all_gather | solution.py:22
  152.7 4.7 %all-to-all-start = ((f32[16,2,2,8,128]{4,3,2,1,0:T(8,128)}), f32[16,2,2,8,128]{4,3,2,1,0:T(8,128)S(1)}, u32[]{:S(2)}, u32[]{:S(2)}) async-start(f32[16,2,2,8,128]{4,3,2,1,0:T(8,128)} %bitcast.97), calls=%async_computation | async-start | bytes 524288 | tf_op jit(solution)/shard_map/all_to_all | solution.py:40
  157.7 10.0 %all-to-all-done = f32[16,2,2,8,128]{4,3,2,1,0:T(8,128)S(1)} async-done(((f32[16,2,2,8,128]{4,3,2,1,0:T(8,128)}), f32[16,2,2,8,128]{4,3,2,1,0:T(8,128)S(1)}, u32[]{:S(2)}, u32[]{:S(2)}) %all-to-all-start) | async-done | bytes 262176 | tf_op jit(solution)/shard_map/all_to_all | solution.py:40
  168.1 12.0 %all_to_all.11 = f32[16,1,1024]{2,1,0:T(1,128)S(1)} all-to-all(f32[16,1,1024]{2,1,0:T(1,128)S(1)} %broadcast_in_dim.34), channel_id=1, replica_groups=mesh['gr'=2,'sp_0'=4,'sp_1'=4,'tp'=8] {'sp_0','sp_1'}, dimensions={0} | all-to-all | bytes 131072 | tf_op jit(solution)/shard_map/all_to_all | solution.py:46
  (111 shorter events, 44.8 us)
Async XLA Ops:
  7.2 5.7 %copy-start = (bf16[2048,256]{1,0:T(8,128)(2,1)S(1)}, bf16[2048,256]{1,0:T(8,128)(2,1)}, u32[]{:S(2)}) copy-start(bf16[2048,256]{1,0:T(8,128)(2,1)} %param.16) | copy-start | bytes 3145732
  7.2 4.3 %copy-start.4 = (f32[2,512,2]{1,2,0:T(2,128)S(1)}, f32[2,512,2]{1,2,0:T(2,128)}, u32[]{:S(2)}) copy-start(f32[2,512,2]{1,2,0:T(2,128)} %param.22) | copy-start | bytes 24580
  7.2 98.3 %all-gather.5.cloned.1.call-start = ((), (), s32[]{:S(2)}) async-start(), calls=%async_computation.2 | async-start | bytes 1310720 | tf_op jit(solution)/shard_map/all_gather | solution.py:22
  19.0 5.6 %copy-start.11 = (f32[16]{0:T(128)S(1)}, f32[16]{0:T(128)}, u32[]{:S(2)}) copy-start(f32[16]{0:T(128)} %param.20) | copy-start | bytes 196
  26.2 1.1 copy-start.3
  34.6 3.9 %copy-start.1 = (bf16[2,512,2048]{2,1,0:T(8,128)(2,1)S(1)}, bf16[2,512,2048]{2,1,0:T(8,128)(2,1)}, u32[]{:S(2)}) copy-start(bf16[2,512,2048]{2,1,0:T(8,128)(2,1)} %param.15) | copy-start | bytes 12582916
  34.6 3.9 %copy-start.10 = (bf16[2048,256]{1,0:T(8,128)(2,1)S(1)}, bf16[2048,256]{1,0:T(8,128)(2,1)}, u32[]{:S(2)}) copy-start(bf16[2048,256]{1,0:T(8,128)(2,1)} %param.17) | copy-start | bytes 3145732
  43.5 3.8 %copy-start.2 = (f32[2,8,64,2,128]{4,3,2,1,0:T(2,128)S(1)}, f32[2,8,64,2,128]{4,3,2,1,0:T(2,128)}, u32[]{:S(2)}) copy-start(f32[2,8,64,2,128]{4,3,2,1,0:T(2,128)} %reshape.136) | copy-start | bytes 3145732
  50.4 61.3 %copy-start.6 = (bf16[2,2,128]{2,1,0:T(2,128)(2,1)S(1)}, bf16[2,2,128]{2,1,0:T(2,128)(2,1)}, u32[]{:S(2)}) copy-start(bf16[2,2,128]{2,1,0:T(2,128)(2,1)} %param.23) | copy-start | bytes 3076
  50.4 61.4 %copy-start.5 = (bf16[2,2,128]{2,1,0:T(2,128)(2,1)S(1)}, bf16[2,2,128]{2,1,0:T(2,128)(2,1)}, u32[]{:S(2)}) copy-start(bf16[2,2,128]{2,1,0:T(2,128)(2,1)} %param.24) | copy-start | bytes 3076
  75.8 70.0 %all-gather.7.cloned.1.call-start = ((), (), s32[]{:S(2)}) async-start(), calls=%async_computation.3 | async-start | bytes 1310720 | tf_op jit(solution)/shard_map/all_gather | solution.py:22
  109.6 48.0 %copy-start.8 = (f32[2,2]{1,0:T(2,128)S(1)}, f32[2,2]{1,0:T(2,128)}, u32[]{:S(2)}) copy-start(f32[2,2]{1,0:T(2,128)} %param.26) | copy-start | bytes 52
  111.6 68.4 %copy-start.7 = (bf16[2,2,128]{2,1,0:T(2,128)(2,1)S(1)}, bf16[2,2,128]{2,1,0:T(2,128)(2,1)}, u32[]{:S(2)}) copy-start(bf16[2,2,128]{2,1,0:T(2,128)(2,1)} %param.25) | copy-start | bytes 3076
  111.7 69.3 %copy-start.9 = (f32[128]{0:T(128)S(1)}, f32[128]{0:T(128)}, u32[]{:S(2)}) copy-start(f32[128]{0:T(128)} %param.27) | copy-start | bytes 1540
  152.7 15.0 %all-to-all-start = ((f32[16,2,2,8,128]{4,3,2,1,0:T(8,128)}), f32[16,2,2,8,128]{4,3,2,1,0:T(8,128)S(1)}, u32[]{:S(2)}, u32[]{:S(2)}) async-start(f32[16,2,2,8,128]{4,3,2,1,0:T(8,128)} %bitcast.97), calls=%async_computation | async-start | bytes 524288 | tf_op jit(solution)/shard_map/all_to_all | solution.py:40
Sparse Core Ops, SparseCore 0:
  75.9 29.6 all-gather.4
  111.8 33.9 all-gather.6
where the time goes:
time: 189 us; the launch traced here: 188 us
  waiting for transfers between devices  73.2 us (39%)
  matrix products  67.7 us (36%)
  between operations  14.5 us (8%)
  blocking collectives  12 us (6%)
  local copies, waits for them, and re-layouts  9.21 us (5%)
  other arithmetic  6.69 us (4%)
  starting transfers between devices  4.81 us (3%)
    all_gather x2, waiting for transfers between devices, entering(): pieces = lax.all_gather(so_far, axis)  63.2 us
    dot_general x23, matrix products, exact_matmul(): return jnp.matmul(left, right, precision=lax.Precision.HIGHEST)  28.6 us
    dot_general x8, matrix products, advance(): jnp.einsum('shck,shcv->shkv', outward, update, precision=lax.Precision.HI...  13.2 us
    all_to_all x1, blocking collectives, copy_for_each(): lax.all_to_all(jnp.broadcast_to(value[None], (count, *value.shape)), axis...  12 us
    dot_general x8, matrix products, advance(): jnp.einsum('shck,shkv->shcv', pull_part, state_mat, precision=lax.Precisi...  11 us
    all_to_all x1, waiting for transfers between devices, summed_on_arrival(): pieces = lax.all_to_all(split_up(value, dim, count), axis, 0, 0, tiled=True)  9.99 us
    all_to_all x1, starting transfers between devices, summed_on_arrival(): pieces = lax.all_to_all(split_up(value, dim, count), axis, 0, 0, tiled=True)  4.73 us
    dot_general x1, matrix products, shards(): key_proj = jnp.dot(flat, key_matrix, preferred_element_type=jnp.float32)  4.43 us
  transfers between devices with their start and end apart: 3, of which 3 were waited for; matrix products, arithmetic and copies ran while one was open for 0% of the time, Pallas kernels for 0%

commit v1 on v0

v1 whole, which is shorter than its diff:
```python
import math

import jax
import jax.numpy as jnp
from jax import lax
from jax.experimental import pallas as pl
from jax.experimental.pallas import tpu as pltpu
from jax.sharding import Mesh
from jax.sharding import PartitionSpec as P

SP = ("sp_0", "sp_1")
CH = 128
F32 = jnp.float32
BF16 = jnp.bfloat16
AB = (((1,), (0,)), ((), ()))
ABT = (((1,), (1,)), ((), ()))
ATB = (((0,), (0,)), ((), ()))


def dot1(a, b, dims=AB):
    return lax.dot_general(a.astype(BF16), b.astype(BF16), dims, preferred_element_type=F32)


def split(a):
    hi = a.astype(BF16)
    return hi, (a - hi.astype(F32)).astype(BF16)


def dot3(a, b, dims=AB):
    ah, al = split(a)
    bh, bl = split(b)
    return dot1(ah, bh, dims) + (dot1(ah, bl, dims) + dot1(al, bh, dims))


def iota(shape, dim):
    return lax.broadcasted_iota(jnp.int32, shape, dim)


def unit_rows(a):
    return a * lax.rsqrt(jnp.sum(a * a, axis=-1, keepdims=True) + 1e-06)


def silu(a):
    return a * (1.0 / (1.0 + jnp.exp(-a)))


def inverse_of(m_mat):
    row = iota((CH, CH), 0)
    col = iota((CH, CH), 1)
    eye = jnp.where(row == col, 1.0, 0.0)
    p1 = jnp.where(row // 16 == col // 16, -m_mat, 0.0)
    inv = eye + p1
    p1 = p1.astype(BF16)
    p2 = dot1(p1, p1).astype(BF16)
    both = dot1(p2, jnp.concatenate([p2, inv.astype(BF16)], axis=1))
    inv = inv + both[:, CH:]
    p4 = both[:, :CH].astype(BF16)
    both = dot1(p4, jnp.concatenate([p4, inv.astype(BF16)], axis=1))
    inv = inv + both[:, CH:]
    p8 = both[:, :CH]
    inv = inv + dot1(p8, inv)
    for b in (16, 32, 64):
        lower = [slice(s + b, s + 2 * b) for s in range(0, CH, 2 * b)]
        m_rows = jnp.concatenate(
            [
                jnp.where(col[r, :] // b == (r.start // b - 1), m_mat[r, :], 0.0)
                for r in lower
            ],
            axis=0,
        )
        t_rows = jnp.concatenate([inv[r, :] for r in lower], axis=0)
        y = dot1(m_rows, inv)
        pieces = []
        for g in range(len(lower)):
            part = y[g * b : (g + 1) * b, :]
            pieces += [part, part]
        new_rows = t_rows - dot1(t_rows, jnp.concatenate(pieces, axis=0))
        pieces = []
        for g, r in enumerate(lower):
            pieces += [inv[r.start - b : r.start, :], new_rows[g * b : (g + 1) * b, :]]
        inv = jnp.concatenate(pieces, axis=0)
    return inv


def maps_kernel(
    x_hbm, wk_hbm, wv_hbm, gate_ref, decay_ref, bias_ref, rate_ref, extra_ref,
    o0, o1, o2, o3,
    xbuf, wkbuf, wvbuf, kbuf, vbuf, gsc, dsc, esc, sbuf, sems,
):
    seqs = xbuf.shape[0] // 2
    first_head = lax.axis_index("tp") * 2
    here = lax.axis_index("sp_1")
    tiles, tile, width = xbuf.shape
    copies = []
    for t in range(tiles):
        s, half = divmod(t, tiles // seqs)
        copies.append(
            pltpu.make_async_copy(x_hbm.at[s, pl.ds(half * tile, tile)], xbuf.at[t], sems.at[t])
        )
    wk_copy = pltpu.make_async_copy(wk_hbm, wkbuf, sems.at[tiles])
    wv_copy = pltpu.make_async_copy(wv_hbm, wvbuf, sems.at[tiles + 1])
    wk_copy.start()
    copies[0].start()
    wv_copy.start()
    for c in copies[1:]:
        c.start()
    per_tile = tile // CH
    gates = jnp.concatenate([gate_ref[...], decay_ref[...]], axis=0)
    heads = gate_ref.shape[0]
    pick = iota((heads, tile), 0)
    wk_copy.wait()
    for t in range(tiles):
        copies[t].wait()
        if t == 0:
            wv_copy.wait()
        x = xbuf[t]
        kp = silu(lax.dot_general(x, wkbuf[...], AB, preferred_element_type=F32))
        rows = slice(t * tile, (t + 1) * tile)
        for h in range(2):
            lanes = slice(h * CH, (h + 1) * CH)
            kbuf[rows, lanes] = unit_rows(kp[:, lanes]).astype(BF16)
        vp = silu(lax.dot_general(x, wvbuf[...], AB, preferred_element_type=F32))
        vbuf[rows, :] = vp.astype(BF16)
        gt = lax.dot_general(gates, x, ABT, preferred_element_type=F32)
        for h in range(2):
            mine = pick == first_head + h
            g_row = jnp.sum(jnp.where(mine, gt[:heads], 0.0), axis=0, keepdims=True)
            d_row = jnp.sum(jnp.where(mine, gt[heads:], 0.0), axis=0, keepdims=True)
            for q in range(per_tile):
                r = 2 * (t * per_tile + q) + h
                gsc[r : r + 1, :] = g_row[:, q * CH : (q + 1) * CH]
                dsc[r : r + 1, :] = d_row[:, q * CH : (q + 1) * CH]
    count = gsc.shape[0]
    chunks = count // 2
    per_seq = chunks // seqs
    for m in range(chunks):
        s, n = divmod(m, per_seq)
        esc[2 * m : 2 * m + 2, :] = extra_ref[s, :, n * CH : (n + 1) * CH]
    odd = iota((count, CH), 0) % 2 == 1
    lane = iota((count, CH), 1)
    bias = jnp.where(odd, bias_ref[first_head + 1], bias_ref[first_head])
    rate = jnp.where(odd, rate_ref[first_head + 1], rate_ref[first_head])
    beta = 1.0 / (1.0 + jnp.exp(-(gsc[...] + bias)))
    z = dsc[...]
    soft = jnp.maximum(z, 0.0) + jnp.log1p(jnp.exp(-jnp.abs(z)))
    cum = -jnp.exp(rate) * soft + esc[...]
    d = 1
    while d < CH:
        cum = cum + jnp.where(lane >= d, pltpu.roll(cum, d, 1), 0.0)
        d *= 2
    total = jnp.broadcast_to(cum[:, CH - 1 : CH], (count, CH))
    carry = jnp.exp(total)
    reach = jnp.exp(total - cum)
    ecum = jnp.exp(cum)
    columns = jnp.transpose(
        jnp.concatenate([beta, cum, reach, jnp.zeros((CH - 3 * count, CH), F32)], axis=0)
    )
    row = iota((CH, CH), 0)
    col = iota((CH, CH), 1)
    eye = jnp.where(row == col, 1.0, 0.0)
    for s in range(seqs):
        for h in range(2):
            state = None
            for n in range(per_seq):
                m = s * per_seq + n
                r = 2 * m + h
                rows = slice(m * CH, (m + 1) * CH)
                lanes = slice(h * CH, (h + 1) * CH)
                k = kbuf[rows, lanes]
                v = vbuf[rows, lanes]
                gram = lax.dot_general(k, k, ABT, preferred_element_type=F32)
                gap = jnp.minimum(columns[:, count + r : count + r + 1] - cum[r : r + 1, :], 0.0)
                m_mat = jnp.where(row > col, columns[:, r : r + 1] * gram * jnp.exp(gap), 0.0)
                inv = inverse_of(m_mat)
                u = columns[:, 2 * count + r : 2 * count + r + 1] * inv * beta[r : r + 1, :]
                u2 = u * ecum[r : r + 1, :]
                uh, ul = split(u)
                u2h, u2l = split(u2)
                fresh = dot1(uh, v) + dot1(ul, v)
                pull = dot1(u2h, k) + dot1(u2l, k)
                wh, wl = split(jnp.concatenate([pull, fresh], axis=1))
                both = dot1(k, wh, ATB) + dot1(k, wl, ATB)
                dmap = both[:, :CH]
                c_row = carry[r : r + 1, :]
                if state is None:
                    state = jnp.concatenate([c_row * eye - dmap, both[:, CH:]], axis=1)
                else:
                    moved = dot3(dmap, state)
                    state = jnp.concatenate([c_row, c_row], axis=1) * state - moved
                    state = state + jnp.concatenate([jnp.zeros((CH, CH), F32), both[:, CH:]], axis=1)
            sbuf[2 * s + h, :CH, :] = state[:, :CH]
            sbuf[2 * s + h, CH:, :] = state[:, CH:]
    for k, o in enumerate((o0, o1, o2, o3)):
        o[...] = sbuf[lax.rem(here + k, 4)]


def ordered(refs, scr, here):
    for k, ref in enumerate(refs):
        scr[lax.rem(here + 4 - k, 4)] = ref[...]


def segments_kernel(r0, r1, r2, r3, o0, o1, o2, o3, scr, bscr):
    ordered((r0, r1, r2, r3), scr, lax.axis_index("sp_1"))
    there = lax.axis_index("sp_0")
    state = jnp.concatenate([scr[0, :CH, :], scr[0, CH:, :]], axis=1)
    for t in range(1, 4):
        state = dot3(scr[t, :CH, :], state)
        state = state + jnp.concatenate([jnp.zeros((CH, CH), F32), scr[t, CH:, :]], axis=1)
    bscr[...] = jnp.transpose(state[:, CH:])
    for k, o in enumerate((o0, o1, o2, o3)):
        q = lax.rem(there + k, 4)
        o[:CH, :] = state[:, :CH]
        o[CH:, :] = bscr[pl.ds(pl.multiple_of(q * 32, 32), 32), :]


def row_of(ref, s, h):
    two = ref[s].astype(F32)
    return jnp.sum(jnp.where(iota(two.shape, 0) == h, two, 0.0), axis=0, keepdims=True)


def columns_kernel(r0, r1, r2, r3, query_ref, key_ref, value_ref, gate_ref, out, scr, wide):
    part = lax.axis_index("sp_0")
    pair = lax.axis_index("sp_1")
    ordered((r0, r1, r2, r3), scr, part)
    f = scr[0, CH:, :]
    for g in range(1, 4):
        f = dot3(f, scr[g, :CH, :], ABT) + scr[g, CH:, :]
    s = pair // 2
    h = lax.rem(pair, 2)
    qn = unit_rows(row_of(query_ref, s, h))
    kn = unit_rows(row_of(key_ref, s, h))
    vn = row_of(value_ref, s, h)
    bn = 1.0 / (1.0 + jnp.exp(-jnp.full((1, CH), gate_ref[s, h], F32)))
    count = f.shape[0]
    mine = iota((count, CH), 1) == iota((count, CH), 0) + part * count
    vn_col = jnp.sum(jnp.where(mine, jnp.broadcast_to(vn, (count, CH)), 0.0), axis=1, keepdims=True)
    missing = vn_col - jnp.sum(f * kn, axis=1, keepdims=True)
    query_read = jnp.sum(f * qn, axis=1, keepdims=True)
    meet = jnp.sum(kn * qn, axis=1, keepdims=True)
    read = (query_read + (bn[:, :1] * meet) * missing) / math.sqrt(CH)
    wide[...] = jnp.zeros_like(wide)
    wide[pl.ds(pl.multiple_of(part * count, 32), count), :] = f + missing * (bn * kn)
    state = jnp.transpose(wide[...])
    read_row = jnp.sum(jnp.where(mine, jnp.broadcast_to(read, (count, CH)), 0.0), axis=0, keepdims=True)
    read_rows = jnp.broadcast_to(read_row, (8, CH))
    for p in range(out.shape[0]):
        out[p, :8, :] = state[8 * p : 8 * p + 8, :]
        out[p, 8:, :] = read_rows


def finish_kernel(r_ref, gain_ref, cache_ref, read_ref):
    for s in range(2):
        reads = []
        for h in range(2):
            j = 2 * s + h
            total = (r_ref[j] + r_ref[4 + j]) + (r_ref[8 + j] + r_ref[12 + j])
            cache_ref[s, h] = total[:8, :].astype(BF16)
            read = total[8:9, :]
            scale = lax.rsqrt(jnp.mean(read * read, axis=-1, keepdims=True) + 1e-06)
            reads.append(read * scale * gain_ref[...])
        read_ref[s] = jnp.concatenate(reads, axis=0).astype(BF16)


def vmem(count):
    return [pl.BlockSpec(memory_space=pltpu.VMEM) for _ in range(count)]


def spread(arrays, axis):
    out = [arrays[0]]
    for k in range(1, 4):
        out.append(lax.ppermute(arrays[k], axis, [(i, (i + k) % 4) for i in range(4)]))
    return out


def shards(
    tokens,
    key_matrix,
    value_matrix,
    gate_matrix,
    decay_matrix,
    gate_bias_offset,
    head_log_decay_rate,
    extra_log_decay,
    next_token_query,
    next_token_key,
    next_token_value,
    next_token_gate,
    readout_norm_gain,
):
    seqs, seg, width = tokens.shape
    cols = key_matrix.shape[1]
    tile = 256
    tiles = seqs * seg // tile
    count = seqs * seg // CH * 2
    smem = pl.BlockSpec(memory_space=pltpu.SMEM)
    hbm = pl.BlockSpec(memory_space=pl.ANY)
    maps = pl.pallas_call(
        maps_kernel,
        out_shape=[jax.ShapeDtypeStruct((2 * CH, CH), F32)] * 4,
        in_specs=[hbm, hbm, hbm, *vmem(2), smem, smem, *vmem(1)],
        out_specs=vmem(4),
        scratch_shapes=[
            pltpu.VMEM((tiles, tile, width), BF16),
            pltpu.VMEM((width, cols), BF16),
            pltpu.VMEM((width, cols), BF16),
            pltpu.VMEM((seqs * seg, cols), BF16),
            pltpu.VMEM((seqs * seg, cols), BF16),
            pltpu.VMEM((count, CH), F32),
            pltpu.VMEM((count, CH), F32),
            pltpu.VMEM((count, CH), F32),
            pltpu.VMEM((4, 2 * CH, CH), F32),
            pltpu.SemaphoreType.DMA((tiles + 2,)),
        ],
        compiler_params=pltpu.CompilerParams(vmem_limit_bytes=40 * 2**20),
        name="maps",
    )(
        tokens,
        key_matrix,
        value_matrix,
        gate_matrix.T,
        decay_matrix.T,
        gate_bias_offset,
        head_log_decay_rate,
        jnp.transpose(extra_log_decay, (0, 2, 1)),
    )
    pieces = pl.pallas_call(
        segments_kernel,
        out_shape=[jax.ShapeDtypeStruct((CH + 32, CH), F32)] * 4,
        in_specs=vmem(4),
        out_specs=vmem(4),
        scratch_shapes=[pltpu.VMEM((4, 2 * CH, CH), F32), pltpu.VMEM((CH, CH), F32)],
        name="segments",
    )(*spread(maps, "sp_1"))
    ranks = lax.axis_size(SP)
    rows = pl.pallas_call(
        columns_kernel,
        out_shape=jax.ShapeDtypeStruct((ranks, 16, CH), F32),
        in_specs=[*vmem(7), smem],
        out_specs=pl.BlockSpec(memory_space=pltpu.VMEM),
        scratch_shapes=[pltpu.VMEM((4, CH + 32, CH), F32), pltpu.VMEM((CH, CH), F32)],
        name="columns",
    )(*spread(pieces, "sp_0"), next_token_query, next_token_key, next_token_value, next_token_gate)
    got = lax.all_to_all(rows, SP, 0, 0, tiled=True)
    return pl.pallas_call(
        finish_kernel,
        out_shape=[
            jax.ShapeDtypeStruct((2, 2, 8, CH), BF16),
            jax.ShapeDtypeStruct((2, 2, CH), BF16),
        ],
        in_specs=vmem(2),
        out_specs=vmem(2),
        name="finish",
    )(got, readout_norm_gain.reshape(1, CH))


def solution(mesh):
    finer = Mesh(
        mesh.devices.reshape(mesh.shape["gr"], 4, 4, mesh.shape["tp"]), ("gr", "sp_0", "sp_1", "tp")
    )
    in_specs = (
        P("gr", SP, None),
        P(None, "tp"),
        P(None, "tp"),
        P(),
        P(),
        P(),
        P(),
        P("gr", SP, "tp"),
        P("gr", "tp", None),
        P("gr", "tp", None),
        P("gr", "tp", None),
        P("gr", "tp"),
        P(),
    )
    out_specs = (P("gr", "tp", SP, None), P("gr", "tp", None))
    return jax.shard_map(
        shards, mesh=finer, in_specs=in_specs, out_specs=out_specs, check_vma=False
    )
```

time: 189 us -> 88.1 us (0.47)
  matrix products: 67.7 us -> 0 us
  waiting for transfers between devices: 73.2 us -> 9.1 us
  Pallas kernels: 0 us -> 40.5 us
  between operations: 14.5 us -> 0.68 us
  starting transfers between devices: 4.81 us -> 12 us
  other arithmetic: 6.69 us -> 0 us
  blocking collectives: 12 us -> 15 us
    dot_general x46 -> x0, matrix products: 67.7 us -> none  [the longest x23 28.6 us: exact_matmul(): return jnp.matmul(left, right, precision=lax.Precision.HIGHEST)]
    all_gather x2 -> x0, waiting for transfers between devices: 63.2 us -> none  [entering(): pieces = lax.all_gather(so_far, axis)]
    pallas_call x0 -> x4, Pallas kernels: none -> 40.5 us  [the longest x1 33.9 us: shards(): pl.pallas_call(maps_kernel, out_shape=[jax.ShapeDtypeStruct((2 * CH, CH),...]
    ppermute x0 -> x6, starting transfers between devices: none -> 12 us  [spread(): lax.ppermute(arrays[k], axis, [(i, (i + k) % 4) for i in range(4)])]
    unnamed x24 -> x30, local copies, waits for them, and re-layouts: 0.07 us -> 10.3 us
    all_to_all x1 -> x0, waiting for transfers between devices: 9.99 us -> none  [summed_on_arrival(): pieces = lax.all_to_all(split_up(value, dim, count), axis, 0, 0, tiled=True)]
    ppermute x0 -> x6, waiting for transfers between devices: none -> 9.1 us  [spread(): lax.ppermute(arrays[k], axis, [(i, (i + k) % 4) for i in range(4)])]
    all_to_all x1 -> x0, starting transfers between devices: 4.73 us -> none  [summed_on_arrival(): pieces = lax.all_to_all(split_up(value, dim, count), axis, 0, 0, tiled=True)]
  transfers between devices with their start and end apart: 3 -> 6, of which waited for: 3 -> 5; matrix products, arithmetic and copies ran while one was open for 0% -> 0% of each run, Pallas kernels for 0% -> 0%
where the time goes in v1:
time: 88.1 us; the launch traced here: 87.6 us
  Pallas kernels  40.5 us (46%)
  blocking collectives  15 us (17%)
  starting transfers between devices  12 us (14%)
  local copies, waits for them, and re-layouts  10.3 us (12%)
  waiting for transfers between devices  9.1 us (10%)
    pallas_call x1, Pallas kernels, shards(): pl.pallas_call(maps_kernel, out_shape=[jax.ShapeDtypeStruct((2 * CH, CH),...  33.9 us
    all_to_all x1, blocking collectives, shards(): got = lax.all_to_all(rows, SP, 0, 0, tiled=True)  15 us
    ppermute x6, starting transfers between devices, spread(): lax.ppermute(arrays[k], axis, [(i, (i + k) % 4) for i in range(4)])  12 us
    unnamed x30, local copies, waits for them, and re-layouts  10.3 us
    ppermute x6, waiting for transfers between devices, spread(): lax.ppermute(arrays[k], axis, [(i, (i + k) % 4) for i in range(4)])  9.1 us
    pallas_call x1, Pallas kernels, shards(): pl.pallas_call(segments_kernel, out_shape=[jax.ShapeDtypeStruct((CH + 32,...  2.59 us
    pallas_call x1, Pallas kernels, shards(): pl.pallas_call(columns_kernel, out_shape=jax.ShapeDtypeStruct((ranks, 16,...  2.48 us
  transfers between devices with their start and end apart: 6, of which 5 were waited for; matrix products, arithmetic and copies ran while one was open for 0% of the time, Pallas kernels for 0%

profile of v1, /device:TPU:2, one launch (start us, length us, event | category | flops | bytes accessed | tf_op | source)
XLA Modules:
  0.0 87.6 jit_solution(6579583215949301567)
XLA Ops:
  0.6 2.2 %copy-done = bf16[2,512,2048]{2,1,0:T(8,128)(2,1)S(1)} copy-done((bf16[2,512,2048]{2,1,0:T(8,128)(2,1)S(1)}, bf16[2,512,2048]{2,1,0:T(8,128)(2,1)}, u32[]{:S(2)}) %copy-start) | copy-done | bytes 4194328
  2.8 1.2 %copy-done.1 = bf16[2048,256]{1,0:T(8,128)(2,1)S(1)} copy-done((bf16[2048,256]{1,0:T(8,128)(2,1)S(1)}, bf16[2048,256]{1,0:T(8,128)(2,1)}, u32[]{:S(2)}) %copy-start.1) | copy-done | bytes 1048600
  4.0 1.2 %copy-done.2 = bf16[2048,256]{1,0:T(8,128)(2,1)S(1)} copy-done((bf16[2048,256]{1,0:T(8,128)(2,1)S(1)}, bf16[2048,256]{1,0:T(8,128)(2,1)}, u32[]{:S(2)}) %copy-start.2) | copy-done | bytes 1048600
  5.3 0.8 copy-done.4
  6.1 0.8 copy-done.5
  7.0 0.7 copy-done.6
  7.7 0.7 copy-done.7
  8.3 0.7 copy-done.8
  9.0 33.9 %maps.1 = (f32[256,128]{1,0:T(8,128)S(1)}, f32[256,128]{1,0:T(8,128)S(1)}, f32[256,128]{1,0:T(8,128)S(1)}, f32[256,128]{1,0:T(8,128)S(1)}) custom-call(bf16[2,512,2048]{2,1,0:T(8,128)(2,1)S(1)} %copy-done, bf16[2048,256]{1,0:T(8,128)(2,1)S(1)} %copy-done.1, bf16[2048,256]{1,0:T(8,128)(2,1)S(1)} %copy-done.2, bf16[16,2048]{1,0:T(8,128)(2,1)S(1)} %bitcast.4, ...), custom_call_target="tpu_custom_call" | custom-call | tf_op jit(solution)/shard_map/maps/pallas_call | solution.py:297
  42.8 0.6 copy-done.3
  43.5 1.6 %collective-permute-start = (f32[256,128]{1,0:T(8,128)S(1)}, f32[256,128]{1,0:T(8,128)S(1)}, u32[]{:S(2)}, u32[]{:S(2)}) collective-permute-start(f32[256,128]{1,0:T(8,128)S(1)} %get-tuple-element.11), channel_id=1, source_target_pairs={{0,8},{8,16},{16,24},{24,0},{1,9},{9,17},{17,25},{25,1},{2,10},{10... | collective-permute-start | bytes 393224 | tf_op jit(solution)/shard_map/ppermute | solution.py:271
  45.1 2.9 %collective-permute-start.1 = (f32[256,128]{1,0:T(8,128)S(1)}, f32[256,128]{1,0:T(8,128)S(1)}, u32[]{:S(2)}, u32[]{:S(2)}) collective-permute-start(f32[256,128]{1,0:T(8,128)S(1)} %get-tuple-element.12), channel_id=1, source_target_pairs={{0,16},{8,24},{16,0},{24,8},{1,17},{9,25},{17,1},{25,9},{2,18},{10... | collective-permute-start | bytes 393224 | tf_op jit(solution)/shard_map/ppermute | solution.py:271
  48.0 1.3 %collective-permute-start.2 = (f32[256,128]{1,0:T(8,128)S(1)}, f32[256,128]{1,0:T(8,128)S(1)}, u32[]{:S(2)}, u32[]{:S(2)}) collective-permute-start(f32[256,128]{1,0:T(8,128)S(1)} %get-tuple-element.13), channel_id=1, source_target_pairs={{0,24},{8,0},{16,8},{24,16},{1,25},{9,1},{17,9},{25,17},{2,26},{10... | collective-permute-start | bytes 393224 | tf_op jit(solution)/shard_map/ppermute | solution.py:271
  49.3 0.7 collective-permute-done.r1
  50.0 4.0 %collective-permute-done.1.r2 = f32[256,128]{1,0:T(8,128)S(1)} collective-permute-done((f32[256,128]{1,0:T(8,128)S(1)}, f32[256,128]{1,0:T(8,128)S(1)}, u32[]{:S(2)}, u32[]{:S(2)}) %collective-permute-start.1) | collective-permute-done | bytes 131104 | tf_op jit(solution)/shard_map/ppermute | solution.py:271
  54.7 2.6 %segments.1 = (f32[160,128]{1,0:T(8,128)}, f32[160,128]{1,0:T(8,128)}, f32[160,128]{1,0:T(8,128)}, f32[160,128]{1,0:T(8,128)}) custom-call(f32[256,128]{1,0:T(8,128)} %copy-done.3, f32[256,128]{1,0:T(8,128)} %copy-done.9, f32[256,128]{1,0:T(8,128)} %copy-done.10, f32[256,128]{1,0:T(8,128)} %copy-done.11), custom_call_target="tpu_custom_call" | custom-call | tf_op jit(solution)/shard_map/segments/pallas_call | solution.py:326
  57.3 1.9 %collective-permute-start.3 = (f32[160,128]{1,0:T(8,128)}, f32[160,128]{1,0:T(8,128)S(1)}, u32[]{:S(2)}, u32[]{:S(2)}) collective-permute-start(f32[160,128]{1,0:T(8,128)} %get-tuple-element.15), channel_id=1, source_target_pairs={{0,32},{32,64},{64,96},{96,0},{1,33},{33,65},{65,97},{97,1},{2,34}... | collective-permute-start | bytes 245768 | tf_op jit(solution)/shard_map/ppermute | solution.py:271
  59.2 3.3 %collective-permute-start.4 = (f32[160,128]{1,0:T(8,128)}, f32[160,128]{1,0:T(8,128)S(1)}, u32[]{:S(2)}, u32[]{:S(2)}) collective-permute-start(f32[160,128]{1,0:T(8,128)} %get-tuple-element.16), channel_id=1, source_target_pairs={{0,64},{32,96},{64,0},{96,32},{1,65},{33,97},{65,1},{97,33},{2,66}... | collective-permute-start | bytes 245768 | tf_op jit(solution)/shard_map/ppermute | solution.py:271
  62.5 1.0 %collective-permute-start.5 = (f32[160,128]{1,0:T(8,128)}, f32[160,128]{1,0:T(8,128)S(1)}, u32[]{:S(2)}, u32[]{:S(2)}) collective-permute-start(f32[160,128]{1,0:T(8,128)} %get-tuple-element.17), channel_id=1, source_target_pairs={{0,96},{32,0},{64,32},{96,64},{1,97},{33,1},{65,33},{97,65},{2,98}... | collective-permute-start | bytes 245768 | tf_op jit(solution)/shard_map/ppermute | solution.py:271
  63.5 2.0 %collective-permute-done.3.r1 = f32[160,128]{1,0:T(8,128)S(1)} collective-permute-done((f32[160,128]{1,0:T(8,128)}, f32[160,128]{1,0:T(8,128)S(1)}, u32[]{:S(2)}, u32[]{:S(2)}) %collective-permute-start.3) | collective-permute-done | bytes 81952 | tf_op jit(solution)/shard_map/ppermute | solution.py:271
  65.5 2.0 %collective-permute-done.4.r2 = f32[160,128]{1,0:T(8,128)S(1)} collective-permute-done((f32[160,128]{1,0:T(8,128)}, f32[160,128]{1,0:T(8,128)S(1)}, u32[]{:S(2)}, u32[]{:S(2)}) %collective-permute-start.4) | collective-permute-done | bytes 81952 | tf_op jit(solution)/shard_map/ppermute | solution.py:271
  68.5 2.5 %columns.1 = f32[16,16,128]{2,1,0:T(8,128)} custom-call(f32[160,128]{1,0:T(8,128)} %get-tuple-element.14.r0, f32[160,128]{1,0:T(8,128)} %copy-done.12, f32[160,128]{1,0:T(8,128)} %copy-done.13, f32[160,128]{1,0:T(8,128)} %copy-done.14, bf16[2,2,128]{2,1,0:T(2,128)(2,1)} %query_ref.1, bf16[2,2,128]{2,1,0:T(2,128)(2,1)} %key_ref.1, ...), custom_call_target="tpu_custom_call" | custom-call | tf_op jit(solution)/shard_map/columns/pallas_call | solution.py:335
  71.0 15.0 %all_to_all.5.r_ref = f32[16,16,128]{2,1,0:T(8,128)} all-to-all(f32[16,16,128]{2,1,0:T(8,128)} %columns.1), channel_id=1, replica_groups=mesh['gr'=2,'sp_0'=4,'sp_1'=4,'tp'=8] {'sp_0','sp_1'}, dimensions={0} | all-to-all | bytes 262144 | tf_op jit(solution)/shard_map/all_to_all | solution.py:343
  86.0 1.6 %finish.1 = (bf16[2,2,8,128]{3,2,1,0:T(8,128)(2,1)}, bf16[2,2,128]{2,1,0:T(2,128)(2,1)}) custom-call(f32[16,16,128]{2,1,0:T(8,128)} %all_to_all.5.r_ref, f32[1,128]{1,0:T(1,128)} %bitcast.7), custom_call_target="tpu_custom_call" | custom-call | tf_op jit(solution)/shard_map/finish/pallas_call | solution.py:344
  (23 shorter events, 1.8 us)
Async XLA Ops:
  0.6 2.2 %copy-start = (bf16[2,512,2048]{2,1,0:T(8,128)(2,1)S(1)}, bf16[2,512,2048]{2,1,0:T(8,128)(2,1)}, u32[]{:S(2)}) copy-start(bf16[2,512,2048]{2,1,0:T(8,128)(2,1)} %x_hbm.1) | copy-start | bytes 12582916
  2.8 1.2 %copy-start.1 = (bf16[2048,256]{1,0:T(8,128)(2,1)S(1)}, bf16[2048,256]{1,0:T(8,128)(2,1)}, u32[]{:S(2)}) copy-start(bf16[2048,256]{1,0:T(8,128)(2,1)} %wk_hbm.1) | copy-start | bytes 3145732
  4.0 1.2 %copy-start.2 = (bf16[2048,256]{1,0:T(8,128)(2,1)S(1)}, bf16[2048,256]{1,0:T(8,128)(2,1)}, u32[]{:S(2)}) copy-start(bf16[2048,256]{1,0:T(8,128)(2,1)} %wv_hbm.1) | copy-start | bytes 3145732
  5.3 0.8 copy-start.4
  6.1 0.8 copy-start.5
  7.0 0.7 copy-start.6
  7.6 0.7 copy-start.7
  8.3 0.7 copy-start.8
  42.8 0.7 copy-start.3
  43.5 6.5 %collective-permute-start = (f32[256,128]{1,0:T(8,128)S(1)}, f32[256,128]{1,0:T(8,128)S(1)}, u32[]{:S(2)}, u32[]{:S(2)}) collective-permute-start(f32[256,128]{1,0:T(8,128)S(1)} %get-tuple-element.11), channel_id=1, source_target_pairs={{0,8},{8,16},{16,24},{24,0},{1,9},{9,17},{17,25},{25,1},{2,10},{10... | collective-permute-start | bytes 393224 | tf_op jit(solution)/shard_map/ppermute | solution.py:271
  45.1 8.9 %collective-permute-start.1 = (f32[256,128]{1,0:T(8,128)S(1)}, f32[256,128]{1,0:T(8,128)S(1)}, u32[]{:S(2)}, u32[]{:S(2)}) collective-permute-start(f32[256,128]{1,0:T(8,128)S(1)} %get-tuple-element.12), channel_id=1, source_target_pairs={{0,16},{8,24},{16,0},{24,8},{1,17},{9,25},{17,1},{25,9},{2,18},{10... | collective-permute-start | bytes 393224 | tf_op jit(solution)/shard_map/ppermute | solution.py:271
  48.0 6.0 %collective-permute-start.2 = (f32[256,128]{1,0:T(8,128)S(1)}, f32[256,128]{1,0:T(8,128)S(1)}, u32[]{:S(2)}, u32[]{:S(2)}) collective-permute-start(f32[256,128]{1,0:T(8,128)S(1)} %get-tuple-element.13), channel_id=1, source_target_pairs={{0,24},{8,0},{16,8},{24,16},{1,25},{9,1},{17,9},{25,17},{2,26},{10... | collective-permute-start | bytes 393224 | tf_op jit(solution)/shard_map/ppermute | solution.py:271
  50.0 4.0 %copy-start.9 = (f32[256,128]{1,0:T(8,128)}, f32[256,128]{1,0:T(8,128)S(1)}, u32[]{:S(2)}) copy-start(f32[256,128]{1,0:T(8,128)S(1)} %collective-permute-done.r1) | copy-start | bytes 393220
  54.0 0.6 copy-start.10
  54.0 0.7 copy-start.11
  57.3 8.2 %collective-permute-start.3 = (f32[160,128]{1,0:T(8,128)}, f32[160,128]{1,0:T(8,128)S(1)}, u32[]{:S(2)}, u32[]{:S(2)}) collective-permute-start(f32[160,128]{1,0:T(8,128)} %get-tuple-element.15), channel_id=1, source_target_pairs={{0,32},{32,64},{64,96},{96,0},{1,33},{33,65},{65,97},{97,1},{2,34}... | collective-permute-start | bytes 245768 | tf_op jit(solution)/shard_map/ppermute | solution.py:271
  59.2 8.3 %collective-permute-start.4 = (f32[160,128]{1,0:T(8,128)}, f32[160,128]{1,0:T(8,128)S(1)}, u32[]{:S(2)}, u32[]{:S(2)}) collective-permute-start(f32[160,128]{1,0:T(8,128)} %get-tuple-element.16), channel_id=1, source_target_pairs={{0,64},{32,96},{64,0},{96,32},{1,65},{33,97},{65,1},{97,33},{2,66}... | collective-permute-start | bytes 245768 | tf_op jit(solution)/shard_map/ppermute | solution.py:271
  62.5 5.4 %collective-permute-start.5 = (f32[160,128]{1,0:T(8,128)}, f32[160,128]{1,0:T(8,128)S(1)}, u32[]{:S(2)}, u32[]{:S(2)}) collective-permute-start(f32[160,128]{1,0:T(8,128)} %get-tuple-element.17), channel_id=1, source_target_pairs={{0,96},{32,0},{64,32},{96,64},{1,97},{33,1},{65,33},{97,65},{2,98}... | collective-permute-start | bytes 245768 | tf_op jit(solution)/shard_map/ppermute | solution.py:271
  65.5 2.5 %copy-start.12 = (f32[160,128]{1,0:T(8,128)}, f32[160,128]{1,0:T(8,128)S(1)}, u32[]{:S(2)}) copy-start(f32[160,128]{1,0:T(8,128)S(1)} %collective-permute-done.3.r1) | copy-start | bytes 245764
  67.5 0.6 copy-start.13
  67.9 0.6 copy-start.14

commit v2 on v1

v2 whole, which is shorter than its diff:
```python
import math

import jax
import jax.numpy as jnp
from jax import lax
from jax.experimental import pallas as pl
from jax.experimental.pallas import tpu as pltpu
from jax.sharding import Mesh
from jax.sharding import PartitionSpec as P

SP = ("sp_0", "sp_1")
CH = 128
F32 = jnp.float32
BF16 = jnp.bfloat16
AB = (((1,), (0,)), ((), ()))
ABT = (((1,), (1,)), ((), ()))
ATB = (((0,), (0,)), ((), ()))


def dot1(a, b, dims=AB):
    return lax.dot_general(a.astype(BF16), b.astype(BF16), dims, preferred_element_type=F32)


def split(a):
    hi = a.astype(BF16)
    return hi, (a - hi.astype(F32)).astype(BF16)


def dot3(a, b, dims=AB):
    ah, al = split(a)
    bh, bl = split(b)
    return dot1(ah, bh, dims) + (dot1(ah, bl, dims) + dot1(al, bh, dims))


def iota(shape, dim):
    return lax.broadcasted_iota(jnp.int32, shape, dim)


def unit_rows(a):
    return a * lax.rsqrt(jnp.sum(a * a, axis=-1, keepdims=True) + 1e-06)


def silu(a):
    return a * (1.0 / (1.0 + jnp.exp(-a)))


def inverses_of(m_mats):
    row = iota((CH, CH), 0)
    col = iota((CH, CH), 1)
    eye = jnp.where(row == col, 1.0, 0.0)
    near = row // 16 == col // 16
    p1s = [jnp.where(near, -m, 0.0) for m in m_mats]
    invs = [eye + p for p in p1s]
    pows = [p.astype(BF16) for p in p1s]
    pows = [dot1(p, p).astype(BF16) for p in pows]
    for last in (False, False, True):
        if last:
            adds = [dot1(p, i) for p, i in zip(pows, invs)]
        else:
            both = [dot1(p, jnp.concatenate([p, i.astype(BF16)], axis=1)) for p, i in zip(pows, invs)]
            adds = [x[:, CH:] for x in both]
            pows = [x[:, :CH].astype(BF16) for x in both]
        invs = [i + x for i, x in zip(invs, adds)]
    for b in (16, 32, 64):
        lower = [slice(s + b, s + 2 * b) for s in range(0, CH, 2 * b)]

        def gather(rows_of):
            return jnp.concatenate([rows_of(r) for r in lower], axis=0)

        m_rows = [
            gather(lambda r: jnp.where(col[r, :] // b == (r.start // b - 1), m[r, :], 0.0))
            for m in m_mats
        ]
        t_rows = [gather(lambda r: i[r, :]) for i in invs]
        ys = [dot1(m, i).astype(BF16) for m, i in zip(m_rows, invs)]
        spread_out = []
        for y in ys:
            pieces = []
            for g in range(len(lower)):
                pieces += [y[g * b : (g + 1) * b, :]] * 2
            spread_out.append(jnp.concatenate(pieces, axis=0))
        news = [t - dot1(t, y) for t, y in zip(t_rows, spread_out)]
        joined = []
        for i, new in zip(invs, news):
            pieces = []
            for g, r in enumerate(lower):
                pieces += [i[r.start - b : r.start, :], new[g * b : (g + 1) * b, :]]
            joined.append(jnp.concatenate(pieces, axis=0))
        invs = joined
    return invs


def maps_kernel(
    x_hbm, wk_hbm, wv_hbm, gate_hbm, decay_hbm, bias_hbm, rate_hbm, extra_hbm,
    o0, o1, o2, o3,
    xbuf, wkbuf, wvbuf, gatew, extra, bias_ref, rate_ref, kbuf, vbuf, rowbuf, state, sems,
):
    tiles, tile, width = xbuf.shape
    first_head = lax.axis_index("tp") * 2
    here = lax.axis_index("sp_1")
    per_tile = tile // CH
    per_seq = kbuf.shape[0] // (2 * CH)
    heads = gate_hbm.shape[0]

    def x_copy(t):
        half = tiles // 2
        rows = pl.ds(pl.multiple_of(lax.rem(t, half) * tile, tile), tile)
        return pltpu.make_async_copy(x_hbm.at[lax.div(t, half), rows], xbuf.at[t], sems.at[t])

    others = [
        pltpu.make_async_copy(src, dst, sems.at[tiles + i])
        for i, (src, dst) in enumerate(
            (
                (gate_hbm, gatew.at[pl.ds(0, heads)]),
                (decay_hbm, gatew.at[pl.ds(heads, heads)]),
                (wk_hbm, wkbuf),
                (wv_hbm, wvbuf),
                (bias_hbm, bias_ref),
                (rate_hbm, rate_ref),
                (extra_hbm, extra),
            )
        )
    ]
    for c in others[4:] + others[:3]:
        c.start()
    x_copy(0).start()
    others[3].start()
    for t in range(1, tiles):
        x_copy(t).start()
    for c in others[4:] + others[:3]:
        c.wait()
    pick = iota((heads, tile), 0)
    odd = iota((2, tile), 0) == 1
    bias = jnp.where(odd, bias_ref[first_head + 1], bias_ref[first_head])
    rate = jnp.exp(jnp.where(odd, rate_ref[first_head + 1], rate_ref[first_head]))
    row = iota((CH, CH), 0)
    col = iota((CH, CH), 1)
    eye = jnp.where(row == col, 1.0, 0.0)
    upto = jnp.where(row <= col, 1.0, 0.0).astype(BF16)

    def project(t, _):
        x_copy(t).wait()
        x = xbuf[t]
        gt = lax.dot_general(gatew[...], x, ABT, preferred_element_type=F32)
        picked = [
            jnp.sum(jnp.where(pick == first_head + h, part, 0.0), axis=0, keepdims=True)
            for part in (gt[:heads], gt[heads:])
            for h in range(2)
        ]
        beta = 1.0 / (1.0 + jnp.exp(-(jnp.concatenate(picked[:2], axis=0) + bias)))
        z = jnp.concatenate(picked[2:], axis=0)
        soft = jnp.maximum(z, 0.0) + jnp.log1p(jnp.exp(-jnp.abs(z)))
        for q in range(per_tile):
            m = t * per_tile + q
            lanes = slice(q * CH, (q + 1) * CH)
            step = extra[m] - rate[:, lanes] * soft[:, lanes]
            hi, rest = step.astype(BF16), step
            rest = rest - hi.astype(F32)
            mid = rest.astype(BF16)
            low = (rest - mid.astype(F32)).astype(BF16)
            cum = dot1(hi, upto) + (dot1(mid, upto) + dot1(low, upto))
            rowbuf[m, 0:2, :] = beta[:, lanes]
            rowbuf[m, 2:4, :] = cum

        @pl.when(t == 0)
        def _():
            others[3].wait()

        rows = pl.ds(pl.multiple_of(t * tile, tile), tile)
        kp = silu(lax.dot_general(x, wkbuf[...], AB, preferred_element_type=F32))
        for h in range(2):
            lanes = slice(h * CH, (h + 1) * CH)
            kbuf[rows, lanes] = unit_rows(kp[:, lanes]).astype(BF16)
        vp = silu(lax.dot_general(x, wvbuf[...], AB, preferred_element_type=F32))
        vbuf[rows, :] = vp.astype(BF16)
        return 0

    lax.fori_loop(0, tiles, project, 0)

    start = jnp.concatenate([eye, jnp.zeros((CH, CH), F32)], axis=1)
    for p in range(4):
        state[p] = start

    def advance(n, _):
        blocks = [rowbuf[n], rowbuf[per_seq + n]]
        beta = jnp.concatenate([b[0:2] for b in blocks], axis=0)
        cum = jnp.concatenate([b[2:4] for b in blocks], axis=0)
        total = jnp.broadcast_to(cum[:, CH - 1 : CH], (4, CH))
        carry = jnp.exp(total)
        reach = jnp.exp(total - cum)
        ecum = jnp.exp(cum)
        columns = jnp.transpose(
            jnp.concatenate([beta, cum, reach, jnp.zeros((CH - 12, CH), F32)], axis=0)
        )
        ks, vs, ms = [], [], []
        for p in range(4):
            s, h = divmod(p, 2)
            rows = pl.ds(pl.multiple_of((s * per_seq + n) * CH, CH), CH)
            lanes = slice(h * CH, (h + 1) * CH)
            ks.append(kbuf[rows, lanes])
            vs.append(vbuf[rows, lanes])
        grams = [lax.dot_general(k, k, ABT, preferred_element_type=F32) for k in ks]
        for p in range(4):
            gap = jnp.minimum(columns[:, 4 + p : 5 + p] - cum[p : p + 1, :], 0.0)
            ms.append(jnp.where(row > col, columns[:, p : p + 1] * grams[p] * jnp.exp(gap), 0.0))
        invs = inverses_of(ms)
        us = [columns[:, 8 + p : 9 + p] * invs[p] * beta[p : p + 1, :] for p in range(4)]
        pulls = [dot1(us[p] * ecum[p : p + 1, :], ks[p]).astype(BF16) for p in range(4)]
        freshs = [dot1(us[p], vs[p]).astype(BF16) for p in range(4)]
        boths = [
            dot1(k, jnp.concatenate([pull, fresh], axis=1), ATB)
            for k, pull, fresh in zip(ks, pulls, freshs)
        ]
        for p in range(4):
            before = state[p]
            moved = dot1(boths[p][:, :CH], before)
            c_row = carry[p : p + 1, :]
            state[p, :, :CH] = c_row * before[:, :CH] - moved[:, :CH]
            state[p, :, CH:] = c_row * before[:, CH:] - moved[:, CH:] + boths[p][:, CH:]
        return 0

    lax.fori_loop(0, per_seq, advance, 0)
    for k, o in enumerate((o0, o1, o2, o3)):
        p = lax.rem(here + k, 4)
        o[:CH, :] = state[p, :, :CH]
        o[CH:, :] = state[p, :, CH:]


def ordered(refs, scr, here):
    for k, ref in enumerate(refs):
        scr[lax.rem(here + 4 - k, 4)] = ref[...]


def segments_kernel(r0, r1, r2, r3, o0, o1, o2, o3, scr, bscr):
    ordered((r0, r1, r2, r3), scr, lax.axis_index("sp_1"))
    there = lax.axis_index("sp_0")
    state = jnp.concatenate([scr[0, :CH, :], scr[0, CH:, :]], axis=1)
    for t in range(1, 4):
        state = dot3(scr[t, :CH, :], state)
        state = state + jnp.concatenate([jnp.zeros((CH, CH), F32), scr[t, CH:, :]], axis=1)
    bscr[...] = jnp.transpose(state[:, CH:])
    for k, o in enumerate((o0, o1, o2, o3)):
        q = lax.rem(there + k, 4)
        o[:CH, :] = state[:, :CH]
        o[CH:, :] = bscr[pl.ds(pl.multiple_of(q * 32, 32), 32), :]


def row_of(ref, s, h):
    two = ref[s].astype(F32)
    return jnp.sum(jnp.where(iota(two.shape, 0) == h, two, 0.0), axis=0, keepdims=True)


def columns_kernel(r0, r1, r2, r3, query_ref, key_ref, value_ref, gate_ref, out, scr, wide):
    part = lax.axis_index("sp_0")
    pair = lax.axis_index("sp_1")
    ordered((r0, r1, r2, r3), scr, part)
    f = scr[0, CH:, :]
    for g in range(1, 4):
        f = dot3(f, scr[g, :CH, :], ABT) + scr[g, CH:, :]
    s = pair // 2
    h = lax.rem(pair, 2)
    qn = unit_rows(row_of(query_ref, s, h))
    kn = unit_rows(row_of(key_ref, s, h))
    vn = row_of(value_ref, s, h)
    bn = 1.0 / (1.0 + jnp.exp(-jnp.full((1, CH), gate_ref[s, h], F32)))
    count = f.shape[0]
    mine = iota((count, CH), 1) == iota((count, CH), 0) + part * count
    vn_col = jnp.sum(jnp.where(mine, jnp.broadcast_to(vn, (count, CH)), 0.0), axis=1, keepdims=True)
    missing = vn_col - jnp.sum(f * kn, axis=1, keepdims=True)
    query_read = jnp.sum(f * qn, axis=1, keepdims=True)
    meet = jnp.sum(kn * qn, axis=1, keepdims=True)
    read = (query_read + (bn[:, :1] * meet) * missing) / math.sqrt(CH)
    wide[...] = jnp.zeros_like(wide)
    wide[pl.ds(pl.multiple_of(part * count, 32), count), :] = f + missing * (bn * kn)
    state = jnp.transpose(wide[...])
    read_row = jnp.sum(jnp.where(mine, jnp.broadcast_to(read, (count, CH)), 0.0), axis=0, keepdims=True)
    read_rows = jnp.broadcast_to(read_row, (8, CH))
    for p in range(out.shape[0]):
        out[p, :8, :] = state[8 * p : 8 * p + 8, :]
        out[p, 8:, :] = read_rows


def finish_kernel(r_ref, gain_ref, cache_ref, read_ref):
    for s in range(2):
        reads = []
        for h in range(2):
            j = 2 * s + h
            total = (r_ref[j] + r_ref[4 + j]) + (r_ref[8 + j] + r_ref[12 + j])
            cache_ref[s, h] = total[:8, :].astype(BF16)
            read = total[8:9, :]
            scale = lax.rsqrt(jnp.mean(read * read, axis=-1, keepdims=True) + 1e-06)
            reads.append(read * scale * gain_ref[...])
        read_ref[s] = jnp.concatenate(reads, axis=0).astype(BF16)


def vmem(count):
    return [pl.BlockSpec(memory_space=pltpu.VMEM) for _ in range(count)]


def spread(arrays, axis):
    out = [arrays[0]]
    for k in range(1, 4):
        out.append(lax.ppermute(arrays[k], axis, [(i, (i + k) % 4) for i in range(4)]))
    return out


def shards(
    tokens,
    key_matrix,
    value_matrix,
    gate_matrix,
    decay_matrix,
    gate_bias_offset,
    head_log_decay_rate,
    extra_log_decay,
    next_token_query,
    next_token_key,
    next_token_value,
    next_token_gate,
    readout_norm_gain,
):
    seqs, seg, width = tokens.shape
    cols = key_matrix.shape[1]
    tile = 256
    tiles = seqs * seg // tile
    chunks = seqs * seg // CH
    extra = jnp.transpose(extra_log_decay.reshape(chunks, CH, 2), (0, 2, 1))
    hbm = pl.BlockSpec(memory_space=pltpu.HBM)
    smem = pl.BlockSpec(memory_space=pltpu.SMEM)
    maps = pl.pallas_call(
        maps_kernel,
        out_shape=[jax.ShapeDtypeStruct((2 * CH, CH), F32)] * 4,
        in_specs=[hbm] * 8,
        out_specs=vmem(4),
        scratch_shapes=[
            pltpu.VMEM((tiles, tile, width), BF16),
            pltpu.VMEM((width, cols), BF16),
            pltpu.VMEM((width, cols), BF16),
            pltpu.VMEM((2 * gate_matrix.shape[1], width), BF16),
            pltpu.VMEM((chunks, 2, CH), F32),
            pltpu.SMEM(gate_bias_offset.shape, F32),
            pltpu.SMEM(head_log_decay_rate.shape, F32),
            pltpu.VMEM((seqs * seg, cols), BF16),
            pltpu.VMEM((seqs * seg, cols), BF16),
            pltpu.VMEM((chunks, 8, CH), F32),
            pltpu.VMEM((4, CH, 2 * CH), F32),
            pltpu.SemaphoreType.DMA((tiles + 7,)),
        ],
        compiler_params=pltpu.CompilerParams(vmem_limit_bytes=24 * 2**20),
        name="maps",
    )(
        *(
            pltpu.with_memory_space_constraint(a, pltpu.HBM)
            for a in (
                tokens,
                key_matrix,
                value_matrix,
                gate_matrix.T,
                decay_matrix.T,
                gate_bias_offset,
                head_log_decay_rate,
                extra,
            )
        )
    )
    small = pltpu.CompilerParams(vmem_limit_bytes=8 * 2**20)
    pieces = pl.pallas_call(
        segments_kernel,
        out_shape=[jax.ShapeDtypeStruct((CH + 32, CH), F32)] * 4,
        in_specs=vmem(4),
        out_specs=vmem(4),
        scratch_shapes=[pltpu.VMEM((4, 2 * CH, CH), F32), pltpu.VMEM((CH, CH), F32)],
        compiler_params=small,
        name="segments",
    )(*spread(maps, "sp_1"))
    ranks = lax.axis_size(SP)
    rows = pl.pallas_call(
        columns_kernel,
        out_shape=jax.ShapeDtypeStruct((ranks, 16, CH), F32),
        in_specs=[*vmem(7), smem],
        out_specs=pl.BlockSpec(memory_space=pltpu.VMEM),
        scratch_shapes=[pltpu.VMEM((4, CH + 32, CH), F32), pltpu.VMEM((CH, CH), F32)],
        compiler_params=small,
        name="columns",
    )(*spread(pieces, "sp_0"), next_token_query, next_token_key, next_token_value, next_token_gate)
    got = lax.all_to_all(rows, SP, 0, 0, tiled=True)
    return pl.pallas_call(
        finish_kernel,
        out_shape=[
            jax.ShapeDtypeStruct((2, 2, 8, CH), BF16),
            jax.ShapeDtypeStruct((2, 2, CH), BF16),
        ],
        in_specs=vmem(2),
        out_specs=vmem(2),
        compiler_params=small,
        name="finish",
    )(got, readout_norm_gain.reshape(1, CH))


def solution(mesh):
    finer = Mesh(
        mesh.devices.reshape(mesh.shape["gr"], 4, 4, mesh.shape["tp"]), ("gr", "sp_0", "sp_1", "tp")
    )
    in_specs = (
        P("gr", SP, None),
        P(None, "tp"),
        P(None, "tp"),
        P(),
        P(),
        P(),
        P(),
        P("gr", SP, "tp"),
        P("gr", "tp", None),
        P("gr", "tp", None),
        P("gr", "tp", None),
        P("gr", "tp"),
        P(),
    )
    out_specs = (P("gr", "tp", SP, None), P("gr", "tp", None))
    return jax.shard_map(
        shards, mesh=finer, in_specs=in_specs, out_specs=out_specs, check_vma=False
    )
```

time: 88.1 us -> 57.3 us (0.65)
  Pallas kernels: 40.5 us -> 20.4 us
  local copies, waits for them, and re-layouts: 10.3 us -> 0.02 us
    pallas_call x1, Pallas kernels: 33.9 us -> 17.6 us  [shards(): pl.pallas_call(maps_kernel, out_shape=[jax.ShapeDtypeStruct((2 * CH, CH),...]
    unnamed x30 -> x10, local copies, waits for them, and re-layouts: 10.3 us -> 0.02 us
    pallas_call x1, Pallas kernels: 2.59 us -> 0.76 us  [shards(): pl.pallas_call(segments_kernel, out_shape=[jax.ShapeDtypeStruct((CH + 32,...]
    pallas_call x1, Pallas kernels: 2.48 us -> 1.33 us  [shards(): pl.pallas_call(columns_kernel, out_shape=jax.ShapeDtypeStruct((ranks, 16,...]
    pallas_call x1, Pallas kernels: 1.56 us -> 0.66 us  [shards(): pl.pallas_call(finish_kernel, out_shape=[jax.ShapeDtypeStruct((2, 2, 8, C...]
where the time goes in v2:
time: 57.3 us; the launch traced here: 57.1 us
  Pallas kernels  20.4 us (36%)
  blocking collectives  15 us (26%)
  starting transfers between devices  12.2 us (21%)
  waiting for transfers between devices  8.91 us (16%)
  between operations  0.72 us (1%)
    pallas_call x1, Pallas kernels, shards(): pl.pallas_call(maps_kernel, out_shape=[jax.ShapeDtypeStruct((2 * CH, CH),...  17.6 us
    all_to_all x1, blocking collectives, shards(): got = lax.all_to_all(rows, SP, 0, 0, tiled=True)  15 us
    ppermute x6, starting transfers between devices, spread(): lax.ppermute(arrays[k], axis, [(i, (i + k) % 4) for i in range(4)])  12.2 us
    ppermute x6, waiting for transfers between devices, spread(): lax.ppermute(arrays[k], axis, [(i, (i + k) % 4) for i in range(4)])  8.91 us
    pallas_call x1, Pallas kernels, shards(): pl.pallas_call(columns_kernel, out_shape=jax.ShapeDtypeStruct((ranks, 16,...  1.33 us
  transfers between devices with their start and end apart: 6, of which 5 were waited for; matrix products, arithmetic and copies ran while one was open for 0% of the time, Pallas kernels for 0%

profile of v2, /device:TPU:2, one launch (start us, length us, event | category | flops | bytes accessed | tf_op | source)
XLA Modules:
  0.0 57.1 jit_solution(8144673155676554335)
XLA Ops:
  0.6 0.0 copy-start.3
  0.6 0.0 copy-start.2
  0.7 0.0 copy-start.1
  0.7 0.0 copy-start
  0.7 0.0 copy-start.4
  0.7 17.6 %maps.1 = (f32[256,128]{1,0:T(8,128)S(1)}, f32[256,128]{1,0:T(8,128)S(1)}, f32[256,128]{1,0:T(8,128)S(1)}, f32[256,128]{1,0:T(8,128)S(1)}) custom-call(bf16[2,512,2048]{2,1,0:T(8,128)(2,1)} %x_hbm.1, bf16[2048,256]{1,0:T(8,128)(2,1)} %wk_hbm.1, bf16[2048,256]{1,0:T(8,128)(2,1)} %wv_hbm.1, bf16[16,2048]{1,0:T(8,128)(2,1)} %bitcast.7, ...), custom_call_target="tpu_custom_call" | custom-call | tf_op jit(solution)/shard_map/maps/pallas_call | solution.py:330
  18.3 1.6 %collective-permute-start = (f32[256,128]{1,0:T(8,128)S(1)}, f32[256,128]{1,0:T(8,128)S(1)}, u32[]{:S(2)}, u32[]{:S(2)}) collective-permute-start(f32[256,128]{1,0:T(8,128)S(1)} %get-tuple-element.11), channel_id=1, source_target_pairs={{0,8},{8,16},{16,24},{24,0},{1,9},{9,17},{17,25},{25,1},{2,10},{10... | collective-permute-start | bytes 393224 | tf_op jit(solution)/shard_map/ppermute | solution.py:303
  20.0 2.9 %collective-permute-start.1 = (f32[256,128]{1,0:T(8,128)S(1)}, f32[256,128]{1,0:T(8,128)S(1)}, u32[]{:S(2)}, u32[]{:S(2)}) collective-permute-start(f32[256,128]{1,0:T(8,128)S(1)} %get-tuple-element.12), channel_id=1, source_target_pairs={{0,16},{8,24},{16,0},{24,8},{1,17},{9,25},{17,1},{25,9},{2,18},{10... | collective-permute-start | bytes 393224 | tf_op jit(solution)/shard_map/ppermute | solution.py:303
  22.9 1.3 %collective-permute-start.2 = (f32[256,128]{1,0:T(8,128)S(1)}, f32[256,128]{1,0:T(8,128)S(1)}, u32[]{:S(2)}, u32[]{:S(2)}) collective-permute-start(f32[256,128]{1,0:T(8,128)S(1)} %get-tuple-element.13), channel_id=1, source_target_pairs={{0,24},{8,0},{16,8},{24,16},{1,25},{9,1},{17,9},{25,17},{2,26},{10... | collective-permute-start | bytes 393224 | tf_op jit(solution)/shard_map/ppermute | solution.py:303
  24.2 0.7 %collective-permute-done.r1 = f32[256,128]{1,0:T(8,128)S(1)} collective-permute-done((f32[256,128]{1,0:T(8,128)S(1)}, f32[256,128]{1,0:T(8,128)S(1)}, u32[]{:S(2)}, u32[]{:S(2)}) %collective-permute-start) | collective-permute-done | bytes 131104 | tf_op jit(solution)/shard_map/ppermute | solution.py:303
  24.9 4.0 %collective-permute-done.1.r2 = f32[256,128]{1,0:T(8,128)S(1)} collective-permute-done((f32[256,128]{1,0:T(8,128)S(1)}, f32[256,128]{1,0:T(8,128)S(1)}, u32[]{:S(2)}, u32[]{:S(2)}) %collective-permute-start.1) | collective-permute-done | bytes 131104 | tf_op jit(solution)/shard_map/ppermute | solution.py:303
  28.9 0.0 collective-permute-done.2.r3
  28.9 0.8 %segments.1 = (f32[160,128]{1,0:T(8,128)S(1)}, f32[160,128]{1,0:T(8,128)S(1)}, f32[160,128]{1,0:T(8,128)S(1)}, f32[160,128]{1,0:T(8,128)S(1)}) custom-call(f32[256,128]{1,0:T(8,128)S(1)} %get-tuple-element.10.r0, f32[256,128]{1,0:T(8,128)S(1)} %collective-permute-done.r1, f32[256,128]{1,0:T(8,128)S(1)} %collective-permute-done.1.r2, ...), custom_call_target="tpu_custom_call" | custom-call | tf_op jit(solution)/shard_map/segments/pallas_call | solution.py:367
  29.6 2.0 %collective-permute-start.3 = (f32[160,128]{1,0:T(8,128)S(1)}, f32[160,128]{1,0:T(8,128)S(1)}, u32[]{:S(2)}, u32[]{:S(2)}) collective-permute-start(f32[160,128]{1,0:T(8,128)S(1)} %get-tuple-element.15), channel_id=1, source_target_pairs={{0,32},{32,64},{64,96},{96,0},{1,33},{33,65},{65,97},{97,1},{2,34}... | collective-permute-start | bytes 245768 | tf_op jit(solution)/shard_map/ppermute | solution.py:303
  31.6 3.3 %collective-permute-start.4 = (f32[160,128]{1,0:T(8,128)S(1)}, f32[160,128]{1,0:T(8,128)S(1)}, u32[]{:S(2)}, u32[]{:S(2)}) collective-permute-start(f32[160,128]{1,0:T(8,128)S(1)} %get-tuple-element.16), channel_id=1, source_target_pairs={{0,64},{32,96},{64,0},{96,32},{1,65},{33,97},{65,1},{97,33},{2,66}... | collective-permute-start | bytes 245768 | tf_op jit(solution)/shard_map/ppermute | solution.py:303
  34.9 1.0 %collective-permute-start.5 = (f32[160,128]{1,0:T(8,128)S(1)}, f32[160,128]{1,0:T(8,128)S(1)}, u32[]{:S(2)}, u32[]{:S(2)}) collective-permute-start(f32[160,128]{1,0:T(8,128)S(1)} %get-tuple-element.17), channel_id=1, source_target_pairs={{0,96},{32,0},{64,32},{96,64},{1,97},{33,1},{65,33},{97,65},{2,98}... | collective-permute-start | bytes 245768 | tf_op jit(solution)/shard_map/ppermute | solution.py:303
  35.9 1.8 %collective-permute-done.3.r1 = f32[160,128]{1,0:T(8,128)S(1)} collective-permute-done((f32[160,128]{1,0:T(8,128)S(1)}, f32[160,128]{1,0:T(8,128)S(1)}, u32[]{:S(2)}, u32[]{:S(2)}) %collective-permute-start.3) | collective-permute-done | bytes 81952 | tf_op jit(solution)/shard_map/ppermute | solution.py:303
  37.7 2.0 %collective-permute-done.4.r2 = f32[160,128]{1,0:T(8,128)S(1)} collective-permute-done((f32[160,128]{1,0:T(8,128)S(1)}, f32[160,128]{1,0:T(8,128)S(1)}, u32[]{:S(2)}, u32[]{:S(2)}) %collective-permute-start.4) | collective-permute-done | bytes 81952 | tf_op jit(solution)/shard_map/ppermute | solution.py:303
  39.7 0.4 collective-permute-done.5.r3
  40.2 0.0 copy-done.1
  40.2 1.3 %columns.1 = f32[16,16,128]{2,1,0:T(8,128)S(1)} custom-call(f32[160,128]{1,0:T(8,128)S(1)} %get-tuple-element.14.r0, f32[160,128]{1,0:T(8,128)S(1)} %collective-permute-done.3.r1, f32[160,128]{1,0:T(8,128)S(1)} %collective-permute-done.4.r2, f32[160,128]{1,0:T(8,128)S(1)} %collective-permute-done.5.r3, bf16[2,2,128]{2,1,0:T(2,128)(2,1)S(1)} %copy-done, ...), custom_call_target="tpu_custom_call" | custom-call | tf_op jit(solution)/shard_map/columns/pallas_call | solution.py:377
  41.5 15.0 %all_to_all.5.r_ref = f32[16,16,128]{2,1,0:T(8,128)S(1)} all-to-all(f32[16,16,128]{2,1,0:T(8,128)S(1)} %columns.1), channel_id=1, replica_groups=mesh['gr'=2,'sp_0'=4,'sp_1'=4,'tp'=8] {'sp_0','sp_1'}, dimensions={0} | all-to-all | bytes 262144 | tf_op jit(solution)/shard_map/all_to_all | solution.py:386
  56.5 0.0 copy-done.4
  56.5 0.7 %finish.1 = (bf16[2,2,8,128]{3,2,1,0:T(8,128)(2,1)}, bf16[2,2,128]{2,1,0:T(2,128)(2,1)}) custom-call(f32[16,16,128]{2,1,0:T(8,128)S(1)} %all_to_all.5.r_ref, f32[1,128]{1,0:T(1,128)S(1)} %bitcast.6), custom_call_target="tpu_custom_call" | custom-call | tf_op jit(solution)/shard_map/finish/pallas_call | solution.py:387
  (3 shorter events, 0.0 us)
Async XLA Ops:
  0.6 39.5 %copy-start.3 = (f32[2,2]{1,0:T(2,128)S(1)}, f32[2,2]{1,0:T(2,128)}, u32[]{:S(2)}) copy-start(f32[2,2]{1,0:T(2,128)} %gate_ref.1) | copy-start | bytes 52
  0.6 39.5 %copy-start.2 = (bf16[2,2,128]{2,1,0:T(2,128)(2,1)S(1)}, bf16[2,2,128]{2,1,0:T(2,128)(2,1)}, u32[]{:S(2)}) copy-start(bf16[2,2,128]{2,1,0:T(2,128)(2,1)} %value_ref.1) | copy-start | bytes 3076
  0.7 39.5 %copy-start.1 = (bf16[2,2,128]{2,1,0:T(2,128)(2,1)S(1)}, bf16[2,2,128]{2,1,0:T(2,128)(2,1)}, u32[]{:S(2)}) copy-start(bf16[2,2,128]{2,1,0:T(2,128)(2,1)} %key_ref.1) | copy-start | bytes 3076
  0.7 39.5 %copy-start = (bf16[2,2,128]{2,1,0:T(2,128)(2,1)S(1)}, bf16[2,2,128]{2,1,0:T(2,128)(2,1)}, u32[]{:S(2)}) copy-start(bf16[2,2,128]{2,1,0:T(2,128)(2,1)} %query_ref.1) | copy-start | bytes 3076
  0.7 55.8 %copy-start.4 = (f32[128]{0:T(128)S(1)}, f32[128]{0:T(128)}, u32[]{:S(2)}) copy-start(f32[128]{0:T(128)} %param.25) | copy-start | bytes 1540
  18.3 6.6 %collective-permute-start = (f32[256,128]{1,0:T(8,128)S(1)}, f32[256,128]{1,0:T(8,128)S(1)}, u32[]{:S(2)}, u32[]{:S(2)}) collective-permute-start(f32[256,128]{1,0:T(8,128)S(1)} %get-tuple-element.11), channel_id=1, source_target_pairs={{0,8},{8,16},{16,24},{24,0},{1,9},{9,17},{17,25},{25,1},{2,10},{10... | collective-permute-start | bytes 393224 | tf_op jit(solution)/shard_map/ppermute | solution.py:303
  20.0 8.9 %collective-permute-start.1 = (f32[256,128]{1,0:T(8,128)S(1)}, f32[256,128]{1,0:T(8,128)S(1)}, u32[]{:S(2)}, u32[]{:S(2)}) collective-permute-start(f32[256,128]{1,0:T(8,128)S(1)} %get-tuple-element.12), channel_id=1, source_target_pairs={{0,16},{8,24},{16,0},{24,8},{1,17},{9,25},{17,1},{25,9},{2,18},{10... | collective-permute-start | bytes 393224 | tf_op jit(solution)/shard_map/ppermute | solution.py:303
  22.9 6.0 %collective-permute-start.2 = (f32[256,128]{1,0:T(8,128)S(1)}, f32[256,128]{1,0:T(8,128)S(1)}, u32[]{:S(2)}, u32[]{:S(2)}) collective-permute-start(f32[256,128]{1,0:T(8,128)S(1)} %get-tuple-element.13), channel_id=1, source_target_pairs={{0,24},{8,0},{16,8},{24,16},{1,25},{9,1},{17,9},{25,17},{2,26},{10... | collective-permute-start | bytes 393224 | tf_op jit(solution)/shard_map/ppermute | solution.py:303
  29.6 8.1 %collective-permute-start.3 = (f32[160,128]{1,0:T(8,128)S(1)}, f32[160,128]{1,0:T(8,128)S(1)}, u32[]{:S(2)}, u32[]{:S(2)}) collective-permute-start(f32[160,128]{1,0:T(8,128)S(1)} %get-tuple-element.15), channel_id=1, source_target_pairs={{0,32},{32,64},{64,96},{96,0},{1,33},{33,65},{65,97},{97,1},{2,34}... | collective-permute-start | bytes 245768 | tf_op jit(solution)/shard_map/ppermute | solution.py:303
  31.6 8.1 %collective-permute-start.4 = (f32[160,128]{1,0:T(8,128)S(1)}, f32[160,128]{1,0:T(8,128)S(1)}, u32[]{:S(2)}, u32[]{:S(2)}) collective-permute-start(f32[160,128]{1,0:T(8,128)S(1)} %get-tuple-element.16), channel_id=1, source_target_pairs={{0,64},{32,96},{64,0},{96,32},{1,65},{33,97},{65,1},{97,33},{2,66}... | collective-permute-start | bytes 245768 | tf_op jit(solution)/shard_map/ppermute | solution.py:303
  34.9 5.2 %collective-permute-start.5 = (f32[160,128]{1,0:T(8,128)S(1)}, f32[160,128]{1,0:T(8,128)S(1)}, u32[]{:S(2)}, u32[]{:S(2)}) collective-permute-start(f32[160,128]{1,0:T(8,128)S(1)} %get-tuple-element.17), channel_id=1, source_target_pairs={{0,96},{32,0},{64,32},{96,64},{1,97},{33,1},{65,33},{97,65},{2,98}... | collective-permute-start | bytes 245768 | tf_op jit(solution)/shard_map/ppermute | solution.py:303

commit v3 on v2

--- a/solution.py
+++ b/solution.py
@@ -77,7 +77,7 @@
         for y in ys:
             pieces = []
             for g in range(len(lower)):
-                pieces += [y[g * b : (g + 1) * b, :]] * 2
+                pieces += [jnp.zeros((b, CH), BF16), y[g * b : (g + 1) * b, :]]
             spread_out.append(jnp.concatenate(pieces, axis=0))
         news = [t - dot1(t, y) for t, y in zip(t_rows, spread_out)]
         joined = []
@@ -93,19 +93,18 @@
 def maps_kernel(
     x_hbm, wk_hbm, wv_hbm, gate_hbm, decay_hbm, bias_hbm, rate_hbm, extra_hbm,
     o0, o1, o2, o3,
-    xbuf, wkbuf, wvbuf, gatew, extra, bias_ref, rate_ref, kbuf, vbuf, rowbuf, state, sems,
+    xbuf, wkbuf, wvbuf, gatew, extra, bias_ref, rate_ref, kbuf, vbuf, state, sems,
 ):
     tiles, tile, width = xbuf.shape
     first_head = lax.axis_index("tp") * 2
     here = lax.axis_index("sp_1")
-    per_tile = tile // CH
     per_seq = kbuf.shape[0] // (2 * CH)
     heads = gate_hbm.shape[0]
 
     def x_copy(t):
-        half = tiles // 2
-        rows = pl.ds(pl.multiple_of(lax.rem(t, half) * tile, tile), tile)
-        return pltpu.make_async_copy(x_hbm.at[lax.div(t, half), rows], xbuf.at[t], sems.at[t])
+        s, part = divmod(t, tiles // 2)
+        rows = pl.ds(part * tile, tile)
+        return pltpu.make_async_copy(x_hbm.at[s, rows], xbuf.at[t], sems.at[t])
 
     others = [
         pltpu.make_async_copy(src, dst, sems.at[tiles + i])
@@ -138,88 +137,113 @@
     eye = jnp.where(row == col, 1.0, 0.0)
     upto = jnp.where(row <= col, 1.0, 0.0).astype(BF16)
 
-    def project(t, _):
-        x_copy(t).wait()
-        x = xbuf[t]
-        gt = lax.dot_general(gatew[...], x, ABT, preferred_element_type=F32)
+    def halves(t, weights, dims, count):
+        size = tile // count
+        return [
+            lax.dot_general(
+                xbuf[t, i * size : (i + 1) * size], weights[...], dims, preferred_element_type=F32
+            )
+            for i in range(count)
+        ]
+
+    def scalars(t, gt):
         picked = [
             jnp.sum(jnp.where(pick == first_head + h, part, 0.0), axis=0, keepdims=True)
             for part in (gt[:heads], gt[heads:])
             for h in range(2)
         ]
-        beta = 1.0 / (1.0 + jnp.exp(-(jnp.concatenate(picked[:2], axis=0) + bias)))
         z = jnp.concatenate(picked[2:], axis=0)
         soft = jnp.maximum(z, 0.0) + jnp.log1p(jnp.exp(-jnp.abs(z)))
-        for q in range(per_tile):
-            m = t * per_tile + q
-            lanes = slice(q * CH, (q + 1) * CH)
-            step = extra[m] - rate[:, lanes] * soft[:, lanes]
-            hi, rest = step.astype(BF16), step
-            rest = rest - hi.astype(F32)
-            mid = rest.astype(BF16)
-            low = (rest - mid.astype(F32)).astype(BF16)
-            cum = dot1(hi, upto) + (dot1(mid, upto) + dot1(low, upto))
-            rowbuf[m, 0:2, :] = beta[:, lanes]
-            rowbuf[m, 2:4, :] = cum
-
-        @pl.when(t == 0)
-        def _():
-            others[3].wait()
-
-        rows = pl.ds(pl.multiple_of(t * tile, tile), tile)
-        kp = silu(lax.dot_general(x, wkbuf[...], AB, preferred_element_type=F32))
+        gate = jnp.concatenate(picked[:2], axis=0) + bias
+        steps, gates = [], []
+        for n in range(per_seq):
+            lanes = slice(n * CH, (n + 1) * CH)
+            steps.append(extra[t * per_seq + n] - rate[:, lanes] * soft[:, lanes])
+            gates.append(gate[:, lanes])
+        step = jnp.concatenate(steps, axis=0)
+        beta = 1.0 / (1.0 + jnp.exp(-jnp.concatenate(gates, axis=0)))
+        hi = step.astype(BF16)
+        rest = step - hi.astype(F32)
+        mid = rest.astype(BF16)
+        low = (rest - mid.astype(F32)).astype(BF16)
+        cum = dot1(hi, upto) + (dot1(mid, upto) + dot1(low, upto))
+        count = cum.shape[0]
+        total = jnp.broadcast_to(cum[:, CH - 1 : CH], (count, CH))
+        columns = jnp.transpose(
+            jnp.concatenate(
+                [cum + jnp.log(beta), jnp.exp(total - cum), jnp.zeros((CH - 2 * count, CH), F32)], axis=0
+            )
+        )
+        return beta, cum, jnp.exp(total), jnp.exp(cum), columns
+
+    def weighted(t, kp, rows):
+        kp = silu(kp)
         for h in range(2):
             lanes = slice(h * CH, (h + 1) * CH)
             kbuf[rows, lanes] = unit_rows(kp[:, lanes]).astype(BF16)
-        vp = silu(lax.dot_general(x, wvbuf[...], AB, preferred_element_type=F32))
-        vbuf[rows, :] = vp.astype(BF16)
-        return 0
-
-    lax.fori_loop(0, tiles, project, 0)
-
-    start = jnp.concatenate([eye, jnp.zeros((CH, CH), F32)], axis=1)
-    for p in range(4):
-        state[p] = start
-
-    def advance(n, _):
-        blocks = [rowbuf[n], rowbuf[per_seq + n]]
-        beta = jnp.concatenate([b[0:2] for b in blocks], axis=0)
-        cum = jnp.concatenate([b[2:4] for b in blocks], axis=0)
-        total = jnp.broadcast_to(cum[:, CH - 1 : CH], (4, CH))
-        carry = jnp.exp(total)
-        reach = jnp.exp(total - cum)
-        ecum = jnp.exp(cum)
-        columns = jnp.transpose(
-            jnp.concatenate([beta, cum, reach, jnp.zeros((CH - 12, CH), F32)], axis=0)
-        )
-        ks, vs, ms = [], [], []
+
+    def matrices(t, cum, columns):
+        ms = []
+        for n in range(per_seq):
+            for h in range(2):
+                k = part(kbuf, t, n, h)
+                gram = lax.dot_general(k, k, ABT, preferred_element_type=F32)
+                r = 2 * n + h
+                ms.append(jnp.where(row > col, gram * jnp.exp(columns[:, r : r + 1] - cum[r : r + 1, :]), 0.0))
+        return ms
+
+    def part(buf, s, n, h):
+        start = (s * per_seq + n) * CH
+        return buf[start : start + CH, h * CH : (h + 1) * CH]
+
+    rows_of = []
+    ms = []
+    for t in range(tiles):
+        x_copy(t).wait()
+        gt = jnp.concatenate([jnp.transpose(g) for g in halves(t, gatew, ABT, 2)], axis=1)
+        count = 2 if True or (True and t == tiles - 1) else 1
+        size = tile // count
+        kps = halves(t, wkbuf, AB, count)
+        if t == 0:
+            others[3].wait()
+        vps = halves(t, wvbuf, AB, count)
+        rows_of.append(scalars(t, gt))
+        for i in range(count):
+            weighted(t, kps[i], slice(t * tile + i * size, t * tile + (i + 1) * size))
+        ms += matrices(t, rows_of[t][1], rows_of[t][4])
+        for i in range(count):
+            vbuf[t * tile + i * size : t * tile + (i + 1) * size, :] = silu(vps[i]).astype(BF16)
+
+    items = [(s, n, h) for s in range(2) for n in range(per_seq) for h in range(2)]
+    invs = inverses_of(ms)
+    us = []
+    for (s, n, h), inv in zip(items, invs):
+        beta, _, _, _, columns = rows_of[s]
+        r = 2 * n + h
+        us.append(columns[:, 8 + r : 9 + r] * inv * beta[r : r + 1, :])
+    pulls = [
+        dot1(u * rows_of[s][3][2 * n + h : 2 * n + h + 1, :], part(kbuf, s, n, h)).astype(BF16)
+        for (s, n, h), u in zip(items, us)
+    ]
+    freshs = [dot1(u, part(vbuf, s, n, h)).astype(BF16) for (s, n, h), u in zip(items, us)]
+    boths = {
+        (s, n, h): dot1(part(kbuf, s, n, h), jnp.concatenate([pull, fresh], axis=1), ATB)
+        for (s, n, h), pull, fresh in zip(items, pulls, freshs)
+    }
+    for n in range(per_seq):
         for p in range(4):
             s, h = divmod(p, 2)
-            rows = pl.ds(pl.multiple_of((s * per_seq + n) * CH, CH), CH)
-            lanes = slice(h * CH, (h + 1) * CH)
-            ks.append(kbuf[rows, lanes])
-            vs.append(vbuf[rows, lanes])
-        grams = [lax.dot_general(k, k, ABT, preferred_element_type=F32) for k in ks]
-        for p in range(4):
-            gap = jnp.minimum(columns[:, 4 + p : 5 + p] - cum[p : p + 1, :], 0.0)
-            ms.append(jnp.where(row > col, columns[:, p : p + 1] * grams[p] * jnp.exp(gap), 0.0))
-        invs = inverses_of(ms)
-        us = [columns[:, 8 + p : 9 + p] * invs[p] * beta[p : p + 1, :] for p in range(4)]
-        pulls = [dot1(us[p] * ecum[p : p + 1, :], ks[p]).astype(BF16) for p in range(4)]
-        freshs = [dot1(us[p], vs[p]).astype(BF16) for p in range(4)]
-        boths = [
-            dot1(k, jnp.concatenate([pull, fresh], axis=1), ATB)
-            for k, pull, fresh in zip(ks, pulls, freshs)
-        ]
-        for p in range(4):
+            both = boths[s, n, h]
+            c_row = rows_of[s][2][2 * n + h : 2 * n + h + 1, :]
+            if n == 0:
+                state[p, :, :CH] = c_row * eye - both[:, :CH]
+                state[p, :, CH:] = both[:, CH:]
+                continue
             before = state[p]
-            moved = dot1(boths[p][:, :CH], before)
-            c_row = carry[p : p + 1, :]
+            moved = dot1(both[:, :CH], before)
             state[p, :, :CH] = c_row * before[:, :CH] - moved[:, :CH]
-            state[p, :, CH:] = c_row * before[:, CH:] - moved[:, CH:] + boths[p][:, CH:]
-        return 0
-
-    lax.fori_loop(0, per_seq, advance, 0)
+            state[p, :, CH:] = c_row * before[:, CH:] - moved[:, CH:] + both[:, CH:]
+
     for k, o in enumerate((o0, o1, o2, o3)):
         p = lax.rem(here + k, 4)
         o[:CH, :] = state[p, :, :CH]
@@ -321,7 +345,7 @@
 ):
     seqs, seg, width = tokens.shape
     cols = key_matrix.shape[1]
-    tile = 256
+    tile = seg
     tiles = seqs * seg // tile
     chunks = seqs * seg // CH
     extra = jnp.transpose(extra_log_decay.reshape(chunks, CH, 2), (0, 2, 1))
@@ -342,7 +366,6 @@
             pltpu.SMEM(head_log_decay_rate.shape, F32),
             pltpu.VMEM((seqs * seg, cols), BF16),
             pltpu.VMEM((seqs * seg, cols), BF16),
-            pltpu.VMEM((chunks, 8, CH), F32),
             pltpu.VMEM((4, CH, 2 * CH), F32),
             pltpu.SemaphoreType.DMA((tiles + 7,)),
         ],

time: 57.3 us -> 49.4 us (0.86)
  Pallas kernels: 20.4 us -> 12.4 us
    pallas_call x1, Pallas kernels: 17.6 us -> 9.68 us  [shards(): pl.pallas_call(maps_kernel, out_shape=[jax.ShapeDtypeStruct((2 * CH, CH),...]
where the time goes in v3:
time: 49.4 us; the launch traced here: 49.2 us
  blocking collectives  14.9 us (30%)
  Pallas kernels  12.4 us (25%)
  starting transfers between devices  12.2 us (25%)
  waiting for transfers between devices  8.96 us (18%)
  between operations  0.72 us (1%)
    all_to_all x1, blocking collectives, shards(): got = lax.all_to_all(rows, SP, 0, 0, tiled=True)  14.9 us
    ppermute x6, starting transfers between devices, spread(): lax.ppermute(arrays[k], axis, [(i, (i + k) % 4) for i in range(4)])  12.2 us
    pallas_call x1, Pallas kernels, shards(): pl.pallas_call(maps_kernel, out_shape=[jax.ShapeDtypeStruct((2 * CH, CH),...  9.68 us
    ppermute x6, waiting for transfers between devices, spread(): lax.ppermute(arrays[k], axis, [(i, (i + k) % 4) for i in range(4)])  8.96 us
    pallas_call x1, Pallas kernels, shards(): pl.pallas_call(columns_kernel, out_shape=jax.ShapeDtypeStruct((ranks, 16,...  1.33 us
  transfers between devices with their start and end apart: 6, of which 5 were waited for; matrix products, arithmetic and copies ran while one was open for 0% of the time, Pallas kernels for 0%

profile of v3, /device:TPU:2, one launch (start us, length us, event | category | flops | bytes accessed | tf_op | source)
XLA Modules:
  0.0 49.2 jit_solution(10979740029701060839)
XLA Ops:
  0.6 0.0 copy-start.3
  0.6 0.0 copy-start.2
  0.7 0.0 copy-start.1
  0.7 0.0 copy-start
  0.7 0.0 copy-start.4
  0.7 9.7 %maps.1 = (f32[256,128]{1,0:T(8,128)S(1)}, f32[256,128]{1,0:T(8,128)S(1)}, f32[256,128]{1,0:T(8,128)S(1)}, f32[256,128]{1,0:T(8,128)S(1)}) custom-call(bf16[2,512,2048]{2,1,0:T(8,128)(2,1)} %x_hbm.1, bf16[2048,256]{1,0:T(8,128)(2,1)} %wk_hbm.1, bf16[2048,256]{1,0:T(8,128)(2,1)} %wv_hbm.1, bf16[16,2048]{1,0:T(8,128)(2,1)} %bitcast.7, ...), custom_call_target="tpu_custom_call" | custom-call | tf_op jit(solution)/shard_map/maps/pallas_call | solution.py:354
  10.4 1.7 %collective-permute-start = (f32[256,128]{1,0:T(8,128)S(1)}, f32[256,128]{1,0:T(8,128)S(1)}, u32[]{:S(2)}, u32[]{:S(2)}) collective-permute-start(f32[256,128]{1,0:T(8,128)S(1)} %get-tuple-element.11), channel_id=1, source_target_pairs={{0,8},{8,16},{16,24},{24,0},{1,9},{9,17},{17,25},{25,1},{2,10},{10... | collective-permute-start | bytes 393224 | tf_op jit(solution)/shard_map/ppermute | solution.py:327
  12.0 2.9 %collective-permute-start.1 = (f32[256,128]{1,0:T(8,128)S(1)}, f32[256,128]{1,0:T(8,128)S(1)}, u32[]{:S(2)}, u32[]{:S(2)}) collective-permute-start(f32[256,128]{1,0:T(8,128)S(1)} %get-tuple-element.12), channel_id=1, source_target_pairs={{0,16},{8,24},{16,0},{24,8},{1,17},{9,25},{17,1},{25,9},{2,18},{10... | collective-permute-start | bytes 393224 | tf_op jit(solution)/shard_map/ppermute | solution.py:327
  14.9 1.3 %collective-permute-start.2 = (f32[256,128]{1,0:T(8,128)S(1)}, f32[256,128]{1,0:T(8,128)S(1)}, u32[]{:S(2)}, u32[]{:S(2)}) collective-permute-start(f32[256,128]{1,0:T(8,128)S(1)} %get-tuple-element.13), channel_id=1, source_target_pairs={{0,24},{8,0},{16,8},{24,16},{1,25},{9,1},{17,9},{25,17},{2,26},{10... | collective-permute-start | bytes 393224 | tf_op jit(solution)/shard_map/ppermute | solution.py:327
  16.3 0.7 %collective-permute-done.r1 = f32[256,128]{1,0:T(8,128)S(1)} collective-permute-done((f32[256,128]{1,0:T(8,128)S(1)}, f32[256,128]{1,0:T(8,128)S(1)}, u32[]{:S(2)}, u32[]{:S(2)}) %collective-permute-start) | collective-permute-done | bytes 131104 | tf_op jit(solution)/shard_map/ppermute | solution.py:327
  17.0 4.0 %collective-permute-done.1.r2 = f32[256,128]{1,0:T(8,128)S(1)} collective-permute-done((f32[256,128]{1,0:T(8,128)S(1)}, f32[256,128]{1,0:T(8,128)S(1)}, u32[]{:S(2)}, u32[]{:S(2)}) %collective-permute-start.1) | collective-permute-done | bytes 131104 | tf_op jit(solution)/shard_map/ppermute | solution.py:327
  21.0 0.0 collective-permute-done.2.r3
  21.0 0.8 %segments.1 = (f32[160,128]{1,0:T(8,128)S(1)}, f32[160,128]{1,0:T(8,128)S(1)}, f32[160,128]{1,0:T(8,128)S(1)}, f32[160,128]{1,0:T(8,128)S(1)}) custom-call(f32[256,128]{1,0:T(8,128)S(1)} %get-tuple-element.10.r0, f32[256,128]{1,0:T(8,128)S(1)} %collective-permute-done.r1, f32[256,128]{1,0:T(8,128)S(1)} %collective-permute-done.1.r2, ...), custom_call_target="tpu_custom_call" | custom-call | tf_op jit(solution)/shard_map/segments/pallas_call | solution.py:390
  21.7 2.0 %collective-permute-start.3 = (f32[160,128]{1,0:T(8,128)S(1)}, f32[160,128]{1,0:T(8,128)S(1)}, u32[]{:S(2)}, u32[]{:S(2)}) collective-permute-start(f32[160,128]{1,0:T(8,128)S(1)} %get-tuple-element.15), channel_id=1, source_target_pairs={{0,32},{32,64},{64,96},{96,0},{1,33},{33,65},{65,97},{97,1},{2,34}... | collective-permute-start | bytes 245768 | tf_op jit(solution)/shard_map/ppermute | solution.py:327
  23.7 3.3 %collective-permute-start.4 = (f32[160,128]{1,0:T(8,128)S(1)}, f32[160,128]{1,0:T(8,128)S(1)}, u32[]{:S(2)}, u32[]{:S(2)}) collective-permute-start(f32[160,128]{1,0:T(8,128)S(1)} %get-tuple-element.16), channel_id=1, source_target_pairs={{0,64},{32,96},{64,0},{96,32},{1,65},{33,97},{65,1},{97,33},{2,66}... | collective-permute-start | bytes 245768 | tf_op jit(solution)/shard_map/ppermute | solution.py:327
  27.0 1.0 %collective-permute-start.5 = (f32[160,128]{1,0:T(8,128)S(1)}, f32[160,128]{1,0:T(8,128)S(1)}, u32[]{:S(2)}, u32[]{:S(2)}) collective-permute-start(f32[160,128]{1,0:T(8,128)S(1)} %get-tuple-element.17), channel_id=1, source_target_pairs={{0,96},{32,0},{64,32},{96,64},{1,97},{33,1},{65,33},{97,65},{2,98}... | collective-permute-start | bytes 245768 | tf_op jit(solution)/shard_map/ppermute | solution.py:327
  28.0 1.8 %collective-permute-done.3.r1 = f32[160,128]{1,0:T(8,128)S(1)} collective-permute-done((f32[160,128]{1,0:T(8,128)S(1)}, f32[160,128]{1,0:T(8,128)S(1)}, u32[]{:S(2)}, u32[]{:S(2)}) %collective-permute-start.3) | collective-permute-done | bytes 81952 | tf_op jit(solution)/shard_map/ppermute | solution.py:327
  29.8 2.0 %collective-permute-done.4.r2 = f32[160,128]{1,0:T(8,128)S(1)} collective-permute-done((f32[160,128]{1,0:T(8,128)S(1)}, f32[160,128]{1,0:T(8,128)S(1)}, u32[]{:S(2)}, u32[]{:S(2)}) %collective-permute-start.4) | collective-permute-done | bytes 81952 | tf_op jit(solution)/shard_map/ppermute | solution.py:327
  31.8 0.5 collective-permute-done.5.r3
  32.3 0.0 copy-done
  32.3 1.3 %columns.1 = f32[16,16,128]{2,1,0:T(8,128)S(1)} custom-call(f32[160,128]{1,0:T(8,128)S(1)} %get-tuple-element.14.r0, f32[160,128]{1,0:T(8,128)S(1)} %collective-permute-done.3.r1, f32[160,128]{1,0:T(8,128)S(1)} %collective-permute-done.4.r2, f32[160,128]{1,0:T(8,128)S(1)} %collective-permute-done.5.r3, bf16[2,2,128]{2,1,0:T(2,128)(2,1)S(1)} %copy-done, ...), custom_call_target="tpu_custom_call" | custom-call | tf_op jit(solution)/shard_map/columns/pallas_call | solution.py:400
  33.6 14.9 %all_to_all.5.r_ref = f32[16,16,128]{2,1,0:T(8,128)S(1)} all-to-all(f32[16,16,128]{2,1,0:T(8,128)S(1)} %columns.1), channel_id=1, replica_groups=mesh['gr'=2,'sp_0'=4,'sp_1'=4,'tp'=8] {'sp_0','sp_1'}, dimensions={0} | all-to-all | bytes 262144 | tf_op jit(solution)/shard_map/all_to_all | solution.py:409
  48.6 0.0 copy-done.4
  48.6 0.7 %finish.1 = (bf16[2,2,8,128]{3,2,1,0:T(8,128)(2,1)}, bf16[2,2,128]{2,1,0:T(2,128)(2,1)}) custom-call(f32[16,16,128]{2,1,0:T(8,128)S(1)} %all_to_all.5.r_ref, f32[1,128]{1,0:T(1,128)S(1)} %bitcast.6), custom_call_target="tpu_custom_call" | custom-call | tf_op jit(solution)/shard_map/finish/pallas_call | solution.py:410
  (3 shorter events, 0.0 us)
Async XLA Ops:
  0.6 31.6 %copy-start.3 = (f32[2,2]{1,0:T(2,128)S(1)}, f32[2,2]{1,0:T(2,128)}, u32[]{:S(2)}) copy-start(f32[2,2]{1,0:T(2,128)} %gate_ref.1) | copy-start | bytes 52
  0.6 31.6 %copy-start.2 = (bf16[2,2,128]{2,1,0:T(2,128)(2,1)S(1)}, bf16[2,2,128]{2,1,0:T(2,128)(2,1)}, u32[]{:S(2)}) copy-start(bf16[2,2,128]{2,1,0:T(2,128)(2,1)} %value_ref.1) | copy-start | bytes 3076
  0.7 31.6 %copy-start.1 = (bf16[2,2,128]{2,1,0:T(2,128)(2,1)S(1)}, bf16[2,2,128]{2,1,0:T(2,128)(2,1)}, u32[]{:S(2)}) copy-start(bf16[2,2,128]{2,1,0:T(2,128)(2,1)} %key_ref.1) | copy-start | bytes 3076
  0.7 31.6 %copy-start = (bf16[2,2,128]{2,1,0:T(2,128)(2,1)S(1)}, bf16[2,2,128]{2,1,0:T(2,128)(2,1)}, u32[]{:S(2)}) copy-start(bf16[2,2,128]{2,1,0:T(2,128)(2,1)} %query_ref.1) | copy-start | bytes 3076
  0.7 47.9 %copy-start.4 = (f32[128]{0:T(128)S(1)}, f32[128]{0:T(128)}, u32[]{:S(2)}) copy-start(f32[128]{0:T(128)} %param.25) | copy-start | bytes 1540
  10.4 6.6 %collective-permute-start = (f32[256,128]{1,0:T(8,128)S(1)}, f32[256,128]{1,0:T(8,128)S(1)}, u32[]{:S(2)}, u32[]{:S(2)}) collective-permute-start(f32[256,128]{1,0:T(8,128)S(1)} %get-tuple-element.11), channel_id=1, source_target_pairs={{0,8},{8,16},{16,24},{24,0},{1,9},{9,17},{17,25},{25,1},{2,10},{10... | collective-permute-start | bytes 393224 | tf_op jit(solution)/shard_map/ppermute | solution.py:327
  12.0 8.9 %collective-permute-start.1 = (f32[256,128]{1,0:T(8,128)S(1)}, f32[256,128]{1,0:T(8,128)S(1)}, u32[]{:S(2)}, u32[]{:S(2)}) collective-permute-start(f32[256,128]{1,0:T(8,128)S(1)} %get-tuple-element.12), channel_id=1, source_target_pairs={{0,16},{8,24},{16,0},{24,8},{1,17},{9,25},{17,1},{25,9},{2,18},{10... | collective-permute-start | bytes 393224 | tf_op jit(solution)/shard_map/ppermute | solution.py:327
  14.9 6.0 %collective-permute-start.2 = (f32[256,128]{1,0:T(8,128)S(1)}, f32[256,128]{1,0:T(8,128)S(1)}, u32[]{:S(2)}, u32[]{:S(2)}) collective-permute-start(f32[256,128]{1,0:T(8,128)S(1)} %get-tuple-element.13), channel_id=1, source_target_pairs={{0,24},{8,0},{16,8},{24,16},{1,25},{9,1},{17,9},{25,17},{2,26},{10... | collective-permute-start | bytes 393224 | tf_op jit(solution)/shard_map/ppermute | solution.py:327
  21.7 8.1 %collective-permute-start.3 = (f32[160,128]{1,0:T(8,128)S(1)}, f32[160,128]{1,0:T(8,128)S(1)}, u32[]{:S(2)}, u32[]{:S(2)}) collective-permute-start(f32[160,128]{1,0:T(8,128)S(1)} %get-tuple-element.15), channel_id=1, source_target_pairs={{0,32},{32,64},{64,96},{96,0},{1,33},{33,65},{65,97},{97,1},{2,34}... | collective-permute-start | bytes 245768 | tf_op jit(solution)/shard_map/ppermute | solution.py:327
  23.7 8.1 %collective-permute-start.4 = (f32[160,128]{1,0:T(8,128)S(1)}, f32[160,128]{1,0:T(8,128)S(1)}, u32[]{:S(2)}, u32[]{:S(2)}) collective-permute-start(f32[160,128]{1,0:T(8,128)S(1)} %get-tuple-element.16), channel_id=1, source_target_pairs={{0,64},{32,96},{64,0},{96,32},{1,65},{33,97},{65,1},{97,33},{2,66}... | collective-permute-start | bytes 245768 | tf_op jit(solution)/shard_map/ppermute | solution.py:327
  27.0 5.3 %collective-permute-start.5 = (f32[160,128]{1,0:T(8,128)S(1)}, f32[160,128]{1,0:T(8,128)S(1)}, u32[]{:S(2)}, u32[]{:S(2)}) collective-permute-start(f32[160,128]{1,0:T(8,128)S(1)} %get-tuple-element.17), channel_id=1, source_target_pairs={{0,96},{32,0},{64,32},{96,64},{1,97},{33,1},{65,33},{97,65},{2,98}... | collective-permute-start | bytes 245768 | tf_op jit(solution)/shard_map/ppermute | solution.py:327

commit v4 on v3

--- a/solution.py
+++ b/solution.py
@@ -10,6 +10,8 @@
 
 SP = ("sp_0", "sp_1")
 CH = 128
+ROWS = 32
+SHIFTS = (0, 2, 3, 1)
 F32 = jnp.float32
 BF16 = jnp.bfloat16
 AB = (((1,), (0,)), ((), ()))
@@ -88,6 +90,13 @@
             joined.append(jnp.concatenate(pieces, axis=0))
         invs = joined
     return invs
+
+
+def joined(first, second, eye):
+    c1, d1, b1 = first
+    c2, d2, b2 = second
+    moved = dot1(d2, jnp.concatenate([c1 * eye - d1, b1], axis=1))
+    return c1 * c2, c2 * d1 + moved[:, :CH], c2 * b1 - moved[:, CH:] + b2
 
 
 def maps_kernel(
@@ -201,7 +210,7 @@
     for t in range(tiles):
         x_copy(t).wait()
         gt = jnp.concatenate([jnp.transpose(g) for g in halves(t, gatew, ABT, 2)], axis=1)
-        count = 2 if True or (True and t == tiles - 1) else 1
+        count = 2
         size = tile // count
         kps = halves(t, wkbuf, AB, count)
         if t == 0:
@@ -230,43 +239,35 @@
         (s, n, h): dot1(part(kbuf, s, n, h), jnp.concatenate([pull, fresh], axis=1), ATB)
         for (s, n, h), pull, fresh in zip(items, pulls, freshs)
     }
-    for n in range(per_seq):
-        for p in range(4):
-            s, h = divmod(p, 2)
-            both = boths[s, n, h]
+    maps = []
+    for p in range(4):
+        s, h = divmod(p, 2)
+        parts = []
+        for n in range(per_seq):
             c_row = rows_of[s][2][2 * n + h : 2 * n + h + 1, :]
-            if n == 0:
-                state[p, :, :CH] = c_row * eye - both[:, :CH]
-                state[p, :, CH:] = both[:, CH:]
-                continue
-            before = state[p]
-            moved = dot1(both[:, :CH], before)
-            state[p, :, :CH] = c_row * before[:, :CH] - moved[:, :CH]
-            state[p, :, CH:] = c_row * before[:, CH:] - moved[:, CH:] + both[:, CH:]
-
-    for k, o in enumerate((o0, o1, o2, o3)):
-        p = lax.rem(here + k, 4)
-        o[:CH, :] = state[p, :, :CH]
-        o[CH:, :] = state[p, :, CH:]
-
-
-def ordered(refs, scr, here):
-    for k, ref in enumerate(refs):
+            parts.append((c_row, boths[s, n, h][:, :CH], boths[s, n, h][:, CH:]))
+        maps.append(parts)
+    while len(maps[0]) > 1:
+        maps = [[joined(m[i], m[i + 1], eye) for i in range(0, len(m), 2)] for m in maps]
+    for p in range(4):
+        c_row, drop, gain = maps[p][0]
+        state[p, :CH, :] = c_row * eye - drop
+        state[p, CH:, :] = gain
+
+    for k, o in zip(SHIFTS, (o0, o1, o2, o3)):
+        o[...] = state[lax.rem(here + k, 4)]
+
+
+def segments_kernel(r0, r1, r2, r3, out, scr):
+    here = lax.axis_index("sp_1")
+    for k, ref in zip(SHIFTS, (r0, r1, r2, r3)):
         scr[lax.rem(here + 4 - k, 4)] = ref[...]
-
-
-def segments_kernel(r0, r1, r2, r3, o0, o1, o2, o3, scr, bscr):
-    ordered((r0, r1, r2, r3), scr, lax.axis_index("sp_1"))
-    there = lax.axis_index("sp_0")
     state = jnp.concatenate([scr[0, :CH, :], scr[0, CH:, :]], axis=1)
     for t in range(1, 4):
         state = dot3(scr[t, :CH, :], state)
         state = state + jnp.concatenate([jnp.zeros((CH, CH), F32), scr[t, CH:, :]], axis=1)
-    bscr[...] = jnp.transpose(state[:, CH:])
-    for k, o in enumerate((o0, o1, o2, o3)):
-        q = lax.rem(there + k, 4)
-        o[:CH, :] = state[:, :CH]
-        o[CH:, :] = bscr[pl.ds(pl.multiple_of(q * 32, 32), 32), :]
+    out[:CH, :] = state[:, :CH]
+    out[CH:, :] = state[:, CH:]
 
 
 def row_of(ref, s, h):
@@ -274,47 +275,67 @@
     return jnp.sum(jnp.where(iota(two.shape, 0) == h, two, 0.0), axis=0, keepdims=True)
 
 
-def columns_kernel(r0, r1, r2, r3, query_ref, key_ref, value_ref, gate_ref, out, scr, wide):
+def new_token(query_ref, key_ref):
+    pair = lax.axis_index("sp_1")
+    s, h = lax.div(pair, 2), lax.rem(pair, 2)
+    return s, h, unit_rows(row_of(query_ref, s, h)), unit_rows(row_of(key_ref, s, h))
+
+
+def halves_kernel(own, other, query_ref, key_ref, mine, theirs, scr, amap, gain):
     part = lax.axis_index("sp_0")
-    pair = lax.axis_index("sp_1")
-    ordered((r0, r1, r2, r3), scr, part)
-    f = scr[0, CH:, :]
-    for g in range(1, 4):
-        f = dot3(f, scr[g, :CH, :], ABT) + scr[g, CH:, :]
-    s = pair // 2
-    h = lax.rem(pair, 2)
-    qn = unit_rows(row_of(query_ref, s, h))
-    kn = unit_rows(row_of(key_ref, s, h))
+    odd = lax.rem(part, 2)
+    scr[odd] = own[...]
+    scr[1 - odd] = other[...]
+    _, _, qn, kn = new_token(query_ref, key_ref)
+    both = dot3(scr[1, :CH, :], jnp.concatenate([scr[0, :CH, :], scr[0, CH:, :]], axis=1))
+    amap[...] = both[:, :CH]
+    gain[...] = both[:, CH:] + scr[1, CH:, :]
+
+    @pl.when(part < 2)
+    def _():
+        mine[...] = gain[...]
+        theirs[...] = gain[...]
+
+    @pl.when(part >= 2)
+    def _():
+        reads = jnp.concatenate([kn, qn, jnp.zeros((6, CH), F32)], axis=0)
+        through = dot3(reads, jnp.concatenate([amap[...], gain[...]], axis=1))
+        for ref, owner in ((mine, part), (theirs, part - 2)):
+            rows = pl.ds(pl.multiple_of(owner * ROWS, ROWS), ROWS)
+            ref[:ROWS, :] = amap[rows, :]
+            ref[ROWS : ROWS + 8, :] = through[:, :CH]
+            ref[ROWS + 8 : 2 * ROWS + 8, :] = gain[rows, :]
+            ref[2 * ROWS + 8 : 2 * ROWS + 16, :] = through[:, CH:]
+            ref[2 * ROWS + 16 :, :] = jnp.zeros((CH - 2 * ROWS - 16, CH), F32)
+
+
+def rows_kernel(mine, theirs, query_ref, key_ref, value_ref, gate_ref, gain_ref, out, scr):
+    part = lax.axis_index("sp_0")
+    right = jnp.where(part < 2, 0, 1)
+    scr[right] = mine[...]
+    scr[1 - right] = theirs[...]
+    s, h, qn, kn = new_token(query_ref, key_ref)
     vn = row_of(value_ref, s, h)
     bn = 1.0 / (1.0 + jnp.exp(-jnp.full((1, CH), gate_ref[s, h], F32)))
-    count = f.shape[0]
-    mine = iota((count, CH), 1) == iota((count, CH), 0) + part * count
-    vn_col = jnp.sum(jnp.where(mine, jnp.broadcast_to(vn, (count, CH)), 0.0), axis=1, keepdims=True)
-    missing = vn_col - jnp.sum(f * kn, axis=1, keepdims=True)
-    query_read = jnp.sum(f * qn, axis=1, keepdims=True)
     meet = jnp.sum(kn * qn, axis=1, keepdims=True)
-    read = (query_read + (bn[:, :1] * meet) * missing) / math.sqrt(CH)
-    wide[...] = jnp.zeros_like(wide)
-    wide[pl.ds(pl.multiple_of(part * count, 32), count), :] = f + missing * (bn * kn)
-    state = jnp.transpose(wide[...])
-    read_row = jnp.sum(jnp.where(mine, jnp.broadcast_to(read, (count, CH)), 0.0), axis=0, keepdims=True)
-    read_rows = jnp.broadcast_to(read_row, (8, CH))
-    for p in range(out.shape[0]):
-        out[p, :8, :] = state[8 * p : 8 * p + 8, :]
-        out[p, 8:, :] = read_rows
-
-
-def finish_kernel(r_ref, gain_ref, cache_ref, read_ref):
+    diagonal = iota((ROWS, CH), 1) == iota((ROWS, CH), 0) + part * ROWS
+    k_col = jnp.sum(jnp.where(diagonal, jnp.broadcast_to(kn, (ROWS, CH)), 0.0), axis=1, keepdims=True)
+    final = dot3(scr[1, : ROWS + 8, :], scr[0]) + scr[1, ROWS + 8 : 2 * ROWS + 16, :]
+    missing = vn - final[ROWS : ROWS + 1, :]
+    state = final[:ROWS, :] + k_col * (bn * missing)
+    read = (final[ROWS + 1 : ROWS + 2, :] + bn * meet * missing) / math.sqrt(CH)
+    scale = lax.rsqrt(jnp.mean(read * read, axis=-1, keepdims=True) + 1e-06)
+    read_rows = jnp.broadcast_to(read * scale * gain_ref[...], (8, CH))
+    for y in range(4):
+        out[y, :8, :] = state[8 * y : 8 * y + 8, :]
+        out[y, 8:, :] = read_rows
+
+
+def finish_kernel(got, cache_ref, read_ref):
     for s in range(2):
-        reads = []
         for h in range(2):
-            j = 2 * s + h
-            total = (r_ref[j] + r_ref[4 + j]) + (r_ref[8 + j] + r_ref[12 + j])
-            cache_ref[s, h] = total[:8, :].astype(BF16)
-            read = total[8:9, :]
-            scale = lax.rsqrt(jnp.mean(read * read, axis=-1, keepdims=True) + 1e-06)
-            reads.append(read * scale * gain_ref[...])
-        read_ref[s] = jnp.concatenate(reads, axis=0).astype(BF16)
+            cache_ref[s, h] = got[2 * s + h, :8, :].astype(BF16)
+        read_ref[s] = jnp.concatenate([got[2 * s + h, 8:9, :] for h in range(2)], axis=0).astype(BF16)
 
 
 def vmem(count):
@@ -322,10 +343,14 @@
 
 
 def spread(arrays, axis):
-    out = [arrays[0]]
-    for k in range(1, 4):
-        out.append(lax.ppermute(arrays[k], axis, [(i, (i + k) % 4) for i in range(4)]))
-    return out
+    return [
+        lax.ppermute(a, axis, [(i, (i + k) % 4) for i in range(4)]) if k else a
+        for k, a in zip(SHIFTS, arrays)
+    ]
+
+
+def swap(array, axis, bit):
+    return lax.ppermute(array, axis, [(i, i ^ bit) for i in range(4)])
 
 
 def shards(
@@ -366,7 +391,7 @@
             pltpu.SMEM(head_log_decay_rate.shape, F32),
             pltpu.VMEM((seqs * seg, cols), BF16),
             pltpu.VMEM((seqs * seg, cols), BF16),
-            pltpu.VMEM((4, CH, 2 * CH), F32),
+            pltpu.VMEM((4, 2 * CH, CH), F32),
             pltpu.SemaphoreType.DMA((tiles + 7,)),
         ],
         compiler_params=pltpu.CompilerParams(vmem_limit_bytes=24 * 2**20),
@@ -387,37 +412,57 @@
         )
     )
     small = pltpu.CompilerParams(vmem_limit_bytes=8 * 2**20)
-    pieces = pl.pallas_call(
+    segment = pl.pallas_call(
         segments_kernel,
-        out_shape=[jax.ShapeDtypeStruct((CH + 32, CH), F32)] * 4,
+        out_shape=jax.ShapeDtypeStruct((2 * CH, CH), F32),
         in_specs=vmem(4),
-        out_specs=vmem(4),
-        scratch_shapes=[pltpu.VMEM((4, 2 * CH, CH), F32), pltpu.VMEM((CH, CH), F32)],
+        out_specs=vmem(1)[0],
+        scratch_shapes=[pltpu.VMEM((4, 2 * CH, CH), F32)],
         compiler_params=small,
         name="segments",
     )(*spread(maps, "sp_1"))
-    ranks = lax.axis_size(SP)
+    mine, theirs = pl.pallas_call(
+        halves_kernel,
+        out_shape=[jax.ShapeDtypeStruct((CH, CH), F32)] * 2,
+        in_specs=vmem(4),
+        out_specs=vmem(2),
+        scratch_shapes=[
+            pltpu.VMEM((2, 2 * CH, CH), F32),
+            pltpu.VMEM((CH, CH), F32),
+            pltpu.VMEM((CH, CH), F32),
+        ],
+        compiler_params=small,
+        name="halves",
+    )(segment, swap(segment, "sp_0", 1), next_token_query, next_token_key)
     rows = pl.pallas_call(
-        columns_kernel,
-        out_shape=jax.ShapeDtypeStruct((ranks, 16, CH), F32),
-        in_specs=[*vmem(7), smem],
-        out_specs=pl.BlockSpec(memory_space=pltpu.VMEM),
-        scratch_shapes=[pltpu.VMEM((4, CH + 32, CH), F32), pltpu.VMEM((CH, CH), F32)],
+        rows_kernel,
+        out_shape=jax.ShapeDtypeStruct((4, 16, CH), F32),
+        in_specs=[*vmem(5), smem, *vmem(1)],
+        out_specs=vmem(1)[0],
+        scratch_shapes=[pltpu.VMEM((2, CH, CH), F32)],
         compiler_params=small,
-        name="columns",
-    )(*spread(pieces, "sp_0"), next_token_query, next_token_key, next_token_value, next_token_gate)
-    got = lax.all_to_all(rows, SP, 0, 0, tiled=True)
+        name="rows",
+    )(
+        mine,
+        swap(theirs, "sp_0", 2),
+        next_token_query,
+        next_token_key,
+        next_token_value,
+        next_token_gate,
+        readout_norm_gain.reshape(1, CH),
+    )
+    got = lax.all_to_all(rows, "sp_1", 0, 0, tiled=True)
     return pl.pallas_call(
         finish_kernel,
         out_shape=[
             jax.ShapeDtypeStruct((2, 2, 8, CH), BF16),
             jax.ShapeDtypeStruct((2, 2, CH), BF16),
         ],
-        in_specs=vmem(2),
+        in_specs=vmem(1),
         out_specs=vmem(2),
         compiler_params=small,
         name="finish",
-    )(got, readout_norm_gain.reshape(1, CH))
+    )(got)
 
 
 def solution(mesh):

time: 49.4 us -> 43.4 us (0.88)
  blocking collectives: 14.9 us -> 9.47 us
  waiting for transfers between devices: 8.96 us -> 10.5 us
  starting transfers between devices: 12.2 us -> 10.8 us
  Pallas kernels: 12.4 us -> 11.9 us
    all_to_all x1, blocking collectives: 14.9 us -> 9.47 us  [shards(): got = lax.all_to_all(rows, 'sp_1', 0, 0, tiled=True)]
    ppermute x6 -> x5, waiting for transfers between devices: 8.96 us -> 10.5 us  [the longest x2 5.28 us: swap(): return lax.ppermute(array, axis, [(i, i ^ bit) for i in range(4)])]
    ppermute x6 -> x5, starting transfers between devices: 12.2 us -> 10.8 us  [the longest x2 5.45 us: swap(): return lax.ppermute(array, axis, [(i, i ^ bit) for i in range(4)])]
    pallas_call x2 -> x3, Pallas kernels: 2.09 us -> 1.75 us  [the longest x1 0.83 us: shards(): pl.pallas_call(rows_kernel, out_shape=jax.ShapeDtypeStruct((4, 16, CH), F...]
  transfers between devices with their start and end apart: 6 -> 5, of which waited for: 5 -> 5; matrix products, arithmetic and copies ran while one was open for 0% -> 0% of each run, Pallas kernels for 0% -> 0%
where the time goes in v4:
time: 43.4 us; the launch traced here: 43.3 us
  Pallas kernels  11.9 us (27%)
  starting transfers between devices  10.8 us (25%)
  waiting for transfers between devices  10.5 us (24%)
  blocking collectives  9.47 us (22%)
  between operations  0.71 us (2%)
    pallas_call x1, Pallas kernels, shards(): pl.pallas_call(maps_kernel, out_shape=[jax.ShapeDtypeStruct((2 * CH, CH),...  9.5 us
    all_to_all x1, blocking collectives, shards(): got = lax.all_to_all(rows, 'sp_1', 0, 0, tiled=True)  9.47 us
    ppermute x2, starting transfers between devices, swap(): return lax.ppermute(array, axis, [(i, i ^ bit) for i in range(4)])  5.45 us
    ppermute x3, starting transfers between devices, spread(): lax.ppermute(a, axis, [(i, (i + k) % 4) for i in range(4)])  5.31 us
    ppermute x2, waiting for transfers between devices, swap(): return lax.ppermute(array, axis, [(i, i ^ bit) for i in range(4)])  5.28 us
    ppermute x3, waiting for transfers between devices, spread(): lax.ppermute(a, axis, [(i, (i + k) % 4) for i in range(4)])  5.21 us
  transfers between devices with their start and end apart: 5, of which 5 were waited for; matrix products, arithmetic and copies ran while one was open for 0% of the time, Pallas kernels for 0%

profile of v4, /device:TPU:2, one launch (start us, length us, event | category | flops | bytes accessed | tf_op | source)
XLA Modules:
  0.0 43.3 jit_solution(16492244818516089767)
XLA Ops:
  0.6 0.0 copy-start.1
  0.6 0.0 copy-start
  0.7 0.0 copy-start.4
  0.7 0.0 copy-start.3
  0.7 0.0 copy-start.2
  0.7 9.5 %maps.1 = (f32[256,128]{1,0:T(8,128)S(1)}, f32[256,128]{1,0:T(8,128)S(1)}, f32[256,128]{1,0:T(8,128)S(1)}, f32[256,128]{1,0:T(8,128)S(1)}) custom-call(bf16[2,512,2048]{2,1,0:T(8,128)(2,1)} %x_hbm.1, bf16[2048,256]{1,0:T(8,128)(2,1)} %wk_hbm.1, bf16[2048,256]{1,0:T(8,128)(2,1)} %wv_hbm.1, bf16[16,2048]{1,0:T(8,128)(2,1)} %bitcast.7, ...), custom_call_target="tpu_custom_call" | custom-call | tf_op jit(solution)/shard_map/maps/pallas_call | solution.py:379
  10.2 3.3 %collective-permute-start = (f32[256,128]{1,0:T(8,128)S(1)}, f32[256,128]{1,0:T(8,128)S(1)}, u32[]{:S(2)}, u32[]{:S(2)}) collective-permute-start(f32[256,128]{1,0:T(8,128)S(1)} %get-tuple-element.9), channel_id=1, source_target_pairs={{0,16},{8,24},{16,0},{24,8},{1,17},{9,25},{17,1},{25,9},{2,18},{10... | collective-permute-start | bytes 393224 | tf_op jit(solution)/shard_map/ppermute | solution.py:347
  13.5 1.1 %collective-permute-start.1 = (f32[256,128]{1,0:T(8,128)S(1)}, f32[256,128]{1,0:T(8,128)S(1)}, u32[]{:S(2)}, u32[]{:S(2)}) collective-permute-start(f32[256,128]{1,0:T(8,128)S(1)} %get-tuple-element.10), channel_id=1, source_target_pairs={{0,24},{8,0},{16,8},{24,16},{1,25},{9,1},{17,9},{25,17},{2,26},{10... | collective-permute-start | bytes 393224 | tf_op jit(solution)/shard_map/ppermute | solution.py:347
  14.5 1.0 %collective-permute-start.2 = (f32[256,128]{1,0:T(8,128)S(1)}, f32[256,128]{1,0:T(8,128)S(1)}, u32[]{:S(2)}, u32[]{:S(2)}) collective-permute-start(f32[256,128]{1,0:T(8,128)S(1)} %get-tuple-element.11), channel_id=1, source_target_pairs={{0,8},{8,16},{16,24},{24,0},{1,9},{9,17},{17,25},{25,1},{2,10},{10... | collective-permute-start | bytes 393224 | tf_op jit(solution)/shard_map/ppermute | solution.py:347
  15.5 2.2 %collective-permute-done.r1 = f32[256,128]{1,0:T(8,128)S(1)} collective-permute-done((f32[256,128]{1,0:T(8,128)S(1)}, f32[256,128]{1,0:T(8,128)S(1)}, u32[]{:S(2)}, u32[]{:S(2)}) %collective-permute-start) | collective-permute-done | bytes 131104 | tf_op jit(solution)/shard_map/ppermute | solution.py:347
  17.7 2.5 %collective-permute-done.1.r2 = f32[256,128]{1,0:T(8,128)S(1)} collective-permute-done((f32[256,128]{1,0:T(8,128)S(1)}, f32[256,128]{1,0:T(8,128)S(1)}, u32[]{:S(2)}, u32[]{:S(2)}) %collective-permute-start.1) | collective-permute-done | bytes 131104 | tf_op jit(solution)/shard_map/ppermute | solution.py:347
  20.2 0.5 %collective-permute-done.2.r3 = f32[256,128]{1,0:T(8,128)S(1)} collective-permute-done((f32[256,128]{1,0:T(8,128)S(1)}, f32[256,128]{1,0:T(8,128)S(1)}, u32[]{:S(2)}, u32[]{:S(2)}) %collective-permute-start.2) | collective-permute-done | bytes 131104 | tf_op jit(solution)/shard_map/ppermute | solution.py:347
  20.7 0.7 %segments.1.own = f32[256,128]{1,0:T(8,128)S(1)} custom-call(f32[256,128]{1,0:T(8,128)S(1)} %get-tuple-element.8.r0, f32[256,128]{1,0:T(8,128)S(1)} %collective-permute-done.r1, f32[256,128]{1,0:T(8,128)S(1)} %collective-permute-done.1.r2, f32[256,128]{1,0:T(8,128)S(1)} %collective-permute-done.2.r3), custom_call_target="tpu_custom_call" | custom-call | tf_op jit(solution)/shard_map/segments/pallas_call | solution.py:415
  21.4 2.0 %collective-permute-start.3 = (f32[256,128]{1,0:T(8,128)S(1)}, f32[256,128]{1,0:T(8,128)S(1)}, u32[]{:S(2)}, u32[]{:S(2)}) collective-permute-start(f32[256,128]{1,0:T(8,128)S(1)} %segments.1.own), channel_id=1, source_target_pairs={{0,32},{32,0},{64,96},{96,64},{1,33},{33,1},{65,97},{97,65},{2,34}... | collective-permute-start | bytes 393224 | tf_op jit(solution)/shard_map/ppermute | solution.py:353
  23.4 3.0 %collective-permute-done.3.other = f32[256,128]{1,0:T(8,128)S(1)} collective-permute-done((f32[256,128]{1,0:T(8,128)S(1)}, f32[256,128]{1,0:T(8,128)S(1)}, u32[]{:S(2)}, u32[]{:S(2)}) %collective-permute-start.3) | collective-permute-done | bytes 131104 | tf_op jit(solution)/shard_map/ppermute | solution.py:353
  26.5 0.0 copy-done.1
  26.5 0.0 copy-done
  26.5 0.2 halves.1
  26.7 3.4 %collective-permute-start.4 = (f32[128,128]{1,0:T(8,128)S(1)}, f32[128,128]{1,0:T(8,128)S(1)}, u32[]{:S(2)}, u32[]{:S(2)}) collective-permute-start(f32[128,128]{1,0:T(8,128)S(1)} %get-tuple-element.13), channel_id=1, source_target_pairs={{0,64},{32,96},{64,0},{96,32},{1,65},{33,97},{65,1},{97,33},{2,66}... | collective-permute-start | bytes 196616 | tf_op jit(solution)/shard_map/ppermute | solution.py:353
  30.1 2.2 %collective-permute-done.4.theirs = f32[128,128]{1,0:T(8,128)S(1)} collective-permute-done((f32[128,128]{1,0:T(8,128)S(1)}, f32[128,128]{1,0:T(8,128)S(1)}, u32[]{:S(2)}, u32[]{:S(2)}) %collective-permute-start.4) | collective-permute-done | bytes 65568 | tf_op jit(solution)/shard_map/ppermute | solution.py:353
  32.4 0.0 copy-done.4
  32.4 0.8 %rows.1 = f32[4,16,128]{2,1,0:T(8,128)S(1)} custom-call(f32[128,128]{1,0:T(8,128)S(1)} %get-tuple-element.12.mine, f32[128,128]{1,0:T(8,128)S(1)} %collective-permute-done.4.theirs, bf16[2,2,128]{2,1,0:T(2,128)(2,1)S(1)} %copy-done, bf16[2,2,128]{2,1,0:T(2,128)(2,1)S(1)} %copy-done.1, bf16[2,2,128]{2,1,0:T(2,128)(2,1)S(1)} %copy-done.2, ...), custom_call_target="tpu_custom_call" | custom-call | tf_op jit(solution)/shard_map/rows/pallas_call | solution.py:437
  33.2 9.5 %all_to_all.5.got = f32[4,16,128]{2,1,0:T(8,128)S(1)} all-to-all(f32[4,16,128]{2,1,0:T(8,128)S(1)} %rows.1), channel_id=1, replica_groups=mesh['gr'=2,'sp_0'=4,'sp_1'=4,'tp'=8] {'sp_1'}, dimensions={0} | all-to-all | bytes 65536 | tf_op jit(solution)/shard_map/all_to_all | solution.py:454
  42.7 0.6 %finish.1 = (bf16[2,2,8,128]{3,2,1,0:T(8,128)(2,1)}, bf16[2,2,128]{2,1,0:T(2,128)(2,1)}) custom-call(f32[4,16,128]{2,1,0:T(8,128)S(1)} %all_to_all.5.got), custom_call_target="tpu_custom_call" | custom-call | tf_op jit(solution)/shard_map/finish/pallas_call | solution.py:455
  (2 shorter events, 0.0 us)
Async XLA Ops:
  0.6 25.8 %copy-start.1 = (bf16[2,2,128]{2,1,0:T(2,128)(2,1)S(1)}, bf16[2,2,128]{2,1,0:T(2,128)(2,1)}, u32[]{:S(2)}) copy-start(bf16[2,2,128]{2,1,0:T(2,128)(2,1)} %key_ref.3) | copy-start | bytes 3076
  0.6 25.8 %copy-start = (bf16[2,2,128]{2,1,0:T(2,128)(2,1)S(1)}, bf16[2,2,128]{2,1,0:T(2,128)(2,1)}, u32[]{:S(2)}) copy-start(bf16[2,2,128]{2,1,0:T(2,128)(2,1)} %query_ref.3) | copy-start | bytes 3076
  0.7 31.7 %copy-start.4 = (f32[128]{0:T(128)S(1)}, f32[128]{0:T(128)}, u32[]{:S(2)}) copy-start(f32[128]{0:T(128)} %param.25) | copy-start | bytes 1540
  0.7 31.7 %copy-start.3 = (f32[2,2]{1,0:T(2,128)S(1)}, f32[2,2]{1,0:T(2,128)}, u32[]{:S(2)}) copy-start(f32[2,2]{1,0:T(2,128)} %gate_ref.1) | copy-start | bytes 52
  0.7 31.7 %copy-start.2 = (bf16[2,2,128]{2,1,0:T(2,128)(2,1)S(1)}, bf16[2,2,128]{2,1,0:T(2,128)(2,1)}, u32[]{:S(2)}) copy-start(bf16[2,2,128]{2,1,0:T(2,128)(2,1)} %value_ref.1) | copy-start | bytes 3076
  10.2 7.5 %collective-permute-start = (f32[256,128]{1,0:T(8,128)S(1)}, f32[256,128]{1,0:T(8,128)S(1)}, u32[]{:S(2)}, u32[]{:S(2)}) collective-permute-start(f32[256,128]{1,0:T(8,128)S(1)} %get-tuple-element.9), channel_id=1, source_target_pairs={{0,16},{8,24},{16,0},{24,8},{1,17},{9,25},{17,1},{25,9},{2,18},{10... | collective-permute-start | bytes 393224 | tf_op jit(solution)/shard_map/ppermute | solution.py:347
  13.5 6.7 %collective-permute-start.1 = (f32[256,128]{1,0:T(8,128)S(1)}, f32[256,128]{1,0:T(8,128)S(1)}, u32[]{:S(2)}, u32[]{:S(2)}) collective-permute-start(f32[256,128]{1,0:T(8,128)S(1)} %get-tuple-element.10), channel_id=1, source_target_pairs={{0,24},{8,0},{16,8},{24,16},{1,25},{9,1},{17,9},{25,17},{2,26},{10... | collective-permute-start | bytes 393224 | tf_op jit(solution)/shard_map/ppermute | solution.py:347
  14.5 6.2 %collective-permute-start.2 = (f32[256,128]{1,0:T(8,128)S(1)}, f32[256,128]{1,0:T(8,128)S(1)}, u32[]{:S(2)}, u32[]{:S(2)}) collective-permute-start(f32[256,128]{1,0:T(8,128)S(1)} %get-tuple-element.11), channel_id=1, source_target_pairs={{0,8},{8,16},{16,24},{24,0},{1,9},{9,17},{17,25},{25,1},{2,10},{10... | collective-permute-start | bytes 393224 | tf_op jit(solution)/shard_map/ppermute | solution.py:347
  21.4 5.1 %collective-permute-start.3 = (f32[256,128]{1,0:T(8,128)S(1)}, f32[256,128]{1,0:T(8,128)S(1)}, u32[]{:S(2)}, u32[]{:S(2)}) collective-permute-start(f32[256,128]{1,0:T(8,128)S(1)} %segments.1.own), channel_id=1, source_target_pairs={{0,32},{32,0},{64,96},{96,64},{1,33},{33,1},{65,97},{97,65},{2,34}... | collective-permute-start | bytes 393224 | tf_op jit(solution)/shard_map/ppermute | solution.py:353
  26.7 5.7 %collective-permute-start.4 = (f32[128,128]{1,0:T(8,128)S(1)}, f32[128,128]{1,0:T(8,128)S(1)}, u32[]{:S(2)}, u32[]{:S(2)}) collective-permute-start(f32[128,128]{1,0:T(8,128)S(1)} %get-tuple-element.13), channel_id=1, source_target_pairs={{0,64},{32,96},{64,0},{96,32},{1,65},{33,97},{65,1},{97,33},{2,66}... | collective-permute-start | bytes 196616 | tf_op jit(solution)/shard_map/ppermute | solution.py:353

commit v5 on v4

--- a/solution.py
+++ b/solution.py
@@ -74,7 +74,13 @@
             for m in m_mats
         ]
         t_rows = [gather(lambda r: i[r, :]) for i in invs]
-        ys = [dot1(m, i).astype(BF16) for m, i in zip(m_rows, invs)]
+        uppers = []
+        for i in invs:
+            pieces = []
+            for r in lower:
+                pieces += [i[r.start - b : r.start, :].astype(BF16), jnp.zeros((b, CH), BF16)]
+            uppers.append(jnp.concatenate(pieces, axis=0))
+        ys = [dot1(m, i).astype(BF16) for m, i in zip(m_rows, uppers)]
         spread_out = []
         for y in ys:
             pieces = []
@@ -105,38 +111,31 @@
     xbuf, wkbuf, wvbuf, gatew, extra, bias_ref, rate_ref, kbuf, vbuf, state, sems,
 ):
     tiles, tile, width = xbuf.shape
+    half = tile // 2
     first_head = lax.axis_index("tp") * 2
     here = lax.axis_index("sp_1")
     per_seq = kbuf.shape[0] // (2 * CH)
     heads = gate_hbm.shape[0]
-
-    def x_copy(t):
-        s, part = divmod(t, tiles // 2)
-        rows = pl.ds(part * tile, tile)
-        return pltpu.make_async_copy(x_hbm.at[s, rows], xbuf.at[t], sems.at[t])
-
-    others = [
-        pltpu.make_async_copy(src, dst, sems.at[tiles + i])
-        for i, (src, dst) in enumerate(
-            (
-                (gate_hbm, gatew.at[pl.ds(0, heads)]),
-                (decay_hbm, gatew.at[pl.ds(heads, heads)]),
-                (wk_hbm, wkbuf),
-                (wv_hbm, wvbuf),
-                (bias_hbm, bias_ref),
-                (rate_hbm, rate_ref),
-                (extra_hbm, extra),
-            )
-        )
+    moves = [
+        (gate_hbm, gatew.at[pl.ds(0, heads)]),
+        (decay_hbm, gatew.at[pl.ds(heads, heads)]),
+        (bias_hbm, bias_ref),
+        (rate_hbm, rate_ref),
+        (extra_hbm, extra),
     ]
-    for c in others[4:] + others[:3]:
+    small = len(moves)
+    for t in range(tiles):
+        for i in range(2):
+            rows = pl.ds(i * half, half)
+            moves.append((x_hbm.at[t, rows], xbuf.at[t, rows]))
+            if t == 0:
+                moves.append(((wk_hbm, wkbuf), (wv_hbm, wvbuf))[i])
+    copies = [pltpu.make_async_copy(src, dst, sems.at[i]) for i, (src, dst) in enumerate(moves)]
+    for c in copies:
         c.start()
-    x_copy(0).start()
-    others[3].start()
-    for t in range(1, tiles):
-        x_copy(t).start()
-    for c in others[4:] + others[:3]:
+    for c in copies[:small]:
         c.wait()
+    arrivals = copies[small:]
     pick = iota((heads, tile), 0)
     odd = iota((2, tile), 0) == 1
     bias = jnp.where(odd, bias_ref[first_head + 1], bias_ref[first_head])
@@ -146,14 +145,9 @@
     eye = jnp.where(row == col, 1.0, 0.0)
     upto = jnp.where(row <= col, 1.0, 0.0).astype(BF16)
 
-    def halves(t, weights, dims, count):
-        size = tile // count
-        return [
-            lax.dot_general(
-                xbuf[t, i * size : (i + 1) * size], weights[...], dims, preferred_element_type=F32
-            )
-            for i in range(count)
-        ]
+    def times(t, i, weights, dims=AB):
+        x = xbuf[t, i * half : (i + 1) * half]
+        return lax.dot_general(x, weights[...], dims, preferred_element_type=F32)
 
     def scalars(t, gt):
         picked = [
@@ -205,23 +199,46 @@
         start = (s * per_seq + n) * CH
         return buf[start : start + CH, h * CH : (h + 1) * CH]
 
-    rows_of = []
-    ms = []
-    for t in range(tiles):
-        x_copy(t).wait()
-        gt = jnp.concatenate([jnp.transpose(g) for g in halves(t, gatew, ABT, 2)], axis=1)
-        count = 2
-        size = tile // count
-        kps = halves(t, wkbuf, AB, count)
-        if t == 0:
-            others[3].wait()
-        vps = halves(t, wvbuf, AB, count)
-        rows_of.append(scalars(t, gt))
-        for i in range(count):
-            weighted(t, kps[i], slice(t * tile + i * size, t * tile + (i + 1) * size))
-        ms += matrices(t, rows_of[t][1], rows_of[t][4])
-        for i in range(count):
-            vbuf[t * tile + i * size : t * tile + (i + 1) * size, :] = silu(vps[i]).astype(BF16)
+    def keys(t, i, kp):
+        weighted(t, kp, slice(t * tile + i * half, t * tile + (i + 1) * half))
+
+    def values(t, i, vp):
+        vbuf[t * tile + i * half : t * tile + (i + 1) * half, :] = silu(vp).astype(BF16)
+
+    def rows_from(t, gts):
+        return scalars(t, jnp.concatenate([jnp.transpose(g) for g in gts], axis=1))
+
+    x00, wk, x01, wv, x10, x11 = arrivals
+    x00.wait()
+    wk.wait()
+    g00 = times(0, 0, gatew, ABT)
+    k00 = times(0, 0, wkbuf)
+    x01.wait()
+    g01 = times(0, 1, gatew, ABT)
+    k01 = times(0, 1, wkbuf)
+    keys(0, 0, k00)
+    wv.wait()
+    v00 = times(0, 0, wvbuf)
+    v01 = times(0, 1, wvbuf)
+    keys(0, 1, k01)
+    x10.wait()
+    x11.wait()
+    g10 = times(1, 0, gatew, ABT)
+    k10 = times(1, 0, wkbuf)
+    rows_of = [rows_from(0, (g00, g01))]
+    g11 = times(1, 1, gatew, ABT)
+    k11 = times(1, 1, wkbuf)
+    values(0, 0, v00)
+    values(0, 1, v01)
+    rows_of.append(rows_from(1, (g10, g11)))
+    keys(1, 0, k10)
+    v10 = times(1, 0, wvbuf)
+    v11 = times(1, 1, wvbuf)
+    ms = matrices(0, rows_of[0][1], rows_of[0][4])
+    keys(1, 1, k11)
+    ms += matrices(1, rows_of[1][1], rows_of[1][4])
+    values(1, 0, v10)
+    values(1, 1, v11)
 
     items = [(s, n, h) for s in range(2) for n in range(per_seq) for h in range(2)]
     invs = inverses_of(ms)
@@ -392,7 +409,7 @@
             pltpu.VMEM((seqs * seg, cols), BF16),
             pltpu.VMEM((seqs * seg, cols), BF16),
             pltpu.VMEM((4, 2 * CH, CH), F32),
-            pltpu.SemaphoreType.DMA((tiles + 7,)),
+            pltpu.SemaphoreType.DMA((11,)),
         ],
         compiler_params=pltpu.CompilerParams(vmem_limit_bytes=24 * 2**20),
         name="maps",

time: 43.4 us -> 42.9 us (0.988)
  Pallas kernels: 11.9 us -> 11.4 us
    pallas_call x1, Pallas kernels: 9.5 us -> 9.01 us  [shards(): pl.pallas_call(maps_kernel, out_shape=[jax.ShapeDtypeStruct((2 * CH, CH),...]
where the time goes in v5:
time: 42.9 us; the launch traced here: 42.7 us
  Pallas kernels  11.4 us (27%)
  starting transfers between devices  10.7 us (25%)
  waiting for transfers between devices  10.5 us (24%)
  blocking collectives  9.44 us (22%)
  between operations  0.71 us (2%)
    all_to_all x1, blocking collectives, shards(): got = lax.all_to_all(rows, 'sp_1', 0, 0, tiled=True)  9.44 us
    pallas_call x1, Pallas kernels, shards(): pl.pallas_call(maps_kernel, out_shape=[jax.ShapeDtypeStruct((2 * CH, CH),...  9.01 us
    ppermute x2, starting transfers between devices, swap(): return lax.ppermute(array, axis, [(i, i ^ bit) for i in range(4)])  5.41 us
    ppermute x3, starting transfers between devices, spread(): lax.ppermute(a, axis, [(i, (i + k) % 4) for i in range(4)])  5.31 us
    ppermute x2, waiting for transfers between devices, swap(): return lax.ppermute(array, axis, [(i, i ^ bit) for i in range(4)])  5.3 us
    ppermute x3, waiting for transfers between devices, spread(): lax.ppermute(a, axis, [(i, (i + k) % 4) for i in range(4)])  5.21 us
  transfers between devices with their start and end apart: 5, of which 5 were waited for; matrix products, arithmetic and copies ran while one was open for 0% of the time, Pallas kernels for 0%

profile of v5, /device:TPU:2, one launch (start us, length us, event | category | flops | bytes accessed | tf_op | source)
XLA Modules:
  0.0 42.7 jit_solution(13356799697934668040)
XLA Ops:
  0.6 0.0 copy-start.1
  0.6 0.0 copy-start
  0.7 0.0 copy-start.4
  0.7 0.0 copy-start.3
  0.7 0.0 copy-start.2
  0.7 9.0 %maps.1 = (f32[256,128]{1,0:T(8,128)S(1)}, f32[256,128]{1,0:T(8,128)S(1)}, f32[256,128]{1,0:T(8,128)S(1)}, f32[256,128]{1,0:T(8,128)S(1)}) custom-call(bf16[2,512,2048]{2,1,0:T(8,128)(2,1)} %x_hbm.1, bf16[2048,256]{1,0:T(8,128)(2,1)} %wk_hbm.1, bf16[2048,256]{1,0:T(8,128)(2,1)} %wv_hbm.1, bf16[16,2048]{1,0:T(8,128)(2,1)} %bitcast.7, ...), custom_call_target="tpu_custom_call" | custom-call | tf_op jit(solution)/shard_map/maps/pallas_call | solution.py:396
  9.7 3.3 %collective-permute-start = (f32[256,128]{1,0:T(8,128)S(1)}, f32[256,128]{1,0:T(8,128)S(1)}, u32[]{:S(2)}, u32[]{:S(2)}) collective-permute-start(f32[256,128]{1,0:T(8,128)S(1)} %get-tuple-element.9), channel_id=1, source_target_pairs={{0,16},{8,24},{16,0},{24,8},{1,17},{9,25},{17,1},{25,9},{2,18},{10... | collective-permute-start | bytes 393224 | tf_op jit(solution)/shard_map/ppermute | solution.py:364
  13.0 1.1 %collective-permute-start.1 = (f32[256,128]{1,0:T(8,128)S(1)}, f32[256,128]{1,0:T(8,128)S(1)}, u32[]{:S(2)}, u32[]{:S(2)}) collective-permute-start(f32[256,128]{1,0:T(8,128)S(1)} %get-tuple-element.10), channel_id=1, source_target_pairs={{0,24},{8,0},{16,8},{24,16},{1,25},{9,1},{17,9},{25,17},{2,26},{10... | collective-permute-start | bytes 393224 | tf_op jit(solution)/shard_map/ppermute | solution.py:364
  14.0 1.0 %collective-permute-start.2 = (f32[256,128]{1,0:T(8,128)S(1)}, f32[256,128]{1,0:T(8,128)S(1)}, u32[]{:S(2)}, u32[]{:S(2)}) collective-permute-start(f32[256,128]{1,0:T(8,128)S(1)} %get-tuple-element.11), channel_id=1, source_target_pairs={{0,8},{8,16},{16,24},{24,0},{1,9},{9,17},{17,25},{25,1},{2,10},{10... | collective-permute-start | bytes 393224 | tf_op jit(solution)/shard_map/ppermute | solution.py:364
  15.0 2.2 %collective-permute-done.r1 = f32[256,128]{1,0:T(8,128)S(1)} collective-permute-done((f32[256,128]{1,0:T(8,128)S(1)}, f32[256,128]{1,0:T(8,128)S(1)}, u32[]{:S(2)}, u32[]{:S(2)}) %collective-permute-start) | collective-permute-done | bytes 131104 | tf_op jit(solution)/shard_map/ppermute | solution.py:364
  17.2 2.5 %collective-permute-done.1.r2 = f32[256,128]{1,0:T(8,128)S(1)} collective-permute-done((f32[256,128]{1,0:T(8,128)S(1)}, f32[256,128]{1,0:T(8,128)S(1)}, u32[]{:S(2)}, u32[]{:S(2)}) %collective-permute-start.1) | collective-permute-done | bytes 131104 | tf_op jit(solution)/shard_map/ppermute | solution.py:364
  19.7 0.5 %collective-permute-done.2.r3 = f32[256,128]{1,0:T(8,128)S(1)} collective-permute-done((f32[256,128]{1,0:T(8,128)S(1)}, f32[256,128]{1,0:T(8,128)S(1)}, u32[]{:S(2)}, u32[]{:S(2)}) %collective-permute-start.2) | collective-permute-done | bytes 131104 | tf_op jit(solution)/shard_map/ppermute | solution.py:364
  20.2 0.7 %segments.1.own = f32[256,128]{1,0:T(8,128)S(1)} custom-call(f32[256,128]{1,0:T(8,128)S(1)} %get-tuple-element.8.r0, f32[256,128]{1,0:T(8,128)S(1)} %collective-permute-done.r1, f32[256,128]{1,0:T(8,128)S(1)} %collective-permute-done.1.r2, f32[256,128]{1,0:T(8,128)S(1)} %collective-permute-done.2.r3), custom_call_target="tpu_custom_call" | custom-call | tf_op jit(solution)/shard_map/segments/pallas_call | solution.py:432
  20.9 2.0 %collective-permute-start.3 = (f32[256,128]{1,0:T(8,128)S(1)}, f32[256,128]{1,0:T(8,128)S(1)}, u32[]{:S(2)}, u32[]{:S(2)}) collective-permute-start(f32[256,128]{1,0:T(8,128)S(1)} %segments.1.own), channel_id=1, source_target_pairs={{0,32},{32,0},{64,96},{96,64},{1,33},{33,1},{65,97},{97,65},{2,34}... | collective-permute-start | bytes 393224 | tf_op jit(solution)/shard_map/ppermute | solution.py:370
  22.9 3.1 %collective-permute-done.3.other = f32[256,128]{1,0:T(8,128)S(1)} collective-permute-done((f32[256,128]{1,0:T(8,128)S(1)}, f32[256,128]{1,0:T(8,128)S(1)}, u32[]{:S(2)}, u32[]{:S(2)}) %collective-permute-start.3) | collective-permute-done | bytes 131104 | tf_op jit(solution)/shard_map/ppermute | solution.py:370
  26.0 0.0 copy-done.1
  26.0 0.0 copy-done
  26.0 0.2 halves.1
  26.2 3.4 %collective-permute-start.4 = (f32[128,128]{1,0:T(8,128)S(1)}, f32[128,128]{1,0:T(8,128)S(1)}, u32[]{:S(2)}, u32[]{:S(2)}) collective-permute-start(f32[128,128]{1,0:T(8,128)S(1)} %get-tuple-element.13), channel_id=1, source_target_pairs={{0,64},{32,96},{64,0},{96,32},{1,65},{33,97},{65,1},{97,33},{2,66}... | collective-permute-start | bytes 196616 | tf_op jit(solution)/shard_map/ppermute | solution.py:370
  29.6 2.2 %collective-permute-done.4.theirs = f32[128,128]{1,0:T(8,128)S(1)} collective-permute-done((f32[128,128]{1,0:T(8,128)S(1)}, f32[128,128]{1,0:T(8,128)S(1)}, u32[]{:S(2)}, u32[]{:S(2)}) %collective-permute-start.4) | collective-permute-done | bytes 65568 | tf_op jit(solution)/shard_map/ppermute | solution.py:370
  31.9 0.0 copy-done.4
  31.9 0.8 %rows.1 = f32[4,16,128]{2,1,0:T(8,128)S(1)} custom-call(f32[128,128]{1,0:T(8,128)S(1)} %get-tuple-element.12.mine, f32[128,128]{1,0:T(8,128)S(1)} %collective-permute-done.4.theirs, bf16[2,2,128]{2,1,0:T(2,128)(2,1)S(1)} %copy-done, bf16[2,2,128]{2,1,0:T(2,128)(2,1)S(1)} %copy-done.1, bf16[2,2,128]{2,1,0:T(2,128)(2,1)S(1)} %copy-done.2, ...), custom_call_target="tpu_custom_call" | custom-call | tf_op jit(solution)/shard_map/rows/pallas_call | solution.py:454
  32.7 9.4 %all_to_all.5.got = f32[4,16,128]{2,1,0:T(8,128)S(1)} all-to-all(f32[4,16,128]{2,1,0:T(8,128)S(1)} %rows.1), channel_id=1, replica_groups=mesh['gr'=2,'sp_0'=4,'sp_1'=4,'tp'=8] {'sp_1'}, dimensions={0} | all-to-all | bytes 65536 | tf_op jit(solution)/shard_map/all_to_all | solution.py:471
  42.1 0.6 %finish.1 = (bf16[2,2,8,128]{3,2,1,0:T(8,128)(2,1)}, bf16[2,2,128]{2,1,0:T(2,128)(2,1)}) custom-call(f32[4,16,128]{2,1,0:T(8,128)S(1)} %all_to_all.5.got), custom_call_target="tpu_custom_call" | custom-call | tf_op jit(solution)/shard_map/finish/pallas_call | solution.py:472
  (2 shorter events, 0.0 us)
Async XLA Ops:
  0.6 25.3 %copy-start.1 = (bf16[2,2,128]{2,1,0:T(2,128)(2,1)S(1)}, bf16[2,2,128]{2,1,0:T(2,128)(2,1)}, u32[]{:S(2)}) copy-start(bf16[2,2,128]{2,1,0:T(2,128)(2,1)} %key_ref.3) | copy-start | bytes 3076
  0.6 25.3 %copy-start = (bf16[2,2,128]{2,1,0:T(2,128)(2,1)S(1)}, bf16[2,2,128]{2,1,0:T(2,128)(2,1)}, u32[]{:S(2)}) copy-start(bf16[2,2,128]{2,1,0:T(2,128)(2,1)} %query_ref.3) | copy-start | bytes 3076
  0.7 31.2 %copy-start.4 = (f32[128]{0:T(128)S(1)}, f32[128]{0:T(128)}, u32[]{:S(2)}) copy-start(f32[128]{0:T(128)} %param.25) | copy-start | bytes 1540
  0.7 31.2 %copy-start.3 = (f32[2,2]{1,0:T(2,128)S(1)}, f32[2,2]{1,0:T(2,128)}, u32[]{:S(2)}) copy-start(f32[2,2]{1,0:T(2,128)} %gate_ref.1) | copy-start | bytes 52
  0.7 31.2 %copy-start.2 = (bf16[2,2,128]{2,1,0:T(2,128)(2,1)S(1)}, bf16[2,2,128]{2,1,0:T(2,128)(2,1)}, u32[]{:S(2)}) copy-start(bf16[2,2,128]{2,1,0:T(2,128)(2,1)} %value_ref.1) | copy-start | bytes 3076
  9.7 7.5 %collective-permute-start = (f32[256,128]{1,0:T(8,128)S(1)}, f32[256,128]{1,0:T(8,128)S(1)}, u32[]{:S(2)}, u32[]{:S(2)}) collective-permute-start(f32[256,128]{1,0:T(8,128)S(1)} %get-tuple-element.9), channel_id=1, source_target_pairs={{0,16},{8,24},{16,0},{24,8},{1,17},{9,25},{17,1},{25,9},{2,18},{10... | collective-permute-start | bytes 393224 | tf_op jit(solution)/shard_map/ppermute | solution.py:364
  13.0 6.7 %collective-permute-start.1 = (f32[256,128]{1,0:T(8,128)S(1)}, f32[256,128]{1,0:T(8,128)S(1)}, u32[]{:S(2)}, u32[]{:S(2)}) collective-permute-start(f32[256,128]{1,0:T(8,128)S(1)} %get-tuple-element.10), channel_id=1, source_target_pairs={{0,24},{8,0},{16,8},{24,16},{1,25},{9,1},{17,9},{25,17},{2,26},{10... | collective-permute-start | bytes 393224 | tf_op jit(solution)/shard_map/ppermute | solution.py:364
  14.0 6.2 %collective-permute-start.2 = (f32[256,128]{1,0:T(8,128)S(1)}, f32[256,128]{1,0:T(8,128)S(1)}, u32[]{:S(2)}, u32[]{:S(2)}) collective-permute-start(f32[256,128]{1,0:T(8,128)S(1)} %get-tuple-element.11), channel_id=1, source_target_pairs={{0,8},{8,16},{16,24},{24,0},{1,9},{9,17},{17,25},{25,1},{2,10},{10... | collective-permute-start | bytes 393224 | tf_op jit(solution)/shard_map/ppermute | solution.py:364
  20.9 5.1 %collective-permute-start.3 = (f32[256,128]{1,0:T(8,128)S(1)}, f32[256,128]{1,0:T(8,128)S(1)}, u32[]{:S(2)}, u32[]{:S(2)}) collective-permute-start(f32[256,128]{1,0:T(8,128)S(1)} %segments.1.own), channel_id=1, source_target_pairs={{0,32},{32,0},{64,96},{96,64},{1,33},{33,1},{65,97},{97,65},{2,34}... | collective-permute-start | bytes 393224 | tf_op jit(solution)/shard_map/ppermute | solution.py:370
  26.2 5.6 %collective-permute-start.4 = (f32[128,128]{1,0:T(8,128)S(1)}, f32[128,128]{1,0:T(8,128)S(1)}, u32[]{:S(2)}, u32[]{:S(2)}) collective-permute-start(f32[128,128]{1,0:T(8,128)S(1)} %get-tuple-element.13), channel_id=1, source_target_pairs={{0,64},{32,96},{64,0},{96,32},{1,65},{33,97},{65,1},{97,33},{2,66}... | collective-permute-start | bytes 196616 | tf_op jit(solution)/shard_map/ppermute | solution.py:370

commit v6 on v5

--- a/solution.py
+++ b/solution.py
@@ -275,16 +275,19 @@
         o[...] = state[lax.rem(here + k, 4)]
 
 
+def after(first, second):
+    both = dot3(second[0], jnp.concatenate(first, axis=1))
+    return both[:, :CH], both[:, CH:] + second[1]
+
+
 def segments_kernel(r0, r1, r2, r3, out, scr):
     here = lax.axis_index("sp_1")
     for k, ref in zip(SHIFTS, (r0, r1, r2, r3)):
         scr[lax.rem(here + 4 - k, 4)] = ref[...]
-    state = jnp.concatenate([scr[0, :CH, :], scr[0, CH:, :]], axis=1)
-    for t in range(1, 4):
-        state = dot3(scr[t, :CH, :], state)
-        state = state + jnp.concatenate([jnp.zeros((CH, CH), F32), scr[t, CH:, :]], axis=1)
-    out[:CH, :] = state[:, :CH]
-    out[CH:, :] = state[:, CH:]
+    maps = [(scr[t, :CH, :], scr[t, CH:, :]) for t in range(4)]
+    while len(maps) > 1:
+        maps = [after(maps[i], maps[i + 1]) for i in range(0, len(maps), 2)]
+    out[:CH, :], out[CH:, :] = maps[0]
 
 
 def row_of(ref, s, h):
@@ -292,21 +295,30 @@
     return jnp.sum(jnp.where(iota(two.shape, 0) == h, two, 0.0), axis=0, keepdims=True)
 
 
-def new_token(query_ref, key_ref):
+def token_kernel(query_ref, key_ref, value_ref, gate_ref, out):
+    part = lax.axis_index("sp_0")
     pair = lax.axis_index("sp_1")
     s, h = lax.div(pair, 2), lax.rem(pair, 2)
-    return s, h, unit_rows(row_of(query_ref, s, h)), unit_rows(row_of(key_ref, s, h))
-
-
-def halves_kernel(own, other, query_ref, key_ref, mine, theirs, scr, amap, gain):
+    kn = unit_rows(row_of(key_ref, s, h))
+    qn = unit_rows(row_of(query_ref, s, h))
+    bn = 1.0 / (1.0 + jnp.exp(-jnp.full((1, CH), gate_ref[s, h], F32)))
+    meet = jnp.sum(kn * qn, axis=1, keepdims=True)
+    out[:8, :] = jnp.concatenate(
+        [kn, qn, row_of(value_ref, s, h), bn, bn * meet, jnp.zeros((3, CH), F32)], axis=0
+    )
+    diagonal = iota((ROWS, CH), 1) == iota((ROWS, CH), 0) + part * ROWS
+    k_col = jnp.sum(jnp.where(diagonal, jnp.broadcast_to(kn, (ROWS, CH)), 0.0), axis=1, keepdims=True)
+    out[8:, :] = bn * k_col
+
+
+def halves_kernel(own, other, token, mine, theirs, scr, amap, gain):
     part = lax.axis_index("sp_0")
     odd = lax.rem(part, 2)
     scr[odd] = own[...]
     scr[1 - odd] = other[...]
-    _, _, qn, kn = new_token(query_ref, key_ref)
-    both = dot3(scr[1, :CH, :], jnp.concatenate([scr[0, :CH, :], scr[0, CH:, :]], axis=1))
-    amap[...] = both[:, :CH]
-    gain[...] = both[:, CH:] + scr[1, CH:, :]
+    amap[...], gain[...] = after(
+        (scr[0, :CH, :], scr[0, CH:, :]), (scr[1, :CH, :], scr[1, CH:, :])
+    )
 
     @pl.when(part < 2)
     def _():
@@ -315,8 +327,7 @@
 
     @pl.when(part >= 2)
     def _():
-        reads = jnp.concatenate([kn, qn, jnp.zeros((6, CH), F32)], axis=0)
-        through = dot3(reads, jnp.concatenate([amap[...], gain[...]], axis=1))
+        through = dot3(token[:8, :], jnp.concatenate([amap[...], gain[...]], axis=1))
         for ref, owner in ((mine, part), (theirs, part - 2)):
             rows = pl.ds(pl.multiple_of(owner * ROWS, ROWS), ROWS)
             ref[:ROWS, :] = amap[rows, :]
@@ -326,33 +337,29 @@
             ref[2 * ROWS + 16 :, :] = jnp.zeros((CH - 2 * ROWS - 16, CH), F32)
 
 
-def rows_kernel(mine, theirs, query_ref, key_ref, value_ref, gate_ref, gain_ref, out, scr):
-    part = lax.axis_index("sp_0")
-    right = jnp.where(part < 2, 0, 1)
+def rows_kernel(mine, theirs, token, gain_ref, o0, o1, o2, o3, scr, wide):
+    right = jnp.where(lax.axis_index("sp_0") < 2, 0, 1)
     scr[right] = mine[...]
     scr[1 - right] = theirs[...]
-    s, h, qn, kn = new_token(query_ref, key_ref)
-    vn = row_of(value_ref, s, h)
-    bn = 1.0 / (1.0 + jnp.exp(-jnp.full((1, CH), gate_ref[s, h], F32)))
-    meet = jnp.sum(kn * qn, axis=1, keepdims=True)
-    diagonal = iota((ROWS, CH), 1) == iota((ROWS, CH), 0) + part * ROWS
-    k_col = jnp.sum(jnp.where(diagonal, jnp.broadcast_to(kn, (ROWS, CH)), 0.0), axis=1, keepdims=True)
     final = dot3(scr[1, : ROWS + 8, :], scr[0]) + scr[1, ROWS + 8 : 2 * ROWS + 16, :]
-    missing = vn - final[ROWS : ROWS + 1, :]
-    state = final[:ROWS, :] + k_col * (bn * missing)
-    read = (final[ROWS + 1 : ROWS + 2, :] + bn * meet * missing) / math.sqrt(CH)
+    missing = token[2:3, :] - final[ROWS : ROWS + 1, :]
+    wide[:ROWS, :] = final[:ROWS, :] + token[8:, :] * missing
+    read = (final[ROWS + 1 : ROWS + 2, :] + token[4:5, :] * missing) / math.sqrt(CH)
     scale = lax.rsqrt(jnp.mean(read * read, axis=-1, keepdims=True) + 1e-06)
     read_rows = jnp.broadcast_to(read * scale * gain_ref[...], (8, CH))
-    for y in range(4):
-        out[y, :8, :] = state[8 * y : 8 * y + 8, :]
-        out[y, 8:, :] = read_rows
-
-
-def finish_kernel(got, cache_ref, read_ref):
+    for k, o in zip(SHIFTS, (o0, o1, o2, o3)):
+        y = lax.rem(lax.axis_index("sp_1") + k, 4)
+        o[:8, :] = wide[pl.ds(pl.multiple_of(y * 8, 8), 8), :]
+        o[8:, :] = read_rows
+
+
+def finish_kernel(r0, r1, r2, r3, cache_ref, read_ref, scr):
+    for k, ref in zip(SHIFTS, (r0, r1, r2, r3)):
+        scr[lax.rem(lax.axis_index("sp_1") + 4 - k, 4)] = ref[...]
     for s in range(2):
         for h in range(2):
-            cache_ref[s, h] = got[2 * s + h, :8, :].astype(BF16)
-        read_ref[s] = jnp.concatenate([got[2 * s + h, 8:9, :] for h in range(2)], axis=0).astype(BF16)
+            cache_ref[s, h] = scr[2 * s + h, :8, :].astype(BF16)
+        read_ref[s] = jnp.concatenate([scr[2 * s + h, 8:9, :] for h in range(2)], axis=0).astype(BF16)
 
 
 def vmem(count):
@@ -438,10 +445,18 @@
         compiler_params=small,
         name="segments",
     )(*spread(maps, "sp_1"))
+    token = pl.pallas_call(
+        token_kernel,
+        out_shape=jax.ShapeDtypeStruct((8 + ROWS, CH), F32),
+        in_specs=[*vmem(3), smem],
+        out_specs=vmem(1)[0],
+        compiler_params=small,
+        name="token",
+    )(next_token_query, next_token_key, next_token_value, next_token_gate)
     mine, theirs = pl.pallas_call(
         halves_kernel,
         out_shape=[jax.ShapeDtypeStruct((CH, CH), F32)] * 2,
-        in_specs=vmem(4),
+        in_specs=vmem(3),
         out_specs=vmem(2),
         scratch_shapes=[
             pltpu.VMEM((2, 2 * CH, CH), F32),
@@ -450,36 +465,28 @@
         ],
         compiler_params=small,
         name="halves",
-    )(segment, swap(segment, "sp_0", 1), next_token_query, next_token_key)
+    )(segment, swap(segment, "sp_0", 1), token)
     rows = pl.pallas_call(
         rows_kernel,
-        out_shape=jax.ShapeDtypeStruct((4, 16, CH), F32),
-        in_specs=[*vmem(5), smem, *vmem(1)],
-        out_specs=vmem(1)[0],
-        scratch_shapes=[pltpu.VMEM((2, CH, CH), F32)],
+        out_shape=[jax.ShapeDtypeStruct((16, CH), F32)] * 4,
+        in_specs=vmem(4),
+        out_specs=vmem(4),
+        scratch_shapes=[pltpu.VMEM((2, CH, CH), F32), pltpu.VMEM((ROWS, CH), F32)],
         compiler_params=small,
         name="rows",
-    )(
-        mine,
-        swap(theirs, "sp_0", 2),
-        next_token_query,
-        next_token_key,
-        next_token_value,
-        next_token_gate,
-        readout_norm_gain.reshape(1, CH),
-    )
-    got = lax.all_to_all(rows, "sp_1", 0, 0, tiled=True)
+    )(mine, swap(theirs, "sp_0", 2), token, readout_norm_gain.reshape(1, CH))
     return pl.pallas_call(
         finish_kernel,
         out_shape=[
             jax.ShapeDtypeStruct((2, 2, 8, CH), BF16),
             jax.ShapeDtypeStruct((2, 2, CH), BF16),
         ],
-        in_specs=vmem(1),
+        in_specs=vmem(4),
         out_specs=vmem(2),
+        scratch_shapes=[pltpu.VMEM((4, 16, CH), F32)],
         compiler_params=small,
         name="finish",
-    )(got)
+    )(*spread(rows, "sp_1"))
 
 
 def solution(mesh):

time: 42.9 us -> 41.8 us (0.974)
  blocking collectives: 9.44 us -> 0 us
  starting transfers between devices: 10.7 us -> 15.6 us
  waiting for transfers between devices: 10.5 us -> 14 us
    all_to_all x1 -> x0, blocking collectives: 9.44 us -> none  [shards(): got = lax.all_to_all(rows, 'sp_1', 0, 0, tiled=True)]
    ppermute x3 -> x6, starting transfers between devices: 5.31 us -> 10.2 us  [spread(): lax.ppermute(a, axis, [(i, (i + k) % 4) for i in range(4)])]
    ppermute x3 -> x6, waiting for transfers between devices: 5.21 us -> 9.44 us  [spread(): lax.ppermute(a, axis, [(i, (i + k) % 4) for i in range(4)])]
    ppermute x2, waiting for transfers between devices: 5.3 us -> 4.55 us  [swap(): return lax.ppermute(array, axis, [(i, i ^ bit) for i in range(4)])]
    pallas_call x1 -> x2, Pallas kernels: 0.83 us -> 1 us  [the longest x1 0.73 us: shards(): pl.pallas_call(token_kernel, out_shape=jax.ShapeDtypeStruct((8 + ROWS, CH...]
  transfers between devices with their start and end apart: 5 -> 8, of which waited for: 5 -> 8; matrix products, arithmetic and copies ran while one was open for 0% -> 0% of each run, Pallas kernels for 0% -> 2%
where the time goes in v6:
time: 41.8 us; the launch traced here: 41.7 us
  starting transfers between devices  15.6 us (37%)
  waiting for transfers between devices  14 us (33%)
  Pallas kernels  11.4 us (27%)
  between operations  0.71 us (2%)
    ppermute x6, starting transfers between devices, spread(): lax.ppermute(a, axis, [(i, (i + k) % 4) for i in range(4)])  10.2 us
    ppermute x6, waiting for transfers between devices, spread(): lax.ppermute(a, axis, [(i, (i + k) % 4) for i in range(4)])  9.44 us
    pallas_call x1, Pallas kernels, shards(): pl.pallas_call(maps_kernel, out_shape=[jax.ShapeDtypeStruct((2 * CH, CH),...  9.01 us
    ppermute x2, starting transfers between devices, swap(): return lax.ppermute(array, axis, [(i, i ^ bit) for i in range(4)])  5.4 us
    ppermute x2, waiting for transfers between devices, swap(): return lax.ppermute(array, axis, [(i, i ^ bit) for i in range(4)])  4.55 us
  transfers between devices with their start and end apart: 8, of which 8 were waited for; matrix products, arithmetic and copies ran while one was open for 0% of the time, Pallas kernels for 2%

profile of v6, /device:TPU:2, one launch (start us, length us, event | category | flops | bytes accessed | tf_op | source)
XLA Modules:
  0.0 41.7 jit_solution(8477865511296847628)
XLA Ops:
  0.6 0.0 copy-start
  0.7 9.0 %maps.1 = (f32[256,128]{1,0:T(8,128)S(1)}, f32[256,128]{1,0:T(8,128)S(1)}, f32[256,128]{1,0:T(8,128)S(1)}, f32[256,128]{1,0:T(8,128)S(1)}) custom-call(bf16[2,512,2048]{2,1,0:T(8,128)(2,1)} %x_hbm.1, bf16[2048,256]{1,0:T(8,128)(2,1)} %wk_hbm.1, bf16[2048,256]{1,0:T(8,128)(2,1)} %wv_hbm.1, bf16[16,2048]{1,0:T(8,128)(2,1)} %bitcast.7, ...), custom_call_target="tpu_custom_call" | custom-call | tf_op jit(solution)/shard_map/maps/pallas_call | solution.py:403
  9.7 3.3 %collective-permute-start = (f32[256,128]{1,0:T(8,128)S(1)}, f32[256,128]{1,0:T(8,128)S(1)}, u32[]{:S(2)}, u32[]{:S(2)}) collective-permute-start(f32[256,128]{1,0:T(8,128)S(1)} %get-tuple-element.13), channel_id=1, source_target_pairs={{0,16},{8,24},{16,0},{24,8},{1,17},{9,25},{17,1},{25,9},{2,18},{10... | collective-permute-start | bytes 393224 | tf_op jit(solution)/shard_map/ppermute | solution.py:371
  13.0 1.1 %collective-permute-start.1 = (f32[256,128]{1,0:T(8,128)S(1)}, f32[256,128]{1,0:T(8,128)S(1)}, u32[]{:S(2)}, u32[]{:S(2)}) collective-permute-start(f32[256,128]{1,0:T(8,128)S(1)} %get-tuple-element.14), channel_id=1, source_target_pairs={{0,24},{8,0},{16,8},{24,16},{1,25},{9,1},{17,9},{25,17},{2,26},{10... | collective-permute-start | bytes 393224 | tf_op jit(solution)/shard_map/ppermute | solution.py:371
  14.0 1.0 %collective-permute-start.2 = (f32[256,128]{1,0:T(8,128)S(1)}, f32[256,128]{1,0:T(8,128)S(1)}, u32[]{:S(2)}, u32[]{:S(2)}) collective-permute-start(f32[256,128]{1,0:T(8,128)S(1)} %get-tuple-element.15), channel_id=1, source_target_pairs={{0,8},{8,16},{16,24},{24,0},{1,9},{9,17},{17,25},{25,1},{2,10},{10... | collective-permute-start | bytes 393224 | tf_op jit(solution)/shard_map/ppermute | solution.py:371
  15.0 2.2 %collective-permute-done.r1 = f32[256,128]{1,0:T(8,128)S(1)} collective-permute-done((f32[256,128]{1,0:T(8,128)S(1)}, f32[256,128]{1,0:T(8,128)S(1)}, u32[]{:S(2)}, u32[]{:S(2)}) %collective-permute-start) | collective-permute-done | bytes 131104 | tf_op jit(solution)/shard_map/ppermute | solution.py:371
  17.2 2.5 %collective-permute-done.1.r2 = f32[256,128]{1,0:T(8,128)S(1)} collective-permute-done((f32[256,128]{1,0:T(8,128)S(1)}, f32[256,128]{1,0:T(8,128)S(1)}, u32[]{:S(2)}, u32[]{:S(2)}) %collective-permute-start.1) | collective-permute-done | bytes 131104 | tf_op jit(solution)/shard_map/ppermute | solution.py:371
  19.7 0.5 %collective-permute-done.2.r3 = f32[256,128]{1,0:T(8,128)S(1)} collective-permute-done((f32[256,128]{1,0:T(8,128)S(1)}, f32[256,128]{1,0:T(8,128)S(1)}, u32[]{:S(2)}, u32[]{:S(2)}) %collective-permute-start.2) | collective-permute-done | bytes 131104 | tf_op jit(solution)/shard_map/ppermute | solution.py:371
  20.2 0.5 %segments.1.own = f32[256,128]{1,0:T(8,128)S(1)} custom-call(f32[256,128]{1,0:T(8,128)S(1)} %get-tuple-element.12.r0, f32[256,128]{1,0:T(8,128)S(1)} %collective-permute-done.r1, f32[256,128]{1,0:T(8,128)S(1)} %collective-permute-done.1.r2, f32[256,128]{1,0:T(8,128)S(1)} %collective-permute-done.2.r3), custom_call_target="tpu_custom_call" | custom-call | tf_op jit(solution)/shard_map/segments/pallas_call | solution.py:439
  20.8 2.0 %collective-permute-start.3 = (f32[256,128]{1,0:T(8,128)S(1)}, f32[256,128]{1,0:T(8,128)S(1)}, u32[]{:S(2)}, u32[]{:S(2)}) collective-permute-start(f32[256,128]{1,0:T(8,128)S(1)} %segments.1.own), channel_id=1, source_target_pairs={{0,32},{32,0},{64,96},{96,64},{1,33},{33,1},{65,97},{97,65},{2,34}... | collective-permute-start | bytes 393224 | tf_op jit(solution)/shard_map/ppermute | solution.py:377
  22.8 0.0 copy-done.1
  22.8 0.7 %token_.1.token = f32[40,128]{1,0:T(8,128)S(1)} custom-call(bf16[2,2,128]{2,1,0:T(2,128)(2,1)S(1)} %copy-done, bf16[2,2,128]{2,1,0:T(2,128)(2,1)S(1)} %copy-done.1, bf16[2,2,128]{2,1,0:T(2,128)(2,1)S(1)} %copy-done.2, f32[2,2]{1,0:T(2,128)S(1)} %copy-done.3), custom_call_target="tpu_custom_call" | custom-call | tf_op jit(solution)/shard_map/token/pallas_call | solution.py:448
  23.5 2.3 %collective-permute-done.3.other = f32[256,128]{1,0:T(8,128)S(1)} collective-permute-done((f32[256,128]{1,0:T(8,128)S(1)}, f32[256,128]{1,0:T(8,128)S(1)}, u32[]{:S(2)}, u32[]{:S(2)}) %collective-permute-start.3) | collective-permute-done | bytes 131104 | tf_op jit(solution)/shard_map/ppermute | solution.py:377
  25.8 0.2 halves.1
  26.1 3.4 %collective-permute-start.4 = (f32[128,128]{1,0:T(8,128)S(1)}, f32[128,128]{1,0:T(8,128)S(1)}, u32[]{:S(2)}, u32[]{:S(2)}) collective-permute-start(f32[128,128]{1,0:T(8,128)S(1)} %get-tuple-element.17), channel_id=1, source_target_pairs={{0,64},{32,96},{64,0},{96,32},{1,65},{33,97},{65,1},{97,33},{2,66}... | collective-permute-start | bytes 196616 | tf_op jit(solution)/shard_map/ppermute | solution.py:377
  29.5 2.2 %collective-permute-done.4.theirs = f32[128,128]{1,0:T(8,128)S(1)} collective-permute-done((f32[128,128]{1,0:T(8,128)S(1)}, f32[128,128]{1,0:T(8,128)S(1)}, u32[]{:S(2)}, u32[]{:S(2)}) %collective-permute-start.4) | collective-permute-done | bytes 65568 | tf_op jit(solution)/shard_map/ppermute | solution.py:377
  31.7 0.3 rows.1
  32.0 2.8 %collective-permute-start.5 = (f32[16,128]{1,0:T(8,128)S(1)}, f32[16,128]{1,0:T(8,128)S(1)}, u32[]{:S(2)}, u32[]{:S(2)}) collective-permute-start(f32[16,128]{1,0:T(8,128)S(1)} %get-tuple-element.19), channel_id=1, source_target_pairs={{0,16},{8,24},{16,0},{24,8},{1,17},{9,25},{17,1},{25,9},{2,18},{10... | collective-permute-start | bytes 24584 | tf_op jit(solution)/shard_map/ppermute | solution.py:371
  34.8 1.4 %collective-permute-start.6 = (f32[16,128]{1,0:T(8,128)S(1)}, f32[16,128]{1,0:T(8,128)S(1)}, u32[]{:S(2)}, u32[]{:S(2)}) collective-permute-start(f32[16,128]{1,0:T(8,128)S(1)} %get-tuple-element.20), channel_id=1, source_target_pairs={{0,24},{8,0},{16,8},{24,16},{1,25},{9,1},{17,9},{25,17},{2,26},{10... | collective-permute-start | bytes 24584 | tf_op jit(solution)/shard_map/ppermute | solution.py:371
  36.2 0.6 %collective-permute-start.7 = (f32[16,128]{1,0:T(8,128)S(1)}, f32[16,128]{1,0:T(8,128)S(1)}, u32[]{:S(2)}, u32[]{:S(2)}) collective-permute-start(f32[16,128]{1,0:T(8,128)S(1)} %get-tuple-element.21), channel_id=1, source_target_pairs={{0,8},{8,16},{16,24},{24,0},{1,9},{9,17},{17,25},{25,1},{2,10},{10... | collective-permute-start | bytes 24584 | tf_op jit(solution)/shard_map/ppermute | solution.py:371
  36.8 0.3 collective-permute-done.5.r1
  37.2 1.3 %collective-permute-done.6.r2 = f32[16,128]{1,0:T(8,128)S(1)} collective-permute-done((f32[16,128]{1,0:T(8,128)S(1)}, f32[16,128]{1,0:T(8,128)S(1)}, u32[]{:S(2)}, u32[]{:S(2)}) %collective-permute-start.6) | collective-permute-done | bytes 8224 | tf_op jit(solution)/shard_map/ppermute | solution.py:371
  38.5 2.6 %collective-permute-done.7.r3 = f32[16,128]{1,0:T(8,128)S(1)} collective-permute-done((f32[16,128]{1,0:T(8,128)S(1)}, f32[16,128]{1,0:T(8,128)S(1)}, u32[]{:S(2)}, u32[]{:S(2)}) %collective-permute-start.7) | collective-permute-done | bytes 8224 | tf_op jit(solution)/shard_map/ppermute | solution.py:371
  41.1 0.6 %finish.1 = (bf16[2,2,8,128]{3,2,1,0:T(8,128)(2,1)}, bf16[2,2,128]{2,1,0:T(2,128)(2,1)}) custom-call(f32[16,128]{1,0:T(8,128)S(1)} %get-tuple-element.18.r0, f32[16,128]{1,0:T(8,128)S(1)} %collective-permute-done.5.r1, f32[16,128]{1,0:T(8,128)S(1)} %collective-permute-done.6.r2, f32[16,128]{1,0:T(8,128)S(1)} %collective-permute-done.7.r3), custom_call_target="tpu_custom_call" | custom-call | tf_op jit(solution)/shard_map/finish/pallas_call | solution.py:478
  (8 shorter events, 0.0 us)
Async XLA Ops:
  0.6 22.1 %copy-start = (bf16[2,2,128]{2,1,0:T(2,128)(2,1)S(1)}, bf16[2,2,128]{2,1,0:T(2,128)(2,1)}, u32[]{:S(2)}) copy-start(bf16[2,2,128]{2,1,0:T(2,128)(2,1)} %query_ref.1) | copy-start | bytes 3076
  0.6 22.1 %copy-start.1 = (bf16[2,2,128]{2,1,0:T(2,128)(2,1)S(1)}, bf16[2,2,128]{2,1,0:T(2,128)(2,1)}, u32[]{:S(2)}) copy-start(bf16[2,2,128]{2,1,0:T(2,128)(2,1)} %key_ref.1) | copy-start | bytes 3076
  0.7 22.1 %copy-start.2 = (bf16[2,2,128]{2,1,0:T(2,128)(2,1)S(1)}, bf16[2,2,128]{2,1,0:T(2,128)(2,1)}, u32[]{:S(2)}) copy-start(bf16[2,2,128]{2,1,0:T(2,128)(2,1)} %value_ref.1) | copy-start | bytes 3076
  0.7 22.1 %copy-start.3 = (f32[2,2]{1,0:T(2,128)S(1)}, f32[2,2]{1,0:T(2,128)}, u32[]{:S(2)}) copy-start(f32[2,2]{1,0:T(2,128)} %gate_ref.1) | copy-start | bytes 52
  0.7 31.0 %copy-start.4 = (f32[128]{0:T(128)S(1)}, f32[128]{0:T(128)}, u32[]{:S(2)}) copy-start(f32[128]{0:T(128)} %param.25) | copy-start | bytes 1540
  9.7 7.5 %collective-permute-start = (f32[256,128]{1,0:T(8,128)S(1)}, f32[256,128]{1,0:T(8,128)S(1)}, u32[]{:S(2)}, u32[]{:S(2)}) collective-permute-start(f32[256,128]{1,0:T(8,128)S(1)} %get-tuple-element.13), channel_id=1, source_target_pairs={{0,16},{8,24},{16,0},{24,8},{1,17},{9,25},{17,1},{25,9},{2,18},{10... | collective-permute-start | bytes 393224 | tf_op jit(solution)/shard_map/ppermute | solution.py:371
  13.0 6.7 %collective-permute-start.1 = (f32[256,128]{1,0:T(8,128)S(1)}, f32[256,128]{1,0:T(8,128)S(1)}, u32[]{:S(2)}, u32[]{:S(2)}) collective-permute-start(f32[256,128]{1,0:T(8,128)S(1)} %get-tuple-element.14), channel_id=1, source_target_pairs={{0,24},{8,0},{16,8},{24,16},{1,25},{9,1},{17,9},{25,17},{2,26},{10... | collective-permute-start | bytes 393224 | tf_op jit(solution)/shard_map/ppermute | solution.py:371
  14.0 6.2 %collective-permute-start.2 = (f32[256,128]{1,0:T(8,128)S(1)}, f32[256,128]{1,0:T(8,128)S(1)}, u32[]{:S(2)}, u32[]{:S(2)}) collective-permute-start(f32[256,128]{1,0:T(8,128)S(1)} %get-tuple-element.15), channel_id=1, source_target_pairs={{0,8},{8,16},{16,24},{24,0},{1,9},{9,17},{17,25},{25,1},{2,10},{10... | collective-permute-start | bytes 393224 | tf_op jit(solution)/shard_map/ppermute | solution.py:371
  20.8 5.1 %collective-permute-start.3 = (f32[256,128]{1,0:T(8,128)S(1)}, f32[256,128]{1,0:T(8,128)S(1)}, u32[]{:S(2)}, u32[]{:S(2)}) collective-permute-start(f32[256,128]{1,0:T(8,128)S(1)} %segments.1.own), channel_id=1, source_target_pairs={{0,32},{32,0},{64,96},{96,64},{1,33},{33,1},{65,97},{97,65},{2,34}... | collective-permute-start | bytes 393224 | tf_op jit(solution)/shard_map/ppermute | solution.py:377
  26.1 5.6 %collective-permute-start.4 = (f32[128,128]{1,0:T(8,128)S(1)}, f32[128,128]{1,0:T(8,128)S(1)}, u32[]{:S(2)}, u32[]{:S(2)}) collective-permute-start(f32[128,128]{1,0:T(8,128)S(1)} %get-tuple-element.17), channel_id=1, source_target_pairs={{0,64},{32,96},{64,0},{96,32},{1,65},{33,97},{65,1},{97,33},{2,66}... | collective-permute-start | bytes 196616 | tf_op jit(solution)/shard_map/ppermute | solution.py:377
  32.0 5.2 %collective-permute-start.5 = (f32[16,128]{1,0:T(8,128)S(1)}, f32[16,128]{1,0:T(8,128)S(1)}, u32[]{:S(2)}, u32[]{:S(2)}) collective-permute-start(f32[16,128]{1,0:T(8,128)S(1)} %get-tuple-element.19), channel_id=1, source_target_pairs={{0,16},{8,24},{16,0},{24,8},{1,17},{9,25},{17,1},{25,9},{2,18},{10... | collective-permute-start | bytes 24584 | tf_op jit(solution)/shard_map/ppermute | solution.py:371
  34.8 3.7 %collective-permute-start.6 = (f32[16,128]{1,0:T(8,128)S(1)}, f32[16,128]{1,0:T(8,128)S(1)}, u32[]{:S(2)}, u32[]{:S(2)}) collective-permute-start(f32[16,128]{1,0:T(8,128)S(1)} %get-tuple-element.20), channel_id=1, source_target_pairs={{0,24},{8,0},{16,8},{24,16},{1,25},{9,1},{17,9},{25,17},{2,26},{10... | collective-permute-start | bytes 24584 | tf_op jit(solution)/shard_map/ppermute | solution.py:371
  36.2 4.9 %collective-permute-start.7 = (f32[16,128]{1,0:T(8,128)S(1)}, f32[16,128]{1,0:T(8,128)S(1)}, u32[]{:S(2)}, u32[]{:S(2)}) collective-permute-start(f32[16,128]{1,0:T(8,128)S(1)} %get-tuple-element.21), channel_id=1, source_target_pairs={{0,8},{8,16},{16,24},{24,0},{1,9},{9,17},{17,25},{25,1},{2,10},{10... | collective-permute-start | bytes 24584 | tf_op jit(solution)/shard_map/ppermute | solution.py:371

commit v7 on v6

--- a/solution.py
+++ b/solution.py
@@ -7,6 +7,7 @@
 from jax.experimental.pallas import tpu as pltpu
 from jax.sharding import Mesh
 from jax.sharding import PartitionSpec as P
+
 
 SP = ("sp_0", "sp_1")
 CH = 128
@@ -105,174 +106,162 @@
     return c1 * c2, c2 * d1 + moved[:, :CH], c2 * b1 - moved[:, CH:] + b2
 
 
-def maps_kernel(
+def sequence_maps(x, wk, wv, gatew, extra, rows, kbuf, vbuf, state, seq, arrivals, same, flip):
+    here = lax.axis_index("sp_1")
+    first_head = lax.axis_index("tp") * 2
+    tile = x.shape[0]
+    half = tile // 2
+    chunks = tile // CH
+    heads = gatew.shape[0] // 2
+    pick = iota((heads, tile), 0)
+    row = iota((CH, CH), 0)
+    col = iota((CH, CH), 1)
+    eye = jnp.where(row == col, 1.0, 0.0)
+    upto = jnp.where(row <= col, 1.0, 0.0).astype(BF16)
+
+    def times(i, weights, dims=AB):
+        return lax.dot_general(
+            x[i * half : (i + 1) * half], weights[...], dims, preferred_element_type=F32
+        )
+
+    def keys(i, kp):
+        kp = silu(kp)
+        for h in range(2):
+            kbuf[h, i * half : (i + 1) * half, :] = unit_rows(kp[:, h * CH : (h + 1) * CH]).astype(BF16)
+
+    def values(i, vp):
+        vp = silu(vp).astype(BF16)
+        for h in range(2):
+            vbuf[h, i * half : (i + 1) * half, :] = vp[:, h * CH : (h + 1) * CH]
+
+    arrivals[0]()
+    g0 = times(0, gatew, ABT)
+    k0 = times(0, wk)
+    arrivals[1]()
+    g1 = times(1, gatew, ABT)
+    k1 = times(1, wk)
+    keys(0, k0)
+    arrivals[2]()
+    bias, rate = rows[0:2, :], rows[2:4, :]
+    gt = jnp.concatenate([jnp.transpose(g) for g in (g0, g1)], axis=1)
+    picked = [
+        jnp.sum(jnp.where(pick == first_head + h, part, 0.0), axis=0, keepdims=True)
+        for part in (gt[:heads], gt[heads:])
+        for h in range(2)
+    ]
+    gate = jnp.concatenate(picked[:2], axis=0)
+    z = jnp.concatenate(picked[2:], axis=0)
+    soft = jnp.maximum(z, 0.0) + jnp.log1p(jnp.exp(-jnp.abs(z)))
+    steps, gates = [], []
+    for n in range(chunks):
+        lanes = slice(n * CH, (n + 1) * CH)
+        steps.append(extra[seq * chunks + n] - rate * soft[:, lanes])
+        gates.append(gate[:, lanes] + bias)
+    step = jnp.concatenate(steps, axis=0)
+    beta = 1.0 / (1.0 + jnp.exp(-jnp.concatenate(gates, axis=0)))
+    hi = step.astype(BF16)
+    rest = step - hi.astype(F32)
+    mid = rest.astype(BF16)
+    low = (rest - mid.astype(F32)).astype(BF16)
+    cum = dot1(hi, upto) + (dot1(mid, upto) + dot1(low, upto))
+    count = cum.shape[0]
+    total = jnp.broadcast_to(cum[:, CH - 1 : CH], (count, CH))
+    carry = jnp.exp(total)
+    ecum = jnp.exp(cum)
+    columns = jnp.transpose(
+        jnp.concatenate(
+            [cum + jnp.log(beta), jnp.exp(total - cum), jnp.zeros((CH - 2 * count, CH), F32)], axis=0
+        )
+    )
+    keys(1, k1)
+    v0 = times(0, wv)
+    v1 = times(1, wv)
+    values(0, v0)
+    values(1, v1)
+    items = [(n, h) for n in range(chunks) for h in range(2)]
+    ks = [kbuf[h, n * CH : (n + 1) * CH, :] for n, h in items]
+    grams = [lax.dot_general(k, k, ABT, preferred_element_type=F32) for k in ks]
+    ms = [
+        jnp.where(row > col, g * jnp.exp(columns[:, r : r + 1] - cum[r : r + 1, :]), 0.0)
+        for r, g in enumerate(grams)
+    ]
+    invs = inverses_of(ms)
+    us = [columns[:, count + r : count + r + 1] * inv * beta[r : r + 1, :] for r, inv in enumerate(invs)]
+    pulls = [
+        dot1(u * ecum[r : r + 1, :], k).astype(BF16) for r, (u, k) in enumerate(zip(us, ks))
+    ]
+    freshs = [
+        dot1(u, vbuf[h, n * CH : (n + 1) * CH, :]).astype(BF16) for (n, h), u in zip(items, us)
+    ]
+    boths = [
+        dot1(k, jnp.concatenate([pull, fresh], axis=1), ATB)
+        for k, pull, fresh in zip(ks, pulls, freshs)
+    ]
+    maps = [
+        [
+            (carry[2 * n + h : 2 * n + h + 1, :], boths[2 * n + h][:, :CH], boths[2 * n + h][:, CH:])
+            for n in range(chunks)
+        ]
+        for h in range(2)
+    ]
+    while len(maps[0]) > 1:
+        maps = [[joined(m[i], m[i + 1], eye) for i in range(0, len(m), 2)] for m in maps]
+    for h in range(2):
+        c_row, drop, gain = maps[h][0]
+        state[h, :CH, :] = c_row * eye - drop
+        state[h, CH:, :] = gain
+    parity = lax.rem(here, 2)
+    same[...] = state[parity]
+    flip[...] = state[1 - parity]
+
+
+def far_kernel(
     x_hbm, wk_hbm, wv_hbm, gate_hbm, decay_hbm, bias_hbm, rate_hbm, extra_hbm,
-    o0, o1, o2, o3,
-    xbuf, wkbuf, wvbuf, gatew, extra, bias_ref, rate_ref, kbuf, vbuf, state, sems,
+    same, flip, x_kept, wk, wv, gatew, extra, rows,
+    x, bias_ref, rate_ref, kbuf, vbuf, state, sems,
 ):
-    tiles, tile, width = xbuf.shape
-    half = tile // 2
     first_head = lax.axis_index("tp") * 2
-    here = lax.axis_index("sp_1")
-    per_seq = kbuf.shape[0] // (2 * CH)
+    own = lax.div(lax.axis_index("sp_1"), 2)
+    half = x.shape[0] // 2
     heads = gate_hbm.shape[0]
+    top, low = pl.ds(0, half), pl.ds(half, half)
     moves = [
         (gate_hbm, gatew.at[pl.ds(0, heads)]),
         (decay_hbm, gatew.at[pl.ds(heads, heads)]),
         (bias_hbm, bias_ref),
         (rate_hbm, rate_ref),
         (extra_hbm, extra),
-    ]
-    small = len(moves)
-    for t in range(tiles):
-        for i in range(2):
-            rows = pl.ds(i * half, half)
-            moves.append((x_hbm.at[t, rows], xbuf.at[t, rows]))
-            if t == 0:
-                moves.append(((wk_hbm, wkbuf), (wv_hbm, wvbuf))[i])
+        (x_hbm.at[1 - own, top], x.at[top]),
+        (wk_hbm, wk),
+        (x_hbm.at[1 - own, low], x.at[low]),
+        (wv_hbm, wv),
+        (x_hbm.at[own], x_kept),
+    ]
     copies = [pltpu.make_async_copy(src, dst, sems.at[i]) for i, (src, dst) in enumerate(moves)]
     for c in copies:
         c.start()
-    for c in copies[:small]:
+    for c in copies[:5]:
         c.wait()
-    arrivals = copies[small:]
-    pick = iota((heads, tile), 0)
-    odd = iota((2, tile), 0) == 1
-    bias = jnp.where(odd, bias_ref[first_head + 1], bias_ref[first_head])
-    rate = jnp.exp(jnp.where(odd, rate_ref[first_head + 1], rate_ref[first_head]))
-    row = iota((CH, CH), 0)
-    col = iota((CH, CH), 1)
-    eye = jnp.where(row == col, 1.0, 0.0)
-    upto = jnp.where(row <= col, 1.0, 0.0).astype(BF16)
-
-    def times(t, i, weights, dims=AB):
-        x = xbuf[t, i * half : (i + 1) * half]
-        return lax.dot_general(x, weights[...], dims, preferred_element_type=F32)
-
-    def scalars(t, gt):
-        picked = [
-            jnp.sum(jnp.where(pick == first_head + h, part, 0.0), axis=0, keepdims=True)
-            for part in (gt[:heads], gt[heads:])
-            for h in range(2)
-        ]
-        z = jnp.concatenate(picked[2:], axis=0)
-        soft = jnp.maximum(z, 0.0) + jnp.log1p(jnp.exp(-jnp.abs(z)))
-        gate = jnp.concatenate(picked[:2], axis=0) + bias
-        steps, gates = [], []
-        for n in range(per_seq):
-            lanes = slice(n * CH, (n + 1) * CH)
-            steps.append(extra[t * per_seq + n] - rate[:, lanes] * soft[:, lanes])
-            gates.append(gate[:, lanes])
-        step = jnp.concatenate(steps, axis=0)
-        beta = 1.0 / (1.0 + jnp.exp(-jnp.concatenate(gates, axis=0)))
-        hi = step.astype(BF16)
-        rest = step - hi.astype(F32)
-        mid = rest.astype(BF16)
-        low = (rest - mid.astype(F32)).astype(BF16)
-        cum = dot1(hi, upto) + (dot1(mid, upto) + dot1(low, upto))
-        count = cum.shape[0]
-        total = jnp.broadcast_to(cum[:, CH - 1 : CH], (count, CH))
-        columns = jnp.transpose(
-            jnp.concatenate(
-                [cum + jnp.log(beta), jnp.exp(total - cum), jnp.zeros((CH - 2 * count, CH), F32)], axis=0
-            )
-        )
-        return beta, cum, jnp.exp(total), jnp.exp(cum), columns
-
-    def weighted(t, kp, rows):
-        kp = silu(kp)
-        for h in range(2):
-            lanes = slice(h * CH, (h + 1) * CH)
-            kbuf[rows, lanes] = unit_rows(kp[:, lanes]).astype(BF16)
-
-    def matrices(t, cum, columns):
-        ms = []
-        for n in range(per_seq):
-            for h in range(2):
-                k = part(kbuf, t, n, h)
-                gram = lax.dot_general(k, k, ABT, preferred_element_type=F32)
-                r = 2 * n + h
-                ms.append(jnp.where(row > col, gram * jnp.exp(columns[:, r : r + 1] - cum[r : r + 1, :]), 0.0))
-        return ms
-
-    def part(buf, s, n, h):
-        start = (s * per_seq + n) * CH
-        return buf[start : start + CH, h * CH : (h + 1) * CH]
-
-    def keys(t, i, kp):
-        weighted(t, kp, slice(t * tile + i * half, t * tile + (i + 1) * half))
-
-    def values(t, i, vp):
-        vbuf[t * tile + i * half : t * tile + (i + 1) * half, :] = silu(vp).astype(BF16)
-
-    def rows_from(t, gts):
-        return scalars(t, jnp.concatenate([jnp.transpose(g) for g in gts], axis=1))
-
-    x00, wk, x01, wv, x10, x11 = arrivals
-    x00.wait()
-    wk.wait()
-    g00 = times(0, 0, gatew, ABT)
-    k00 = times(0, 0, wkbuf)
-    x01.wait()
-    g01 = times(0, 1, gatew, ABT)
-    k01 = times(0, 1, wkbuf)
-    keys(0, 0, k00)
-    wv.wait()
-    v00 = times(0, 0, wvbuf)
-    v01 = times(0, 1, wvbuf)
-    keys(0, 1, k01)
-    x10.wait()
-    x11.wait()
-    g10 = times(1, 0, gatew, ABT)
-    k10 = times(1, 0, wkbuf)
-    rows_of = [rows_from(0, (g00, g01))]
-    g11 = times(1, 1, gatew, ABT)
-    k11 = times(1, 1, wkbuf)
-    values(0, 0, v00)
-    values(0, 1, v01)
-    rows_of.append(rows_from(1, (g10, g11)))
-    keys(1, 0, k10)
-    v10 = times(1, 0, wvbuf)
-    v11 = times(1, 1, wvbuf)
-    ms = matrices(0, rows_of[0][1], rows_of[0][4])
-    keys(1, 1, k11)
-    ms += matrices(1, rows_of[1][1], rows_of[1][4])
-    values(1, 0, v10)
-    values(1, 1, v11)
-
-    items = [(s, n, h) for s in range(2) for n in range(per_seq) for h in range(2)]
-    invs = inverses_of(ms)
-    us = []
-    for (s, n, h), inv in zip(items, invs):
-        beta, _, _, _, columns = rows_of[s]
-        r = 2 * n + h
-        us.append(columns[:, 8 + r : 9 + r] * inv * beta[r : r + 1, :])
-    pulls = [
-        dot1(u * rows_of[s][3][2 * n + h : 2 * n + h + 1, :], part(kbuf, s, n, h)).astype(BF16)
-        for (s, n, h), u in zip(items, us)
-    ]
-    freshs = [dot1(u, part(vbuf, s, n, h)).astype(BF16) for (s, n, h), u in zip(items, us)]
-    boths = {
-        (s, n, h): dot1(part(kbuf, s, n, h), jnp.concatenate([pull, fresh], axis=1), ATB)
-        for (s, n, h), pull, fresh in zip(items, pulls, freshs)
-    }
-    maps = []
-    for p in range(4):
-        s, h = divmod(p, 2)
-        parts = []
-        for n in range(per_seq):
-            c_row = rows_of[s][2][2 * n + h : 2 * n + h + 1, :]
-            parts.append((c_row, boths[s, n, h][:, :CH], boths[s, n, h][:, CH:]))
-        maps.append(parts)
-    while len(maps[0]) > 1:
-        maps = [[joined(m[i], m[i + 1], eye) for i in range(0, len(m), 2)] for m in maps]
-    for p in range(4):
-        c_row, drop, gain = maps[p][0]
-        state[p, :CH, :] = c_row * eye - drop
-        state[p, CH:, :] = gain
-
-    for k, o in zip(SHIFTS, (o0, o1, o2, o3)):
-        o[...] = state[lax.rem(here + k, 4)]
+    odd = iota((2, CH), 0) == 1
+    rows[0:2, :] = jnp.where(odd, bias_ref[first_head + 1], bias_ref[first_head])
+    rows[2:4, :] = jnp.exp(jnp.where(odd, rate_ref[first_head + 1], rate_ref[first_head]))
+    rows[4:, :] = jnp.zeros((4, CH), F32)
+
+    def first():
+        copies[5].wait()
+        copies[6].wait()
+
+    arrivals = (first, copies[7].wait, copies[8].wait)
+    sequence_maps(
+        x, wk, wv, gatew, extra, rows, kbuf, vbuf, state, 1 - own, arrivals, same, flip
+    )
+    copies[9].wait()
+
+
+def near_kernel(x, wk, wv, gatew, extra, rows, same, flip, kbuf, vbuf, state):
+    own = lax.div(lax.axis_index("sp_1"), 2)
+    arrivals = (lambda: None,) * 3
+    sequence_maps(x, wk, wv, gatew, extra, rows, kbuf, vbuf, state, own, arrivals, same, flip)
 
 
 def after(first, second):
@@ -282,8 +271,8 @@
 
 def segments_kernel(r0, r1, r2, r3, out, scr):
     here = lax.axis_index("sp_1")
-    for k, ref in zip(SHIFTS, (r0, r1, r2, r3)):
-        scr[lax.rem(here + 4 - k, 4)] = ref[...]
+    for k, ref in enumerate((r0, r1, r2, r3)):
+        scr[jnp.bitwise_xor(here, k)] = ref[...]
     maps = [(scr[t, :CH, :], scr[t, CH:, :]) for t in range(4)]
     while len(maps) > 1:
         maps = [after(maps[i], maps[i + 1]) for i in range(0, len(maps), 2)]
@@ -394,32 +383,34 @@
 ):
     seqs, seg, width = tokens.shape
     cols = key_matrix.shape[1]
-    tile = seg
-    tiles = seqs * seg // tile
+    gate_count = gate_matrix.shape[1]
     chunks = seqs * seg // CH
     extra = jnp.transpose(extra_log_decay.reshape(chunks, CH, 2), (0, 2, 1))
     hbm = pl.BlockSpec(memory_space=pltpu.HBM)
     smem = pl.BlockSpec(memory_space=pltpu.SMEM)
-    maps = pl.pallas_call(
-        maps_kernel,
-        out_shape=[jax.ShapeDtypeStruct((2 * CH, CH), F32)] * 4,
+    halved = [pltpu.VMEM((2, seg, CH), BF16)] * 2 + [pltpu.VMEM((2, 2 * CH, CH), F32)]
+    far2, far3, *kept = pl.pallas_call(
+        far_kernel,
+        out_shape=[jax.ShapeDtypeStruct((2 * CH, CH), F32)] * 2
+        + [
+            jax.ShapeDtypeStruct((seg, width), BF16),
+            jax.ShapeDtypeStruct((width, cols), BF16),
+            jax.ShapeDtypeStruct((width, cols), BF16),
+            jax.ShapeDtypeStruct((2 * gate_count, width), BF16),
+            jax.ShapeDtypeStruct((chunks, 2, CH), F32),
+            jax.ShapeDtypeStruct((8, CH), F32),
+        ],
         in_specs=[hbm] * 8,
-        out_specs=vmem(4),
+        out_specs=vmem(8),
         scratch_shapes=[
-            pltpu.VMEM((tiles, tile, width), BF16),
-            pltpu.VMEM((width, cols), BF16),
-            pltpu.VMEM((width, cols), BF16),
-            pltpu.VMEM((2 * gate_matrix.shape[1], width), BF16),
-            pltpu.VMEM((chunks, 2, CH), F32),
+            pltpu.VMEM((seg, width), BF16),
             pltpu.SMEM(gate_bias_offset.shape, F32),
             pltpu.SMEM(head_log_decay_rate.shape, F32),
-            pltpu.VMEM((seqs * seg, cols), BF16),
-            pltpu.VMEM((seqs * seg, cols), BF16),
-            pltpu.VMEM((4, 2 * CH, CH), F32),
-            pltpu.SemaphoreType.DMA((11,)),
+            *halved,
+            pltpu.SemaphoreType.DMA((10,)),
         ],
         compiler_params=pltpu.CompilerParams(vmem_limit_bytes=24 * 2**20),
-        name="maps",
+        name="far",
     )(
         *(
             pltpu.with_memory_space_constraint(a, pltpu.HBM)
@@ -435,6 +426,19 @@
             )
         )
     )
+    from2 = swap(far2, "sp_1", 2)
+    from3 = swap(far3, "sp_1", 3)
+    near = pl.pallas_call(
+        near_kernel,
+        out_shape=[jax.ShapeDtypeStruct((2 * CH, CH), F32)] * 2,
+        in_specs=vmem(6),
+        out_specs=vmem(2),
+        scratch_shapes=halved,
+        compiler_params=pltpu.CompilerParams(vmem_limit_bytes=16 * 2**20),
+        cost_estimate=pl.CostEstimate(flops=3 * 10**9, bytes_accessed=10**6, transcendentals=0),
+        name="near",
+    )
+    mine, near1 = near(*kept)
     small = pltpu.CompilerParams(vmem_limit_bytes=8 * 2**20)
     segment = pl.pallas_call(
         segments_kernel,
@@ -444,7 +448,7 @@
         scratch_shapes=[pltpu.VMEM((4, 2 * CH, CH), F32)],
         compiler_params=small,
         name="segments",
-    )(*spread(maps, "sp_1"))
+    )(mine, swap(near1, "sp_1", 1), from2, from3)
     token = pl.pallas_call(
         token_kernel,
         out_shape=jax.ShapeDtypeStruct((8 + ROWS, CH), F32),

time: 41.8 us -> 44.1 us (1.055)
  waiting for transfers between devices: 14 us -> 17.4 us
  starting transfers between devices: 15.6 us -> 12.3 us
  Pallas kernels: 11.4 us -> 13.2 us
    ppermute x6 -> x3, starting transfers between devices: 10.2 us -> 2.13 us  [spread(): lax.ppermute(a, axis, [(i, (i + k) % 4) for i in range(4)])]
    ppermute x2 -> x5, waiting for transfers between devices: 4.55 us -> 12.5 us  [swap(): return lax.ppermute(array, axis, [(i, i ^ bit) for i in range(4)])]
    ppermute x2 -> x5, starting transfers between devices: 5.4 us -> 10.2 us  [swap(): return lax.ppermute(array, axis, [(i, i ^ bit) for i in range(4)])]
    ppermute x6 -> x3, waiting for transfers between devices: 9.44 us -> 4.85 us  [spread(): lax.ppermute(a, axis, [(i, (i + k) % 4) for i in range(4)])]
    pallas_call x1 -> x2, Pallas kernels: 9.01 us -> 10.8 us  [the longest x1 6.44 us: shards(): pl.pallas_call(far_kernel, out_shape=[jax.ShapeDtypeStruct((2 * CH, CH),...]
  transfers between devices with their start and end apart: 8 -> 8, of which waited for: 8 -> 7; matrix products, arithmetic and copies ran while one was open for 0% -> 0% of each run, Pallas kernels for 2% -> 2%
where the time goes in v7:
time: 44.1 us; the launch traced here: 43.7 us
  waiting for transfers between devices  17.4 us (39%)
  Pallas kernels  13.2 us (30%)
  starting transfers between devices  12.3 us (28%)
  between operations  0.72 us (2%)
    ppermute x5, waiting for transfers between devices, swap(): return lax.ppermute(array, axis, [(i, i ^ bit) for i in range(4)])  12.5 us
    ppermute x5, starting transfers between devices, swap(): return lax.ppermute(array, axis, [(i, i ^ bit) for i in range(4)])  10.2 us
    pallas_call x1, Pallas kernels, shards(): pl.pallas_call(far_kernel, out_shape=[jax.ShapeDtypeStruct((2 * CH, CH),...  6.44 us
    ppermute x3, waiting for transfers between devices, spread(): lax.ppermute(a, axis, [(i, (i + k) % 4) for i in range(4)])  4.85 us
    pallas_call x1, Pallas kernels, shards(): mine, near1 = near(*kept)  4.4 us
    ppermute x3, starting transfers between devices, spread(): lax.ppermute(a, axis, [(i, (i + k) % 4) for i in range(4)])  2.13 us
  transfers between devices with their start and end apart: 8, of which 7 were waited for; matrix products, arithmetic and copies ran while one was open for 0% of the time, Pallas kernels for 2%

profile of v7, /device:TPU:2, one launch (start us, length us, event | category | flops | bytes accessed | tf_op | source)
XLA Modules:
  0.0 43.7 jit_solution(3822506435715431915)
XLA Ops:
  0.6 6.4 %far.1 = (f32[256,128]{1,0:T(8,128)S(1)}, f32[256,128]{1,0:T(8,128)S(1)}, bf16[512,2048]{1,0:T(8,128)(2,1)S(1)}, bf16[2048,256]{1,0:T(8,128)(2,1)S(1)}, bf16[204...) custom-call(bf16[2,512,2048]{2,1,0:T(8,128)(2,1)} %x_hbm.1, ...), custom_call_target="tpu_custom_call" | custom-call | tf_op jit(solution)/shard_map/far/pallas_call | solution.py:392
  7.1 0.0 copy-start
  7.1 0.0 copy-start.3
  7.1 4.4 %near.1 = (f32[256,128]{1,0:T(8,128)S(1)}, f32[256,128]{1,0:T(8,128)S(1)}) custom-call(bf16[512,2048]{1,0:T(8,128)(2,1)S(1)} %get-tuple-element.18.x, bf16[2048,256]{1,0:T(8,128)(2,1)S(1)} %get-tuple-element.19.wk, bf16[2048,256]{1,0:T(8,128)(2,1)S(1)} %get-tuple-element.20.wv, bf16[32,2048]{1,0:T(8,128)(2,1)S(1)} %get-tuple-element.21.gatew, ...), custom_call_target="tpu_custom_call" | custom-call | flops 3000000000 | bytes 1000000 | tf_op jit(solution)/shard_map/near/pallas_call | solution.py:441
  11.5 1.7 %collective-permute-start = (f32[256,128]{1,0:T(8,128)S(1)}, f32[256,128]{1,0:T(8,128)S(1)}, u32[]{:S(2)}, u32[]{:S(2)}) collective-permute-start(f32[256,128]{1,0:T(8,128)S(1)} %get-tuple-element.25), channel_id=1, source_target_pairs={{0,8},{8,0},{16,24},{24,16},{1,9},{9,1},{17,25},{25,17},{2,10},{10... | collective-permute-start | bytes 393224 | tf_op jit(solution)/shard_map/ppermute | solution.py:366
  13.2 2.9 %collective-permute-start.1 = (f32[256,128]{1,0:T(8,128)S(1)}, f32[256,128]{1,0:T(8,128)S(1)}, u32[]{:S(2)}, u32[]{:S(2)}) collective-permute-start(f32[256,128]{1,0:T(8,128)S(1)} %get-tuple-element.26), channel_id=1, source_target_pairs={{0,16},{8,24},{16,0},{24,8},{1,17},{9,25},{17,1},{25,9},{2,18},{10... | collective-permute-start | bytes 393224 | tf_op jit(solution)/shard_map/ppermute | solution.py:366
  16.1 0.2 collective-permute-start.2
  16.3 1.0 %collective-permute-done.r1 = f32[256,128]{1,0:T(8,128)S(1)} collective-permute-done((f32[256,128]{1,0:T(8,128)S(1)}, f32[256,128]{1,0:T(8,128)S(1)}, u32[]{:S(2)}, u32[]{:S(2)}) %collective-permute-start) | collective-permute-done | bytes 131104 | tf_op jit(solution)/shard_map/ppermute | solution.py:366
  17.4 4.9 %collective-permute-done.1.r2 = f32[256,128]{1,0:T(8,128)S(1)} collective-permute-done((f32[256,128]{1,0:T(8,128)S(1)}, f32[256,128]{1,0:T(8,128)S(1)}, u32[]{:S(2)}, u32[]{:S(2)}) %collective-permute-start.1) | collective-permute-done | bytes 131104 | tf_op jit(solution)/shard_map/ppermute | solution.py:366
  22.2 2.1 %collective-permute-done.2.r3 = f32[256,128]{1,0:T(8,128)S(1)} collective-permute-done((f32[256,128]{1,0:T(8,128)S(1)}, f32[256,128]{1,0:T(8,128)S(1)}, u32[]{:S(2)}, u32[]{:S(2)}) %collective-permute-start.2) | collective-permute-done | bytes 131104 | tf_op jit(solution)/shard_map/ppermute | solution.py:366
  24.3 0.5 %segments.1.own = f32[256,128]{1,0:T(8,128)S(1)} custom-call(f32[256,128]{1,0:T(8,128)S(1)} %get-tuple-element.24.r0, f32[256,128]{1,0:T(8,128)S(1)} %collective-permute-done.r1, f32[256,128]{1,0:T(8,128)S(1)} %collective-permute-done.1.r2, f32[256,128]{1,0:T(8,128)S(1)} %collective-permute-done.2.r3), custom_call_target="tpu_custom_call" | custom-call | tf_op jit(solution)/shard_map/segments/pallas_call | solution.py:443
  24.8 2.0 %collective-permute-start.3 = (f32[256,128]{1,0:T(8,128)S(1)}, f32[256,128]{1,0:T(8,128)S(1)}, u32[]{:S(2)}, u32[]{:S(2)}) collective-permute-start(f32[256,128]{1,0:T(8,128)S(1)} %segments.1.own), channel_id=1, source_target_pairs={{0,32},{32,0},{64,96},{96,64},{1,33},{33,1},{65,97},{97,65},{2,34}... | collective-permute-start | bytes 393224 | tf_op jit(solution)/shard_map/ppermute | solution.py:366
  26.9 0.7 %token_.1.token = f32[40,128]{1,0:T(8,128)S(1)} custom-call(bf16[2,2,128]{2,1,0:T(2,128)(2,1)S(1)} %copy-done, bf16[2,2,128]{2,1,0:T(2,128)(2,1)S(1)} %copy-done.1, bf16[2,2,128]{2,1,0:T(2,128)(2,1)S(1)} %copy-done.2, f32[2,2]{1,0:T(2,128)S(1)} %copy-done.3), custom_call_target="tpu_custom_call" | custom-call | tf_op jit(solution)/shard_map/token/pallas_call | solution.py:452
  27.6 2.3 %collective-permute-done.3.other = f32[256,128]{1,0:T(8,128)S(1)} collective-permute-done((f32[256,128]{1,0:T(8,128)S(1)}, f32[256,128]{1,0:T(8,128)S(1)}, u32[]{:S(2)}, u32[]{:S(2)}) %collective-permute-start.3) | collective-permute-done | bytes 131104 | tf_op jit(solution)/shard_map/ppermute | solution.py:366
  29.9 0.2 halves.1
  30.1 3.4 %collective-permute-start.4 = (f32[128,128]{1,0:T(8,128)S(1)}, f32[128,128]{1,0:T(8,128)S(1)}, u32[]{:S(2)}, u32[]{:S(2)}) collective-permute-start(f32[128,128]{1,0:T(8,128)S(1)} %get-tuple-element.29), channel_id=1, source_target_pairs={{0,64},{32,96},{64,0},{96,32},{1,65},{33,97},{65,1},{97,33},{2,66}... | collective-permute-start | bytes 196616 | tf_op jit(solution)/shard_map/ppermute | solution.py:366
  33.6 2.2 %collective-permute-done.4.theirs = f32[128,128]{1,0:T(8,128)S(1)} collective-permute-done((f32[128,128]{1,0:T(8,128)S(1)}, f32[128,128]{1,0:T(8,128)S(1)}, u32[]{:S(2)}, u32[]{:S(2)}) %collective-permute-start.4) | collective-permute-done | bytes 65568 | tf_op jit(solution)/shard_map/ppermute | solution.py:366
  35.8 0.3 rows.1
  36.1 0.0 collective-permute-start.5
  36.1 2.1 %collective-permute-start.6 = (f32[16,128]{1,0:T(8,128)S(1)}, f32[16,128]{1,0:T(8,128)S(1)}, u32[]{:S(2)}, u32[]{:S(2)}) collective-permute-start(f32[16,128]{1,0:T(8,128)S(1)} %get-tuple-element.32), channel_id=1, source_target_pairs={{0,24},{8,0},{16,8},{24,16},{1,25},{9,1},{17,9},{25,17},{2,26},{10... | collective-permute-start | bytes 24584 | tf_op jit(solution)/shard_map/ppermute | solution.py:360
  38.2 0.0 collective-permute-start.7
  38.2 3.0 %collective-permute-done.5.r1 = f32[16,128]{1,0:T(8,128)S(1)} collective-permute-done((f32[16,128]{1,0:T(8,128)S(1)}, f32[16,128]{1,0:T(8,128)S(1)}, u32[]{:S(2)}, u32[]{:S(2)}) %collective-permute-start.5) | collective-permute-done | bytes 8224 | tf_op jit(solution)/shard_map/ppermute | solution.py:360
  41.3 1.8 %collective-permute-done.7.r3 = f32[16,128]{1,0:T(8,128)S(1)} collective-permute-done((f32[16,128]{1,0:T(8,128)S(1)}, f32[16,128]{1,0:T(8,128)S(1)}, u32[]{:S(2)}, u32[]{:S(2)}) %collective-permute-start.7) | collective-permute-done | bytes 8224 | tf_op jit(solution)/shard_map/ppermute | solution.py:360
  43.1 0.6 %finish.1 = (bf16[2,2,8,128]{3,2,1,0:T(8,128)(2,1)}, bf16[2,2,128]{2,1,0:T(2,128)(2,1)}) custom-call(f32[16,128]{1,0:T(8,128)S(1)} %get-tuple-element.30.r0, f32[16,128]{1,0:T(8,128)S(1)} %collective-permute-done.5.r1, f32[16,128]{1,0:T(8,128)S(1)} %collective-permute-done.6.r2, f32[16,128]{1,0:T(8,128)S(1)} %collective-permute-done.7.r3), custom_call_target="tpu_custom_call" | custom-call | tf_op jit(solution)/shard_map/finish/pallas_call | solution.py:482
  (9 shorter events, 0.0 us)
Async XLA Ops:
  7.1 19.8 %copy-start = (bf16[2,2,128]{2,1,0:T(2,128)(2,1)S(1)}, bf16[2,2,128]{2,1,0:T(2,128)(2,1)}, u32[]{:S(2)}) copy-start(bf16[2,2,128]{2,1,0:T(2,128)(2,1)} %query_ref.1) | copy-start | bytes 3076
  7.1 19.8 %copy-start.1 = (bf16[2,2,128]{2,1,0:T(2,128)(2,1)S(1)}, bf16[2,2,128]{2,1,0:T(2,128)(2,1)}, u32[]{:S(2)}) copy-start(bf16[2,2,128]{2,1,0:T(2,128)(2,1)} %key_ref.1) | copy-start | bytes 3076
  7.1 19.7 %copy-start.2 = (bf16[2,2,128]{2,1,0:T(2,128)(2,1)S(1)}, bf16[2,2,128]{2,1,0:T(2,128)(2,1)}, u32[]{:S(2)}) copy-start(bf16[2,2,128]{2,1,0:T(2,128)(2,1)} %value_ref.1) | copy-start | bytes 3076
  7.1 19.7 %copy-start.3 = (f32[2,2]{1,0:T(2,128)S(1)}, f32[2,2]{1,0:T(2,128)}, u32[]{:S(2)}) copy-start(f32[2,2]{1,0:T(2,128)} %gate_ref.1) | copy-start | bytes 52
  7.1 28.7 %copy-start.4 = (f32[128]{0:T(128)S(1)}, f32[128]{0:T(128)}, u32[]{:S(2)}) copy-start(f32[128]{0:T(128)} %param.25) | copy-start | bytes 1540
  11.5 5.8 %collective-permute-start = (f32[256,128]{1,0:T(8,128)S(1)}, f32[256,128]{1,0:T(8,128)S(1)}, u32[]{:S(2)}, u32[]{:S(2)}) collective-permute-start(f32[256,128]{1,0:T(8,128)S(1)} %get-tuple-element.25), channel_id=1, source_target_pairs={{0,8},{8,0},{16,24},{24,16},{1,9},{9,1},{17,25},{25,17},{2,10},{10... | collective-permute-start | bytes 393224 | tf_op jit(solution)/shard_map/ppermute | solution.py:366
  13.2 9.0 %collective-permute-start.1 = (f32[256,128]{1,0:T(8,128)S(1)}, f32[256,128]{1,0:T(8,128)S(1)}, u32[]{:S(2)}, u32[]{:S(2)}) collective-permute-start(f32[256,128]{1,0:T(8,128)S(1)} %get-tuple-element.26), channel_id=1, source_target_pairs={{0,16},{8,24},{16,0},{24,8},{1,17},{9,25},{17,1},{25,9},{2,18},{10... | collective-permute-start | bytes 393224 | tf_op jit(solution)/shard_map/ppermute | solution.py:366
  16.1 8.2 %collective-permute-start.2 = (f32[256,128]{1,0:T(8,128)S(1)}, f32[256,128]{1,0:T(8,128)S(1)}, u32[]{:S(2)}, u32[]{:S(2)}) collective-permute-start(f32[256,128]{1,0:T(8,128)S(1)} %get-tuple-element.27), channel_id=1, source_target_pairs={{0,24},{8,16},{16,8},{24,0},{1,25},{9,17},{17,9},{25,1},{2,26},{10... | collective-permute-start | bytes 393224 | tf_op jit(solution)/shard_map/ppermute | solution.py:366
  24.8 5.1 %collective-permute-start.3 = (f32[256,128]{1,0:T(8,128)S(1)}, f32[256,128]{1,0:T(8,128)S(1)}, u32[]{:S(2)}, u32[]{:S(2)}) collective-permute-start(f32[256,128]{1,0:T(8,128)S(1)} %segments.1.own), channel_id=1, source_target_pairs={{0,32},{32,0},{64,96},{96,64},{1,33},{33,1},{65,97},{97,65},{2,34}... | collective-permute-start | bytes 393224 | tf_op jit(solution)/shard_map/ppermute | solution.py:366
  30.1 5.7 %collective-permute-start.4 = (f32[128,128]{1,0:T(8,128)S(1)}, f32[128,128]{1,0:T(8,128)S(1)}, u32[]{:S(2)}, u32[]{:S(2)}) collective-permute-start(f32[128,128]{1,0:T(8,128)S(1)} %get-tuple-element.29), channel_id=1, source_target_pairs={{0,64},{32,96},{64,0},{96,32},{1,65},{33,97},{65,1},{97,33},{2,66}... | collective-permute-start | bytes 196616 | tf_op jit(solution)/shard_map/ppermute | solution.py:366
  36.1 5.2 %collective-permute-start.5 = (f32[16,128]{1,0:T(8,128)S(1)}, f32[16,128]{1,0:T(8,128)S(1)}, u32[]{:S(2)}, u32[]{:S(2)}) collective-permute-start(f32[16,128]{1,0:T(8,128)S(1)} %get-tuple-element.31), channel_id=1, source_target_pairs={{0,16},{8,24},{16,0},{24,8},{1,17},{9,25},{17,1},{25,9},{2,18},{10... | collective-permute-start | bytes 24584 | tf_op jit(solution)/shard_map/ppermute | solution.py:360
  36.1 5.1 %collective-permute-start.6 = (f32[16,128]{1,0:T(8,128)S(1)}, f32[16,128]{1,0:T(8,128)S(1)}, u32[]{:S(2)}, u32[]{:S(2)}) collective-permute-start(f32[16,128]{1,0:T(8,128)S(1)} %get-tuple-element.32), channel_id=1, source_target_pairs={{0,24},{8,0},{16,8},{24,16},{1,25},{9,1},{17,9},{25,17},{2,26},{10... | collective-permute-start | bytes 24584 | tf_op jit(solution)/shard_map/ppermute | solution.py:360
  38.2 4.9 %collective-permute-start.7 = (f32[16,128]{1,0:T(8,128)S(1)}, f32[16,128]{1,0:T(8,128)S(1)}, u32[]{:S(2)}, u32[]{:S(2)}) collective-permute-start(f32[16,128]{1,0:T(8,128)S(1)} %get-tuple-element.33), channel_id=1, source_target_pairs={{0,8},{8,16},{16,24},{24,0},{1,9},{9,17},{17,25},{25,1},{2,10},{10... | collective-permute-start | bytes 24584 | tf_op jit(solution)/shard_map/ppermute | solution.py:360

commit v8 on v6

--- a/solution.py
+++ b/solution.py
@@ -7,6 +7,7 @@
 from jax.experimental.pallas import tpu as pltpu
 from jax.sharding import Mesh
 from jax.sharding import PartitionSpec as P
+
 
 SP = ("sp_0", "sp_1")
 CH = 128
@@ -105,16 +106,64 @@
     return c1 * c2, c2 * d1 + moved[:, :CH], c2 * b1 - moved[:, CH:] + b2
 
 
-def maps_kernel(
+def pair_maps(k_of, v_of, rows_of):
+    row = iota((CH, CH), 0)
+    col = iota((CH, CH), 1)
+    eye = jnp.where(row == col, 1.0, 0.0)
+    pairs = range(len(k_of))
+    chunks = k_of[0].shape[0] // CH
+    beta = [r[:chunks] for r in rows_of]
+    cum = [r[chunks:] for r in rows_of]
+    total = [jnp.broadcast_to(c[:, CH - 1 : CH], (chunks, CH)) for c in cum]
+    carry = [jnp.exp(t) for t in total]
+    ecum = [jnp.exp(c) for c in cum]
+    columns = [
+        jnp.transpose(
+            jnp.concatenate(
+                [c + jnp.log(b), jnp.exp(t - c), jnp.zeros((CH - 2 * chunks, CH), F32)], axis=0
+            )
+        )
+        for b, c, t in zip(beta, cum, total)
+    ]
+    items = [(p, n) for p in pairs for n in range(chunks)]
+    ks = [k_of[p][n * CH : (n + 1) * CH] for p, n in items]
+    vs = [v_of[p][n * CH : (n + 1) * CH] for p, n in items]
+    grams = [lax.dot_general(k, k, ABT, preferred_element_type=F32) for k in ks]
+    ms = [
+        jnp.where(row > col, g * jnp.exp(columns[p][:, n : n + 1] - cum[p][n : n + 1, :]), 0.0)
+        for (p, n), g in zip(items, grams)
+    ]
+    invs = inverses_of(ms)
+    us = [
+        columns[p][:, chunks + n : chunks + n + 1] * inv * beta[p][n : n + 1, :]
+        for (p, n), inv in zip(items, invs)
+    ]
+    pulls = [
+        dot1(u * ecum[p][n : n + 1, :], k).astype(BF16) for (p, n), u, k in zip(items, us, ks)
+    ]
+    freshs = [dot1(u, v).astype(BF16) for u, v in zip(us, vs)]
+    boths = [
+        dot1(k, jnp.concatenate([pull, fresh], axis=1), ATB)
+        for k, pull, fresh in zip(ks, pulls, freshs)
+    ]
+    maps = [[] for _ in pairs]
+    for (p, n), both in zip(items, boths):
+        maps[p].append((carry[p][n : n + 1, :], both[:, :CH], both[:, CH:]))
+    while len(maps[0]) > 1:
+        maps = [[joined(m[i], m[i + 1], eye) for i in range(0, len(m), 2)] for m in maps]
+    return [(c_row * eye - drop, gain) for ((c_row, drop, gain),) in maps]
+
+
+def far_kernel(
     x_hbm, wk_hbm, wv_hbm, gate_hbm, decay_hbm, bias_hbm, rate_hbm, extra_hbm,
-    o0, o1, o2, o3,
-    xbuf, wkbuf, wvbuf, gatew, extra, bias_ref, rate_ref, kbuf, vbuf, state, sems,
+    o2, o3, o1, k_own, v_own, rows_own,
+    xbuf, wkbuf, wvbuf, gatew, extra, bias_ref, rate_ref, kbuf, vbuf, rows, sems,
 ):
-    tiles, tile, width = xbuf.shape
+    tiles, tile, _ = xbuf.shape
     half = tile // 2
     first_head = lax.axis_index("tp") * 2
     here = lax.axis_index("sp_1")
-    per_seq = kbuf.shape[0] // (2 * CH)
+    chunks = tile // CH
     heads = gate_hbm.shape[0]
     moves = [
         (gate_hbm, gatew.at[pl.ds(0, heads)]),
@@ -126,8 +175,8 @@
     small = len(moves)
     for t in range(tiles):
         for i in range(2):
-            rows = pl.ds(i * half, half)
-            moves.append((x_hbm.at[t, rows], xbuf.at[t, rows]))
+            part = pl.ds(i * half, half)
+            moves.append((x_hbm.at[t, part], xbuf.at[t, part]))
             if t == 0:
                 moves.append(((wk_hbm, wkbuf), (wv_hbm, wvbuf))[i])
     copies = [pltpu.make_async_copy(src, dst, sems.at[i]) for i, (src, dst) in enumerate(moves)]
@@ -135,34 +184,43 @@
         c.start()
     for c in copies[:small]:
         c.wait()
-    arrivals = copies[small:]
+    x00, wk, x01, wv, x10, x11 = copies[small:]
     pick = iota((heads, tile), 0)
-    odd = iota((2, tile), 0) == 1
+    odd = iota((2, CH), 0) == 1
     bias = jnp.where(odd, bias_ref[first_head + 1], bias_ref[first_head])
     rate = jnp.exp(jnp.where(odd, rate_ref[first_head + 1], rate_ref[first_head]))
-    row = iota((CH, CH), 0)
-    col = iota((CH, CH), 1)
-    eye = jnp.where(row == col, 1.0, 0.0)
-    upto = jnp.where(row <= col, 1.0, 0.0).astype(BF16)
+    upto = jnp.where(iota((CH, CH), 0) <= iota((CH, CH), 1), 1.0, 0.0).astype(BF16)
 
     def times(t, i, weights, dims=AB):
         x = xbuf[t, i * half : (i + 1) * half]
         return lax.dot_general(x, weights[...], dims, preferred_element_type=F32)
 
-    def scalars(t, gt):
+    def keys(t, i, kp):
+        kp = silu(kp)
+        for h in range(2):
+            part = unit_rows(kp[:, h * CH : (h + 1) * CH])
+            kbuf[2 * t + h, i * half : (i + 1) * half, :] = part.astype(BF16)
+
+    def values(t, i, vp):
+        vp = silu(vp).astype(BF16)
+        for h in range(2):
+            vbuf[2 * t + h, i * half : (i + 1) * half, :] = vp[:, h * CH : (h + 1) * CH]
+
+    def scalars(t, gts):
+        gt = jnp.concatenate([jnp.transpose(g) for g in gts], axis=1)
         picked = [
             jnp.sum(jnp.where(pick == first_head + h, part, 0.0), axis=0, keepdims=True)
             for part in (gt[:heads], gt[heads:])
             for h in range(2)
         ]
+        gate = jnp.concatenate(picked[:2], axis=0)
         z = jnp.concatenate(picked[2:], axis=0)
         soft = jnp.maximum(z, 0.0) + jnp.log1p(jnp.exp(-jnp.abs(z)))
-        gate = jnp.concatenate(picked[:2], axis=0) + bias
         steps, gates = [], []
-        for n in range(per_seq):
+        for n in range(chunks):
             lanes = slice(n * CH, (n + 1) * CH)
-            steps.append(extra[t * per_seq + n] - rate[:, lanes] * soft[:, lanes])
-            gates.append(gate[:, lanes])
+            steps.append(extra[t * chunks + n] - rate * soft[:, lanes])
+            gates.append(gate[:, lanes] + bias)
         step = jnp.concatenate(steps, axis=0)
         beta = 1.0 / (1.0 + jnp.exp(-jnp.concatenate(gates, axis=0)))
         hi = step.astype(BF16)
@@ -170,45 +228,12 @@
         mid = rest.astype(BF16)
         low = (rest - mid.astype(F32)).astype(BF16)
         cum = dot1(hi, upto) + (dot1(mid, upto) + dot1(low, upto))
-        count = cum.shape[0]
-        total = jnp.broadcast_to(cum[:, CH - 1 : CH], (count, CH))
-        columns = jnp.transpose(
-            jnp.concatenate(
-                [cum + jnp.log(beta), jnp.exp(total - cum), jnp.zeros((CH - 2 * count, CH), F32)], axis=0
-            )
-        )
-        return beta, cum, jnp.exp(total), jnp.exp(cum), columns
-
-    def weighted(t, kp, rows):
-        kp = silu(kp)
         for h in range(2):
-            lanes = slice(h * CH, (h + 1) * CH)
-            kbuf[rows, lanes] = unit_rows(kp[:, lanes]).astype(BF16)
-
-    def matrices(t, cum, columns):
-        ms = []
-        for n in range(per_seq):
-            for h in range(2):
-                k = part(kbuf, t, n, h)
-                gram = lax.dot_general(k, k, ABT, preferred_element_type=F32)
+            for n in range(chunks):
                 r = 2 * n + h
-                ms.append(jnp.where(row > col, gram * jnp.exp(columns[:, r : r + 1] - cum[r : r + 1, :]), 0.0))
-        return ms
-
-    def part(buf, s, n, h):
-        start = (s * per_seq + n) * CH
-        return buf[start : start + CH, h * CH : (h + 1) * CH]
-
-    def keys(t, i, kp):
-        weighted(t, kp, slice(t * tile + i * half, t * tile + (i + 1) * half))
-
-    def values(t, i, vp):
-        vbuf[t * tile + i * half : t * tile + (i + 1) * half, :] = silu(vp).astype(BF16)
-
-    def rows_from(t, gts):
-        return scalars(t, jnp.concatenate([jnp.transpose(g) for g in gts], axis=1))
-
-    x00, wk, x01, wv, x10, x11 = arrivals
+                rows[2 * t + h, n : n + 1, :] = beta[r : r + 1, :]
+                rows[2 * t + h, chunks + n : chunks + n + 1, :] = cum[r : r + 1, :]
+
     x00.wait()
     wk.wait()
     g00 = times(0, 0, gatew, ABT)
@@ -225,54 +250,30 @@
     x11.wait()
     g10 = times(1, 0, gatew, ABT)
     k10 = times(1, 0, wkbuf)
-    rows_of = [rows_from(0, (g00, g01))]
+    scalars(0, (g00, g01))
     g11 = times(1, 1, gatew, ABT)
     k11 = times(1, 1, wkbuf)
     values(0, 0, v00)
     values(0, 1, v01)
-    rows_of.append(rows_from(1, (g10, g11)))
+    scalars(1, (g10, g11))
     keys(1, 0, k10)
     v10 = times(1, 0, wvbuf)
     v11 = times(1, 1, wvbuf)
-    ms = matrices(0, rows_of[0][1], rows_of[0][4])
     keys(1, 1, k11)
-    ms += matrices(1, rows_of[1][1], rows_of[1][4])
     values(1, 0, v10)
     values(1, 1, v11)
-
-    items = [(s, n, h) for s in range(2) for n in range(per_seq) for h in range(2)]
-    invs = inverses_of(ms)
-    us = []
-    for (s, n, h), inv in zip(items, invs):
-        beta, _, _, _, columns = rows_of[s]
-        r = 2 * n + h
-        us.append(columns[:, 8 + r : 9 + r] * inv * beta[r : r + 1, :])
-    pulls = [
-        dot1(u * rows_of[s][3][2 * n + h : 2 * n + h + 1, :], part(kbuf, s, n, h)).astype(BF16)
-        for (s, n, h), u in zip(items, us)
-    ]
-    freshs = [dot1(u, part(vbuf, s, n, h)).astype(BF16) for (s, n, h), u in zip(items, us)]
-    boths = {
-        (s, n, h): dot1(part(kbuf, s, n, h), jnp.concatenate([pull, fresh], axis=1), ATB)
-        for (s, n, h), pull, fresh in zip(items, pulls, freshs)
-    }
-    maps = []
-    for p in range(4):
-        s, h = divmod(p, 2)
-        parts = []
-        for n in range(per_seq):
-            c_row = rows_of[s][2][2 * n + h : 2 * n + h + 1, :]
-            parts.append((c_row, boths[s, n, h][:, :CH], boths[s, n, h][:, CH:]))
-        maps.append(parts)
-    while len(maps[0]) > 1:
-        maps = [[joined(m[i], m[i + 1], eye) for i in range(0, len(m), 2)] for m in maps]
-    for p in range(4):
-        c_row, drop, gain = maps[p][0]
-        state[p, :CH, :] = c_row * eye - drop
-        state[p, CH:, :] = gain
-
-    for k, o in zip(SHIFTS, (o0, o1, o2, o3)):
-        o[...] = state[lax.rem(here + k, 4)]
+    others = [jnp.bitwise_xor(here, bit) for bit in (2, 3, 1)]
+    maps = pair_maps([kbuf[p] for p in others], [vbuf[p] for p in others], [rows[p] for p in others])
+    for o, (amap, gain) in zip((o2, o3, o1), maps):
+        o[:CH, :] = amap
+        o[CH:, :] = gain
+    k_own[...] = kbuf[here]
+    v_own[...] = vbuf[here]
+    rows_own[...] = rows[here]
+
+
+def own_kernel(k_own, v_own, rows_own, out):
+    out[:CH, :], out[CH:, :] = pair_maps([k_own[...]], [v_own[...]], [rows_own[...]])[0]
 
 
 def after(first, second):
@@ -282,8 +283,8 @@
 
 def segments_kernel(r0, r1, r2, r3, out, scr):
     here = lax.axis_index("sp_1")
-    for k, ref in zip(SHIFTS, (r0, r1, r2, r3)):
-        scr[lax.rem(here + 4 - k, 4)] = ref[...]
+    for k, ref in enumerate((r0, r1, r2, r3)):
+        scr[jnp.bitwise_xor(here, k)] = ref[...]
     maps = [(scr[t, :CH, :], scr[t, CH:, :]) for t in range(4)]
     while len(maps) > 1:
         maps = [after(maps[i], maps[i + 1]) for i in range(0, len(maps), 2)]
@@ -394,32 +395,34 @@
 ):
     seqs, seg, width = tokens.shape
     cols = key_matrix.shape[1]
-    tile = seg
-    tiles = seqs * seg // tile
+    gate_count = gate_matrix.shape[1]
     chunks = seqs * seg // CH
     extra = jnp.transpose(extra_log_decay.reshape(chunks, CH, 2), (0, 2, 1))
     hbm = pl.BlockSpec(memory_space=pltpu.HBM)
     smem = pl.BlockSpec(memory_space=pltpu.SMEM)
-    maps = pl.pallas_call(
-        maps_kernel,
-        out_shape=[jax.ShapeDtypeStruct((2 * CH, CH), F32)] * 4,
+    tiles = seqs
+    far2, far3, far1, *kept = pl.pallas_call(
+        far_kernel,
+        out_shape=[jax.ShapeDtypeStruct((2 * CH, CH), F32)] * 3
+        + [jax.ShapeDtypeStruct((seg, CH), BF16)] * 2
+        + [jax.ShapeDtypeStruct((2 * seg // CH, CH), F32)],
         in_specs=[hbm] * 8,
-        out_specs=vmem(4),
+        out_specs=vmem(6),
         scratch_shapes=[
-            pltpu.VMEM((tiles, tile, width), BF16),
+            pltpu.VMEM((tiles, seg, width), BF16),
             pltpu.VMEM((width, cols), BF16),
             pltpu.VMEM((width, cols), BF16),
-            pltpu.VMEM((2 * gate_matrix.shape[1], width), BF16),
+            pltpu.VMEM((2 * gate_count, width), BF16),
             pltpu.VMEM((chunks, 2, CH), F32),
             pltpu.SMEM(gate_bias_offset.shape, F32),
             pltpu.SMEM(head_log_decay_rate.shape, F32),
-            pltpu.VMEM((seqs * seg, cols), BF16),
-            pltpu.VMEM((seqs * seg, cols), BF16),
-            pltpu.VMEM((4, 2 * CH, CH), F32),
+            pltpu.VMEM((4, seg, CH), BF16),
+            pltpu.VMEM((4, seg, CH), BF16),
+            pltpu.VMEM((4, 2 * seg // CH, CH), F32),
             pltpu.SemaphoreType.DMA((11,)),
         ],
         compiler_params=pltpu.CompilerParams(vmem_limit_bytes=24 * 2**20),
-        name="maps",
+        name="far",
     )(
         *(
             pltpu.with_memory_space_constraint(a, pltpu.HBM)
@@ -435,6 +438,19 @@
             )
         )
     )
+    arrived = []
+    for array, bit in ((far2, 2), (far3, 3), (far1, 1)):
+        arrived.append(swap(array, "sp_1", bit))
+    near = pl.pallas_call(
+        own_kernel,
+        out_shape=jax.ShapeDtypeStruct((2 * CH, CH), F32),
+        in_specs=vmem(3),
+        out_specs=vmem(1)[0],
+        compiler_params=pltpu.CompilerParams(vmem_limit_bytes=16 * 2**20),
+        cost_estimate=pl.CostEstimate(flops=10**9, bytes_accessed=10**6, transcendentals=0),
+        name="near",
+    )
+    mine = near(*kept)
     small = pltpu.CompilerParams(vmem_limit_bytes=8 * 2**20)
     segment = pl.pallas_call(
         segments_kernel,
@@ -444,7 +460,7 @@
         scratch_shapes=[pltpu.VMEM((4, 2 * CH, CH), F32)],
         compiler_params=small,
         name="segments",
-    )(*spread(maps, "sp_1"))
+    )(mine, arrived[2], arrived[0], arrived[1])
     token = pl.pallas_call(
         token_kernel,
         out_shape=jax.ShapeDtypeStruct((8 + ROWS, CH), F32),

time: 41.8 us -> 41.9 us (level)
  starting transfers between devices: 15.6 us -> 12.3 us
  Pallas kernels: 11.4 us -> 13.3 us
  waiting for transfers between devices: 14 us -> 15.1 us
    ppermute x6 -> x3, starting transfers between devices: 10.2 us -> 2.13 us  [spread(): lax.ppermute(a, axis, [(i, (i + k) % 4) for i in range(4)])]
    ppermute x2 -> x5, waiting for transfers between devices: 4.55 us -> 10.2 us  [swap(): return lax.ppermute(array, axis, [(i, i ^ bit) for i in range(4)])]
    ppermute x2 -> x5, starting transfers between devices: 5.4 us -> 10.2 us  [swap(): return lax.ppermute(array, axis, [(i, i ^ bit) for i in range(4)])]
    ppermute x6 -> x3, waiting for transfers between devices: 9.44 us -> 4.84 us  [spread(): lax.ppermute(a, axis, [(i, (i + k) % 4) for i in range(4)])]
    pallas_call x1 -> x2, Pallas kernels: 9.01 us -> 10.9 us  [the longest x1 8.6 us: shards(): pl.pallas_call(far_kernel, out_shape=[jax.ShapeDtypeStruct((2 * CH, CH),...]
  transfers between devices with their start and end apart: 8 -> 8, of which waited for: 8 -> 6; matrix products, arithmetic and copies ran while one was open for 0% -> 0% of each run, Pallas kernels for 2% -> 7%
where the time goes in v8:
time: 41.9 us; the launch traced here: 41.4 us
  waiting for transfers between devices  15.1 us (36%)
  Pallas kernels  13.3 us (32%)
  starting transfers between devices  12.3 us (29%)
  between operations  0.74 us (2%)
    ppermute x5, waiting for transfers between devices, swap(): return lax.ppermute(array, axis, [(i, i ^ bit) for i in range(4)])  10.2 us
    ppermute x5, starting transfers between devices, swap(): return lax.ppermute(array, axis, [(i, i ^ bit) for i in range(4)])  10.2 us
    pallas_call x1, Pallas kernels, shards(): pl.pallas_call(far_kernel, out_shape=[jax.ShapeDtypeStruct((2 * CH, CH),...  8.6 us
    ppermute x3, waiting for transfers between devices, spread(): lax.ppermute(a, axis, [(i, (i + k) % 4) for i in range(4)])  4.84 us
    pallas_call x1, Pallas kernels, shards(): mine = near(*kept)  2.31 us
    ppermute x3, starting transfers between devices, spread(): lax.ppermute(a, axis, [(i, (i + k) % 4) for i in range(4)])  2.13 us
  transfers between devices with their start and end apart: 8, of which 6 were waited for; matrix products, arithmetic and copies ran while one was open for 0% of the time, Pallas kernels for 7%

profile of v8, /device:TPU:2, one launch (start us, length us, event | category | flops | bytes accessed | tf_op | source)
XLA Modules:
  0.0 41.4 jit_solution(3328644636943108334)
XLA Ops:
  0.7 8.6 %far.1 = (f32[256,128]{1,0:T(8,128)S(1)}, f32[256,128]{1,0:T(8,128)S(1)}, f32[256,128]{1,0:T(8,128)S(1)}, bf16[512,128]{1,0:T(8,128)(2,1)S(1)}, bf16[512,128]{1,0:T(8,128)(2,1)S(1)}, /*index=5*/f32[8,128]{1,0:T(8,128)S(1)}) custom-call(bf16[2,512,2048]{2,1,0:T(8,128)(2,1)} %x_hbm.1, bf16[2048,256]{1,0:T(8,128)(2,1)} %wk_hbm.1, bf16[2048,256]{1,0:T(8,128)(2,1)} %wv_hbm.1, ...), custom_call_target="tpu_custom_call" | custom-call | tf_op jit(solution)/shard_map/far/pallas_call | solution.py:404
  9.3 1.7 %collective-permute-start = (f32[256,128]{1,0:T(8,128)S(1)}, f32[256,128]{1,0:T(8,128)S(1)}, u32[]{:S(2)}, u32[]{:S(2)}) collective-permute-start(f32[256,128]{1,0:T(8,128)S(1)} %get-tuple-element.17), channel_id=1, source_target_pairs={{0,8},{8,0},{16,24},{24,16},{1,9},{9,1},{17,25},{25,17},{2,10},{10... | collective-permute-start | bytes 393224 | tf_op jit(solution)/shard_map/ppermute | solution.py:378
  11.0 2.9 %collective-permute-start.1 = (f32[256,128]{1,0:T(8,128)S(1)}, f32[256,128]{1,0:T(8,128)S(1)}, u32[]{:S(2)}, u32[]{:S(2)}) collective-permute-start(f32[256,128]{1,0:T(8,128)S(1)} %get-tuple-element.18), channel_id=1, source_target_pairs={{0,16},{8,24},{16,0},{24,8},{1,17},{9,25},{17,1},{25,9},{2,18},{10... | collective-permute-start | bytes 393224 | tf_op jit(solution)/shard_map/ppermute | solution.py:378
  13.9 0.2 collective-permute-start.2
  14.1 2.3 %near.1.r0 = f32[256,128]{1,0:T(8,128)S(1)} custom-call(bf16[512,128]{1,0:T(8,128)(2,1)S(1)} %get-tuple-element.14.k_own, bf16[512,128]{1,0:T(8,128)(2,1)S(1)} %get-tuple-element.15.v_own, f32[8,128]{1,0:T(8,128)S(1)} %get-tuple-element.16.rows_own), custom_call_target="tpu_custom_call" | custom-call | flops 1000000000 | bytes 1000000 | tf_op jit(solution)/shard_map/near/pallas_call | solution.py:453
  16.4 0.0 collective-permute-done.r1
  16.4 3.6 %collective-permute-done.1.r2 = f32[256,128]{1,0:T(8,128)S(1)} collective-permute-done((f32[256,128]{1,0:T(8,128)S(1)}, f32[256,128]{1,0:T(8,128)S(1)}, u32[]{:S(2)}, u32[]{:S(2)}) %collective-permute-start.1) | collective-permute-done | bytes 131104 | tf_op jit(solution)/shard_map/ppermute | solution.py:378
  20.0 2.1 %collective-permute-done.2.r3 = f32[256,128]{1,0:T(8,128)S(1)} collective-permute-done((f32[256,128]{1,0:T(8,128)S(1)}, f32[256,128]{1,0:T(8,128)S(1)}, u32[]{:S(2)}, u32[]{:S(2)}) %collective-permute-start.2) | collective-permute-done | bytes 131104 | tf_op jit(solution)/shard_map/ppermute | solution.py:378
  22.1 0.5 %segments.1.own = f32[256,128]{1,0:T(8,128)S(1)} custom-call(f32[256,128]{1,0:T(8,128)S(1)} %near.1.r0, f32[256,128]{1,0:T(8,128)S(1)} %collective-permute-done.r1, f32[256,128]{1,0:T(8,128)S(1)} %collective-permute-done.1.r2, f32[256,128]{1,0:T(8,128)S(1)} %collective-permute-done.2.r3), custom_call_target="tpu_custom_call" | custom-call | tf_op jit(solution)/shard_map/segments/pallas_call | solution.py:455
  22.6 2.0 %collective-permute-start.3 = (f32[256,128]{1,0:T(8,128)S(1)}, f32[256,128]{1,0:T(8,128)S(1)}, u32[]{:S(2)}, u32[]{:S(2)}) collective-permute-start(f32[256,128]{1,0:T(8,128)S(1)} %segments.1.own), channel_id=1, source_target_pairs={{0,32},{32,0},{64,96},{96,64},{1,33},{33,1},{65,97},{97,65},{2,34}... | collective-permute-start | bytes 393224 | tf_op jit(solution)/shard_map/ppermute | solution.py:378
  24.6 0.0 copy-done
  24.6 0.7 %token_.1.token = f32[40,128]{1,0:T(8,128)S(1)} custom-call(bf16[2,2,128]{2,1,0:T(2,128)(2,1)S(1)} %copy-done, bf16[2,2,128]{2,1,0:T(2,128)(2,1)S(1)} %copy-done.1, bf16[2,2,128]{2,1,0:T(2,128)(2,1)S(1)} %copy-done.2, f32[2,2]{1,0:T(2,128)S(1)} %copy-done.3), custom_call_target="tpu_custom_call" | custom-call | tf_op jit(solution)/shard_map/token/pallas_call | solution.py:464
  25.4 2.3 %collective-permute-done.3.other = f32[256,128]{1,0:T(8,128)S(1)} collective-permute-done((f32[256,128]{1,0:T(8,128)S(1)}, f32[256,128]{1,0:T(8,128)S(1)}, u32[]{:S(2)}, u32[]{:S(2)}) %collective-permute-start.3) | collective-permute-done | bytes 131104 | tf_op jit(solution)/shard_map/ppermute | solution.py:378
  27.7 0.2 halves.1
  27.9 3.4 %collective-permute-start.4 = (f32[128,128]{1,0:T(8,128)S(1)}, f32[128,128]{1,0:T(8,128)S(1)}, u32[]{:S(2)}, u32[]{:S(2)}) collective-permute-start(f32[128,128]{1,0:T(8,128)S(1)} %get-tuple-element.21), channel_id=1, source_target_pairs={{0,64},{32,96},{64,0},{96,32},{1,65},{33,97},{65,1},{97,33},{2,66}... | collective-permute-start | bytes 196616 | tf_op jit(solution)/shard_map/ppermute | solution.py:378
  31.3 2.2 %collective-permute-done.4.theirs = f32[128,128]{1,0:T(8,128)S(1)} collective-permute-done((f32[128,128]{1,0:T(8,128)S(1)}, f32[128,128]{1,0:T(8,128)S(1)}, u32[]{:S(2)}, u32[]{:S(2)}) %collective-permute-start.4) | collective-permute-done | bytes 65568 | tf_op jit(solution)/shard_map/ppermute | solution.py:378
  33.6 0.3 rows.1
  33.8 0.0 collective-permute-start.5
  33.9 2.1 %collective-permute-start.6 = (f32[16,128]{1,0:T(8,128)S(1)}, f32[16,128]{1,0:T(8,128)S(1)}, u32[]{:S(2)}, u32[]{:S(2)}) collective-permute-start(f32[16,128]{1,0:T(8,128)S(1)} %get-tuple-element.24), channel_id=1, source_target_pairs={{0,24},{8,0},{16,8},{24,16},{1,25},{9,1},{17,9},{25,17},{2,26},{10... | collective-permute-start | bytes 24584 | tf_op jit(solution)/shard_map/ppermute | solution.py:372
  36.0 0.0 collective-permute-start.7
  36.0 3.0 %collective-permute-done.5.r1 = f32[16,128]{1,0:T(8,128)S(1)} collective-permute-done((f32[16,128]{1,0:T(8,128)S(1)}, f32[16,128]{1,0:T(8,128)S(1)}, u32[]{:S(2)}, u32[]{:S(2)}) %collective-permute-start.5) | collective-permute-done | bytes 8224 | tf_op jit(solution)/shard_map/ppermute | solution.py:372
  39.0 0.0 collective-permute-done.6.r2
  39.0 1.8 %collective-permute-done.7.r3 = f32[16,128]{1,0:T(8,128)S(1)} collective-permute-done((f32[16,128]{1,0:T(8,128)S(1)}, f32[16,128]{1,0:T(8,128)S(1)}, u32[]{:S(2)}, u32[]{:S(2)}) %collective-permute-start.7) | collective-permute-done | bytes 8224 | tf_op jit(solution)/shard_map/ppermute | solution.py:372
  40.8 0.6 %finish.1 = (bf16[2,2,8,128]{3,2,1,0:T(8,128)(2,1)}, bf16[2,2,128]{2,1,0:T(2,128)(2,1)}) custom-call(f32[16,128]{1,0:T(8,128)S(1)} %get-tuple-element.22.r0, f32[16,128]{1,0:T(8,128)S(1)} %collective-permute-done.5.r1, f32[16,128]{1,0:T(8,128)S(1)} %collective-permute-done.6.r2, f32[16,128]{1,0:T(8,128)S(1)} %collective-permute-done.7.r3), custom_call_target="tpu_custom_call" | custom-call | tf_op jit(solution)/shard_map/finish/pallas_call | solution.py:494
  (9 shorter events, 0.0 us)
Async XLA Ops:
  0.6 24.0 %copy-start = (bf16[2,2,128]{2,1,0:T(2,128)(2,1)S(1)}, bf16[2,2,128]{2,1,0:T(2,128)(2,1)}, u32[]{:S(2)}) copy-start(bf16[2,2,128]{2,1,0:T(2,128)(2,1)} %query_ref.1) | copy-start | bytes 3076
  0.6 24.0 %copy-start.1 = (bf16[2,2,128]{2,1,0:T(2,128)(2,1)S(1)}, bf16[2,2,128]{2,1,0:T(2,128)(2,1)}, u32[]{:S(2)}) copy-start(bf16[2,2,128]{2,1,0:T(2,128)(2,1)} %key_ref.1) | copy-start | bytes 3076
  0.7 24.0 %copy-start.2 = (bf16[2,2,128]{2,1,0:T(2,128)(2,1)S(1)}, bf16[2,2,128]{2,1,0:T(2,128)(2,1)}, u32[]{:S(2)}) copy-start(bf16[2,2,128]{2,1,0:T(2,128)(2,1)} %value_ref.1) | copy-start | bytes 3076
  0.7 24.0 %copy-start.3 = (f32[2,2]{1,0:T(2,128)S(1)}, f32[2,2]{1,0:T(2,128)}, u32[]{:S(2)}) copy-start(f32[2,2]{1,0:T(2,128)} %gate_ref.1) | copy-start | bytes 52
  0.7 32.9 %copy-start.4 = (f32[128]{0:T(128)S(1)}, f32[128]{0:T(128)}, u32[]{:S(2)}) copy-start(f32[128]{0:T(128)} %param.25) | copy-start | bytes 1540
  9.3 7.1 %collective-permute-start = (f32[256,128]{1,0:T(8,128)S(1)}, f32[256,128]{1,0:T(8,128)S(1)}, u32[]{:S(2)}, u32[]{:S(2)}) collective-permute-start(f32[256,128]{1,0:T(8,128)S(1)} %get-tuple-element.17), channel_id=1, source_target_pairs={{0,8},{8,0},{16,24},{24,16},{1,9},{9,1},{17,25},{25,17},{2,10},{10... | collective-permute-start | bytes 393224 | tf_op jit(solution)/shard_map/ppermute | solution.py:378
  11.0 9.0 %collective-permute-start.1 = (f32[256,128]{1,0:T(8,128)S(1)}, f32[256,128]{1,0:T(8,128)S(1)}, u32[]{:S(2)}, u32[]{:S(2)}) collective-permute-start(f32[256,128]{1,0:T(8,128)S(1)} %get-tuple-element.18), channel_id=1, source_target_pairs={{0,16},{8,24},{16,0},{24,8},{1,17},{9,25},{17,1},{25,9},{2,18},{10... | collective-permute-start | bytes 393224 | tf_op jit(solution)/shard_map/ppermute | solution.py:378
  13.9 8.2 %collective-permute-start.2 = (f32[256,128]{1,0:T(8,128)S(1)}, f32[256,128]{1,0:T(8,128)S(1)}, u32[]{:S(2)}, u32[]{:S(2)}) collective-permute-start(f32[256,128]{1,0:T(8,128)S(1)} %get-tuple-element.19), channel_id=1, source_target_pairs={{0,24},{8,16},{16,8},{24,0},{1,25},{9,17},{17,9},{25,1},{2,26},{10... | collective-permute-start | bytes 393224 | tf_op jit(solution)/shard_map/ppermute | solution.py:378
  22.6 5.1 %collective-permute-start.3 = (f32[256,128]{1,0:T(8,128)S(1)}, f32[256,128]{1,0:T(8,128)S(1)}, u32[]{:S(2)}, u32[]{:S(2)}) collective-permute-start(f32[256,128]{1,0:T(8,128)S(1)} %segments.1.own), channel_id=1, source_target_pairs={{0,32},{32,0},{64,96},{96,64},{1,33},{33,1},{65,97},{97,65},{2,34}... | collective-permute-start | bytes 393224 | tf_op jit(solution)/shard_map/ppermute | solution.py:378
  27.9 5.6 %collective-permute-start.4 = (f32[128,128]{1,0:T(8,128)S(1)}, f32[128,128]{1,0:T(8,128)S(1)}, u32[]{:S(2)}, u32[]{:S(2)}) collective-permute-start(f32[128,128]{1,0:T(8,128)S(1)} %get-tuple-element.21), channel_id=1, source_target_pairs={{0,64},{32,96},{64,0},{96,32},{1,65},{33,97},{65,1},{97,33},{2,66}... | collective-permute-start | bytes 196616 | tf_op jit(solution)/shard_map/ppermute | solution.py:378
  33.8 5.2 %collective-permute-start.5 = (f32[16,128]{1,0:T(8,128)S(1)}, f32[16,128]{1,0:T(8,128)S(1)}, u32[]{:S(2)}, u32[]{:S(2)}) collective-permute-start(f32[16,128]{1,0:T(8,128)S(1)} %get-tuple-element.23), channel_id=1, source_target_pairs={{0,16},{8,24},{16,0},{24,8},{1,17},{9,25},{17,1},{25,9},{2,18},{10... | collective-permute-start | bytes 24584 | tf_op jit(solution)/shard_map/ppermute | solution.py:372
  33.9 5.1 %collective-permute-start.6 = (f32[16,128]{1,0:T(8,128)S(1)}, f32[16,128]{1,0:T(8,128)S(1)}, u32[]{:S(2)}, u32[]{:S(2)}) collective-permute-start(f32[16,128]{1,0:T(8,128)S(1)} %get-tuple-element.24), channel_id=1, source_target_pairs={{0,24},{8,0},{16,8},{24,16},{1,25},{9,1},{17,9},{25,17},{2,26},{10... | collective-permute-start | bytes 24584 | tf_op jit(solution)/shard_map/ppermute | solution.py:372
  36.0 4.9 %collective-permute-start.7 = (f32[16,128]{1,0:T(8,128)S(1)}, f32[16,128]{1,0:T(8,128)S(1)}, u32[]{:S(2)}, u32[]{:S(2)}) collective-permute-start(f32[16,128]{1,0:T(8,128)S(1)} %get-tuple-element.25), channel_id=1, source_target_pairs={{0,8},{8,16},{16,24},{24,0},{1,9},{9,17},{17,25},{25,1},{2,10},{10... | collective-permute-start | bytes 24584 | tf_op jit(solution)/shard_map/ppermute | solution.py:372
